TPU v7x, 512 devices: a whole 4x4x16 slice. The times are simulated.
512 devices in a mesh: kv: 16 (over y, x), tp: 32 (over z, core).
Axes of the slice: x: 4, y: 4, z: 16, core: 2. Of those that a mesh axis runs over, the one named last changes fastest.
Arguments:
- tokens: bfloat16 [2048, 2048], P('tp', 'kv'), may hold values from -16 to 16
- lengths: int32 [2048], P('tp'), may hold values from 1 to 8192, 2097152 in all
- query_weight: bfloat16 [2048, 1024], P(None, 'kv'), may hold values from -0.125 to 0.125
- key_weight: bfloat16 [2048, 1024], P(None, 'kv'), may hold values from -0.125 to 0.125
- value_weight: bfloat16 [2048, 1024], P(None, 'kv'), may hold values from -0.125 to 0.125
- gate_weight: bfloat16 [2048, 1024], P(None, 'kv'), may hold values from -0.125 to 0.125
- output_weight: bfloat16 [1024, 2048], P('kv'), may hold values from -0.1875 to 0.1875
- mixer_gain: float32 [2048], replicated, may hold values from 0.1 to 1.9
- group_gain: float32 [1024], P('kv'), may hold values from 0.1 to 1.9
- channel_gain: float32 [2048], P('kv'), may hold values from 0.1 to 1.9
- up_weight: bfloat16 [2048, 8192], P('kv', 'tp'), may hold values from -0.125 to 0.125
- down_weight: bfloat16 [8192, 2048], P('tp', 'kv'), may hold values from -0.0625 to 0.0625
- memory_state: float32 [2048, 16, 64, 64], P('tp', 'kv'), may hold values from -0.6 to 0.6
Outputs:
- mixed: bfloat16 [2048, 2048], P('tp', 'kv')
- new_state: float32 [2048, 16, 64, 64], P('tp', 'kv')
All inputs are finite; a program needn't handle non-finite values. No bound on the sum of `lengths` on one device may be relied on, other than what follows from the above.
Results may differ from a plain program's by a relative error of at most 0.012.
Values may be sent and summed in bfloat16 or wider, within the bound.
No kernel may reach another device: no remote copies, remote signals or barrier semaphores. Data moves between devices by JAX's collectives and lax.ppermute only.
A program may use at most 64 MiB of HBM per device.

v0:
```python
import jax
import jax.numpy as jnp
import numpy as np
from jax import lax
from jax.sharding import Mesh
from jax.sharding import PartitionSpec as P

D = 2048
HEADS = 16
HEAD_DIM = 64
EPS = 1e-06
THETA = 10000.0

KV = ("y", "xh", "xl")
TP = ("b3", "b2", "b1", "b0", "c")
KAPPA = ("y", "xh")
RHO = ("xl",)
PLANES = ("b1", "b0", "c")
FAR = ("b3", "b2")


def size_of(axes):
    return int(np.prod([lax.axis_size(a) for a in axes]))


def swap(blocks, axes):
    return lax.all_to_all(blocks, axes, split_axis=0, concat_axis=0, tiled=True)


def to_all(value, axes):
    return swap(jnp.broadcast_to(value, (size_of(axes), *value.shape)), axes)


def rotate(vectors, position):
    breadth = vectors.shape[-1]
    middle = breadth // 2
    inverse = THETA ** (-jnp.arange(middle, dtype=jnp.float32) * 2.0 / breadth)
    angles = position.astype(jnp.float32)[:, None] * inverse[None, :]
    cosine = jnp.cos(angles)
    sine = jnp.sin(angles)
    former = vectors[..., :middle]
    latter = vectors[..., middle:]
    return jnp.concatenate(
        [former * cosine - latter * sine, former * sine + latter * cosine], axis=-1
    )


def layer(
    tokens,
    lengths,
    query_weight,
    key_weight,
    value_weight,
    gate_weight,
    output_weight,
    mixer_gain,
    group_gain,
    channel_gain,
    up_weight,
    down_weight,
    memory_state,
):
    bf16, f32 = jnp.bfloat16, jnp.float32
    served, feats = tokens.shape
    kv, kappa, rho = size_of(KV), size_of(KAPPA), size_of(RHO)
    planes, far = size_of(PLANES), size_of(FAR)
    wide = feats * rho
    units = up_weight.shape[1] // rho

    up_cut = jnp.moveaxis(up_weight.reshape(feats, rho, units), 1, 0)
    down_cut = down_weight.reshape(rho, units, feats)
    first = channel_gain.astype(bf16)
    rest = channel_gain - first.astype(f32)
    second = rest.astype(bf16)
    third = (rest - second.astype(f32)).astype(bf16)
    gain_rows = jnp.concatenate(
        [first[None], second[None], third[None], jnp.zeros((5, feats), bf16)]
    )
    gain_rows = jnp.broadcast_to(gain_rows, (rho, *gain_rows.shape))
    both = jnp.concatenate(
        [up_cut.reshape(rho, -1, 128), down_cut.reshape(rho, -1, 128), gain_rows], axis=1
    )
    side = lax.axis_index(RHO)
    got = lax.ppermute(both[1 - side], RHO, [(0, 1), (1, 0)])
    pair = jnp.where(side == 0, jnp.stack([both[0], got]), jnp.stack([got, both[1]]))
    pairs = [pair]
    for step in (2, 1, 3):
        pairs.append(lax.ppermute(pair, FAR, [(i, (i + step) % far) for i in range(far)]))
    half = (pair.shape[1] - 8) // 2
    up = jnp.concatenate([p[:, :half].reshape(wide, units) for p in pairs], axis=1)
    down = jnp.concatenate(
        [jnp.moveaxis(p[:, half : 2 * half], 0, 1).reshape(units, wide) for p in pairs]
    )
    pieces = pair[:, 2 * half :].astype(f32)
    gains = (pieces[:, 0] + pieces[:, 1] + pieces[:, 2]).reshape(wide)

    blocks = to_all(tokens, KV)
    whole_rows = jnp.moveaxis(blocks, 0, 1).reshape(served, kv * feats)
    widened = whole_rows.astype(f32)
    normed = (
        widened * lax.rsqrt(jnp.mean(widened * widened, axis=1, keepdims=True) + EPS) * mixer_gain
    ).astype(bf16)

    def project(weight):
        return jnp.dot(normed, weight, preferred_element_type=f32)

    queries = rotate(project(query_weight), lengths)
    keys_new = rotate(project(key_weight), lengths) * HEAD_DIM ** (-0.5)
    values_new = project(value_weight)
    gating = project(gate_weight)
    head = lax.axis_index(KV).astype(f32)
    decay = 1.0 - 2.0 ** (-5.0 - 5.0 * head / (HEADS - 1))
    new_state = decay * memory_state[:, 0] + keys_new[:, :, None] * values_new[:, None, :]
    readout = jnp.einsum("bkv,bk->bv", new_state, queries, precision=lax.Precision.HIGHEST)
    grouped = readout * lax.rsqrt(jnp.mean(readout * readout, axis=-1, keepdims=True) + EPS)
    merged = (grouped * group_gain * jax.nn.silu(gating)).astype(bf16)
    shares = jnp.dot(merged, output_weight, preferred_element_type=f32).astype(bf16)

    shares = jnp.moveaxis(shares.reshape(served, kappa, wide), 1, 0)
    shares = jnp.broadcast_to(shares[:, None], (kappa, rho, served, wide)).reshape(kv, served, wide)
    shares = swap(shares, KV)
    mixed_part = jnp.sum(shares.astype(f32), axis=0)
    at = lax.axis_index(KAPPA) * rho
    own = jnp.moveaxis(lax.dynamic_slice_in_dim(blocks, at, rho, 0), 0, 1).reshape(served, wide)
    after_wide = (own.astype(f32) + mixed_part).astype(bf16)

    rows = to_all(after_wide, PLANES).reshape(planes * served, wide)
    residual = rows.astype(f32)
    squares = jnp.sum(residual * residual, axis=1)
    scaled = (residual * gains).astype(bf16)
    raised_part = jnp.dot(scaled, up, preferred_element_type=f32).astype(bf16)
    part = planes * served // kappa
    hidden_units = far * units
    extra = jnp.zeros((kappa, 8, hidden_units), bf16)
    high = squares.astype(bf16)
    low = (squares - high.astype(f32)).astype(bf16)
    extra = extra.at[:, 0, :part].set(high.reshape(kappa, part))
    extra = extra.at[:, 1, :part].set(low.reshape(kappa, part))
    sent = jnp.concatenate([raised_part.reshape(kappa, part, hidden_units), extra], axis=1)
    arrived = jnp.sum(swap(sent, KAPPA).astype(f32), axis=0)
    raised = arrived[:part]
    totals = arrived[part, :part] + arrived[part + 1, :part]
    factor = lax.rsqrt(totals / D + EPS)
    hidden = jnp.square(jax.nn.relu(raised * factor[:, None])).astype(bf16)
    hidden = to_all(hidden, KAPPA).reshape(planes * served, hidden_units)
    lowered = jnp.dot(hidden, down, preferred_element_type=f32).astype(bf16)

    lowered = lowered.reshape(planes, served, rho, feats)
    lowered = jnp.transpose(lowered, (2, 0, 1, 3)).reshape(rho * planes, served, feats)
    lowered = jnp.sum(swap(lowered, RHO + PLANES).astype(f32), axis=0)
    mine = lax.axis_index(RHO) * feats
    after_mixer = lax.dynamic_slice_in_dim(after_wide, mine, feats, 1)
    mixed = (after_mixer.astype(f32) + lowered).astype(bf16)
    return (mixed, new_state[:, None])


def solution(mesh):
    fine = Mesh(mesh.devices.reshape(4, 2, 2, 2, 2, 2, 2, 2), KV + TP)
    return jax.shard_map(
        layer,
        mesh=fine,
        in_specs=(
            P(TP, KV),
            P(TP),
            P(None, KV),
            P(None, KV),
            P(None, KV),
            P(None, KV),
            P(KV, None),
            P(None),
            P(KV),
            P(KV),
            P(KV, TP),
            P(TP, KV),
            P(TP, KV, None, None),
        ),
        out_specs=(P(TP, KV), P(TP, KV, None, None)),
        check_vma=False,
    )
```

profile of v0, /device:TPU:1, one launch (start us, length us, event | category | flops | bytes accessed | tf_op | source)
XLA Modules:
  0.0 154.2 jit_solution(3779278416918095696)
XLA Ops:
  0.7 1.5 broadcast_in_dim.18
  2.2 7.7 %all-to-all-start = ((bf16[16,64,128]{2,1,0:T(8,128)(2,1)}), bf16[16,64,128]{2,1,0:T(8,128)(2,1)S(1)}, u32[]{:S(2)}, u32[]{:S(2)}) async-start(bf16[16,64,128]{2,1,0:T(8,128)(2,1)} %broadcast_in_dim.18), calls=%async_computation | async-start | bytes 524288 | tf_op jit(solution)/shard_map/all_to_all | solution.py:27
  9.9 0.7 convert_bitcast_fusion.4
  10.8 0.7 convert_element_type.139
  11.4 0.1 copy.77
  11.6 0.9 copy.76
  12.5 1.0 copy.78
  13.6 4.0 %all-to-all-done = bf16[16,64,128]{2,1,0:T(8,128)(2,1)S(1)} async-done(((bf16[16,64,128]{2,1,0:T(8,128)(2,1)}), bf16[16,64,128]{2,1,0:T(8,128)(2,1)S(1)}, u32[]{:S(2)}, u32[]{:S(2)}) %all-to-all-start) | async-done | bytes 262176 | tf_op jit(solution)/shard_map/all_to_all | solution.py:27
  17.6 0.2 fusion.6
  17.8 0.8 fusion.8
  18.6 0.2 fusion.57
  18.8 1.2 fusion.58
  20.0 1.2 fusion.56
  21.2 0.2 fusion.37
  21.6 2.2 %fusion = f32[64,1,64]{2,1,0:T(1,128)S(1)} fusion(f32[64,64,1]{1,2,0:T(1,128)S(1)} %copy.86, f32[64,1,64,64]{3,2,1,0:T(8,128)S(1)} %copy-done.1, f32[64,64]{1,0:T(8,128)S(1)} %fusion.57, f32[64,64]{1,0:T(8,128)S(1)} %copy.74, f32[]{:T(128)S(6)} %sub.32), kind=kOutput, calls=%fused_computation.2 | convolution fusion | flops 3932160 | bytes 1114116 | tf_op jit(solution)/shard_map/bkv,bk->bv/dot_general | solution.py:114
  23.9 1.5 convolution_convert_fusion
  25.5 0.9 broadcast_in_dim.19
  26.3 3.6 %all-to-all-start.1 = ((bf16[16,64,256]{2,1,0:T(8,128)(2,1)}), bf16[16,64,256]{2,1,0:T(8,128)(2,1)S(1)}, u32[]{:S(2)}, u32[]{:S(2)}) async-start(bf16[16,64,256]{2,1,0:T(8,128)(2,1)} %bitcast.89), calls=%async_computation.1 | async-start | bytes 1048576 | tf_op jit(solution)/shard_map/all_to_all | solution.py:27
  29.9 0.7 fusion.53
  30.6 3.1 %collective-permute-start = (bf16[264,128]{0,1:T(8,128)(2,1)}, bf16[264,128]{0,1:T(8,128)(2,1)S(1)}, u32[]{:S(2)}, u32[]{:S(2)}) collective-permute-start(bf16[264,128]{0,1:T(8,128)(2,1)} %get-tuple-element.37), channel_id=1, source_target_pairs={{0,32},{32,0},{1,33},{33,1},{2,34},{34,2},{3,35},{35,3},{4,36},{36... | collective-permute-start | bytes 202760 | tf_op jit(solution)/shard_map/ppermute | solution.py:84
  33.7 2.9 %collective-permute-done = bf16[264,128]{0,1:T(8,128)(2,1)S(1)} collective-permute-done((bf16[264,128]{0,1:T(8,128)(2,1)}, bf16[264,128]{0,1:T(8,128)(2,1)S(1)}, u32[]{:S(2)}, u32[]{:S(2)}) %collective-permute-start) | collective-permute-done | bytes 67616 | tf_op jit(solution)/shard_map/ppermute | solution.py:84
  36.6 0.6 copy-done.7
  37.2 1.0 maximum_select_fusion
  38.3 13.6 %collective-permute-start.3 = (bf16[2,264,128]{1,2,0:T(8,128)(2,1)S(1)}, bf16[2,264,128]{1,2,0:T(8,128)(2,1)}, u32[]{:S(2)}, u32[]{:S(2)}) collective-permute-start(bf16[2,264,128]{1,2,0:T(8,128)(2,1)S(1)} %maximum_select_fusion), channel_id=1, source_target_pairs={{0,24},{8,0},{16,8},{24,16},{1,25},{9,1},{17,9},{25,17},{2,26},{10... | collective-permute-start | bytes 405512 | tf_op jit(solution)/shard_map/ppermute | solution.py:88
  52.0 0.7 broadcast_in_dim.20
  52.7 6.5 %all-to-all-start.2 = ((bf16[8,64,256]{2,1,0:T(8,128)(2,1)}), bf16[8,64,256]{2,1,0:T(8,128)(2,1)S(1)}, u32[]{:S(2)}, u32[]{:S(2)}) async-start(bf16[8,64,256]{2,1,0:T(8,128)(2,1)} %broadcast_in_dim.20), calls=%async_computation.2 | async-start | bytes 524288 | tf_op jit(solution)/shard_map/all_to_all | solution.py:27
  59.2 1.9 %collective-permute-start.2 = (bf16[2,264,128]{1,2,0:T(8,128)(2,1)S(1)}, bf16[2,264,128]{1,2,0:T(8,128)(2,1)}, u32[]{:S(2)}, u32[]{:S(2)}) collective-permute-start(bf16[2,264,128]{1,2,0:T(8,128)(2,1)S(1)} %maximum_select_fusion), channel_id=1, source_target_pairs={{0,8},{8,16},{16,24},{24,0},{1,9},{9,17},{17,25},{25,1},{2,10},{10... | collective-permute-start | bytes 405512 | tf_op jit(solution)/shard_map/ppermute | solution.py:88
  61.2 10.3 %collective-permute-start.1 = (bf16[2,264,128]{1,2,0:T(8,128)(2,1)S(1)}, bf16[2,264,128]{1,2,0:T(8,128)(2,1)S(1)}, u32[]{:S(2)}, u32[]{:S(2)}) collective-permute-start(bf16[2,264,128]{1,2,0:T(8,128)(2,1)S(1)} %maximum_select_fusion), channel_id=1, source_target_pairs={{0,16},{8,24},{16,0},{24,8},{1,17},{9,25},{17,1},{25,9},{2,18},{10... | collective-permute-start | bytes 405512 | tf_op jit(solution)/shard_map/ppermute | solution.py:88
  71.4 0.1 copy.79
  71.6 0.2 fusion.27
  71.8 0.9 fusion.52
  72.7 0.1 copy.82
  72.8 0.9 fusion.51
  73.7 0.1 copy.81
  73.8 28.5 %collective-permute-done.1 = bf16[2,264,128]{1,2,0:T(8,128)(2,1)S(1)} collective-permute-done((bf16[2,264,128]{1,2,0:T(8,128)(2,1)S(1)}, bf16[2,264,128]{1,2,0:T(8,128)(2,1)S(1)}, u32[]{:S(2)}, u32[]{:S(2)}) %collective-permute-start.1) | collective-permute-done | bytes 135200 | tf_op jit(solution)/shard_map/ppermute | solution.py:88
  102.3 0.6 fusion.50
  102.9 0.1 copy.80
  103.1 0.1 multiply_reduce_fusion
  103.2 0.2 scatter.9
  103.5 0.3 convolution_convert_fusion.1
  103.9 17.1 %all_to_all.30 = bf16[8,72,512]{2,1,0:T(8,128)(2,1)S(1)} all-to-all(bf16[8,72,512]{2,1,0:T(8,128)(2,1)S(1)} %pad_maximum_fusion), channel_id=1, replica_groups=mesh['y'=4,'xh'=2,'xl'=2,'b3'=2,'b2'=2,'b1'=2,'b0'=2,'c'=2] {'y','xh'}, dimensions={0} | all-to-all | bytes 1179648 | tf_op jit(solution)/shard_map/all_to_all | solution.py:27
  121.2 12.4 %all_to_all.31 = bf16[8,64,512]{2,1,0:T(8,128)(2,1)S(1)} all-to-all(bf16[8,64,512]{2,1,0:T(8,128)(2,1)S(1)} %broadcast_in_dim.51), channel_id=1, replica_groups=mesh['y'=4,'xh'=2,'xl'=2,'b3'=2,'b2'=2,'b1'=2,'b0'=2,'c'=2] {'y','xh'}, dimensions={0} | all-to-all | bytes 1048576 | tf_op jit(solution)/shard_map/all_to_all | solution.py:27
  133.6 0.3 convolution_convert_fusion.2
  134.0 0.8 copy.84
  134.7 9.2 %all-to-all-start.5 = ((bf16[16,64,128]{2,1,0:T(8,128)(2,1)}), bf16[16,64,128]{2,1,0:T(8,128)(2,1)S(1)}, u32[]{:S(2)}, u32[]{:S(2)}) async-start(bf16[16,64,128]{2,1,0:T(8,128)(2,1)} %bitcast.34), calls=%async_computation.5 | async-start | bytes 524288 | tf_op jit(solution)/shard_map/all_to_all | solution.py:27
  144.0 1.7 %multiply_add_fusion = f32[64,1,64,64]{3,2,1,0:T(8,128)} fusion(f32[64,1,64,64]{3,2,1,0:T(8,128)S(1)} %copy-done.1, f32[64,64]{1,0:T(8,128)S(1)} %copy-done.3, f32[64,64]{1,0:T(8,128)S(1)} %copy-done.5, f32[]{:T(128)S(6)} %sub.32), kind=kLoop, calls=%fused_computation.3 | loop fusion | flops 786432 | bytes 2129924 | tf_op jit(solution)/shard_map/add | solution.py:113
  145.7 7.8 %all-to-all-done.5 = bf16[16,64,128]{2,1,0:T(8,128)(2,1)S(1)} async-done(((bf16[16,64,128]{2,1,0:T(8,128)(2,1)}), bf16[16,64,128]{2,1,0:T(8,128)(2,1)S(1)}, u32[]{:S(2)}, u32[]{:S(2)}) %all-to-all-start.5) | async-done | bytes 262176 | tf_op jit(solution)/shard_map/all_to_all | solution.py:27
  153.6 0.6 add_convert_fusion
  (53 shorter events, 1.2 us)
Async XLA Ops:
  0.6 23.2 %copy-start = (bf16[64,2048]{1,0:T(8,128)(2,1)S(1)}, bf16[64,2048]{1,0:T(8,128)(2,1)}, u32[]{:S(2)}) copy-start(bf16[64,2048]{1,0:T(8,128)(2,1)} %param.23) | copy-start | bytes 786436
  0.6 17.9 %copy-start.6 = (bf16[2048,64]{0,1:T(8,128)(2,1)S(1)}, bf16[2048,64]{0,1:T(8,128)(2,1)}, u32[]{:S(2)}) copy-start(bf16[2048,64]{0,1:T(8,128)(2,1)} %param.21) | copy-start | bytes 786436
  2.2 19.4 %copy-start.1 = (f32[64,1,64,64]{3,2,1,0:T(8,128)S(1)}, f32[64,1,64,64]{3,2,1,0:T(8,128)}, u32[]{:S(2)}) copy-start(f32[64,1,64,64]{3,2,1,0:T(8,128)} %param.29) | copy-start | bytes 3145732
  2.2 15.4 %all-to-all-start = ((bf16[16,64,128]{2,1,0:T(8,128)(2,1)}), bf16[16,64,128]{2,1,0:T(8,128)(2,1)S(1)}, u32[]{:S(2)}, u32[]{:S(2)}) async-start(bf16[16,64,128]{2,1,0:T(8,128)(2,1)} %broadcast_in_dim.18), calls=%async_computation | async-start | bytes 524288 | tf_op jit(solution)/shard_map/all_to_all | solution.py:27
  18.6 5.3 %copy-start.9 = (f32[64]{0:T(128)S(1)}, f32[64]{0:T(128)}, u32[]{:S(2)}) copy-start(f32[64]{0:T(128)} %param.25) | copy-start | bytes 772
  18.8 5.0 %copy-start.2 = (f32[64,64]{1,0:T(8,128)}, f32[64,64]{1,0:T(8,128)S(1)}, u32[]{:S(2)}) copy-start(f32[64,64]{1,0:T(8,128)S(1)} %fusion.57) | copy-start | bytes 49156
  21.4 2.4 %copy-start.4 = (f32[64,64]{1,0:T(8,128)}, f32[64,64]{1,0:T(8,128)S(1)}, u32[]{:S(2)}) copy-start(f32[64,64]{1,0:T(8,128)S(1)} %copy.74) | copy-start | bytes 49156
  26.3 25.5 %all-to-all-start.1 = ((bf16[16,64,256]{2,1,0:T(8,128)(2,1)}), bf16[16,64,256]{2,1,0:T(8,128)(2,1)S(1)}, u32[]{:S(2)}, u32[]{:S(2)}) async-start(bf16[16,64,256]{2,1,0:T(8,128)(2,1)} %bitcast.89), calls=%async_computation.1 | async-start | bytes 1048576 | tf_op jit(solution)/shard_map/all_to_all | solution.py:27
  30.6 6.0 %collective-permute-start = (bf16[264,128]{0,1:T(8,128)(2,1)}, bf16[264,128]{0,1:T(8,128)(2,1)S(1)}, u32[]{:S(2)}, u32[]{:S(2)}) collective-permute-start(bf16[264,128]{0,1:T(8,128)(2,1)} %get-tuple-element.37), channel_id=1, source_target_pairs={{0,32},{32,0},{1,33},{33,1},{2,34},{34,2},{3,35},{35,3},{4,36},{36... | collective-permute-start | bytes 202760 | tf_op jit(solution)/shard_map/ppermute | solution.py:84
  36.6 0.6 copy-start.7
  38.3 33.5 %collective-permute-start.3 = (bf16[2,264,128]{1,2,0:T(8,128)(2,1)S(1)}, bf16[2,264,128]{1,2,0:T(8,128)(2,1)}, u32[]{:S(2)}, u32[]{:S(2)}) collective-permute-start(bf16[2,264,128]{1,2,0:T(8,128)(2,1)S(1)} %maximum_select_fusion), channel_id=1, source_target_pairs={{0,24},{8,0},{16,8},{24,16},{1,25},{9,1},{17,9},{25,17},{2,26},{10... | collective-permute-start | bytes 405512 | tf_op jit(solution)/shard_map/ppermute | solution.py:88
  52.7 50.4 %all-to-all-start.2 = ((bf16[8,64,256]{2,1,0:T(8,128)(2,1)}), bf16[8,64,256]{2,1,0:T(8,128)(2,1)S(1)}, u32[]{:S(2)}, u32[]{:S(2)}) async-start(bf16[8,64,256]{2,1,0:T(8,128)(2,1)} %broadcast_in_dim.20), calls=%async_computation.2 | async-start | bytes 524288 | tf_op jit(solution)/shard_map/all_to_all | solution.py:27
  59.2 13.6 %collective-permute-start.2 = (bf16[2,264,128]{1,2,0:T(8,128)(2,1)S(1)}, bf16[2,264,128]{1,2,0:T(8,128)(2,1)}, u32[]{:S(2)}, u32[]{:S(2)}) collective-permute-start(bf16[2,264,128]{1,2,0:T(8,128)(2,1)S(1)} %maximum_select_fusion), channel_id=1, source_target_pairs={{0,8},{8,16},{16,24},{24,0},{1,9},{9,17},{17,25},{25,1},{2,10},{10... | collective-permute-start | bytes 405512 | tf_op jit(solution)/shard_map/ppermute | solution.py:88
  61.2 41.1 %collective-permute-start.1 = (bf16[2,264,128]{1,2,0:T(8,128)(2,1)S(1)}, bf16[2,264,128]{1,2,0:T(8,128)(2,1)S(1)}, u32[]{:S(2)}, u32[]{:S(2)}) collective-permute-start(bf16[2,264,128]{1,2,0:T(8,128)(2,1)S(1)} %maximum_select_fusion), channel_id=1, source_target_pairs={{0,16},{8,24},{16,0},{24,8},{1,17},{9,25},{17,1},{25,9},{2,18},{10... | collective-permute-start | bytes 405512 | tf_op jit(solution)/shard_map/ppermute | solution.py:88
  103.9 29.7 %copy-start.8 = (bf16[2,128,128]{1,2,0:T(8,128)(2,1)S(1)}, bf16[2,128,128]{1,2,0:T(8,128)(2,1)}, u32[]{:S(2)}) copy-start(bf16[2,128,128]{1,2,0:T(8,128)(2,1)} %get-tuple-element.30) | copy-start | bytes 196612
  121.2 22.8 %copy-start.3 = (f32[64,64]{1,0:T(8,128)S(1)}, f32[64,64]{1,0:T(8,128)}, u32[]{:S(2)}) copy-start(f32[64,64]{1,0:T(8,128)} %copy-done.2) | copy-start | bytes 49156
  121.2 22.8 %copy-start.5 = (f32[64,64]{1,0:T(8,128)S(1)}, f32[64,64]{1,0:T(8,128)}, u32[]{:S(2)}) copy-start(f32[64,64]{1,0:T(8,128)} %copy-done.4) | copy-start | bytes 49156
  134.7 18.8 %all-to-all-start.5 = ((bf16[16,64,128]{2,1,0:T(8,128)(2,1)}), bf16[16,64,128]{2,1,0:T(8,128)(2,1)S(1)}, u32[]{:S(2)}, u32[]{:S(2)}) async-start(bf16[16,64,128]{2,1,0:T(8,128)(2,1)} %bitcast.34), calls=%async_computation.5 | async-start | bytes 524288 | tf_op jit(solution)/shard_map/all_to_all | solution.py:27
where the time goes:
time: 155 us; the launch traced here: 154 us
  starting transfers between devices  55.9 us (36%)
  waiting for transfers between devices  43.1 us (28%)
  blocking collectives  29.5 us (19%)
  local copies, waits for them, and re-layouts  10.8 us (7%)
  other arithmetic  6.9 us (4%)
  matrix products  6.81 us (4%)
    all_to_all x2, blocking collectives, swap(): return lax.all_to_all(blocks, axes, split_axis=0, concat_axis=0, tiled=True)  29.5 us
    ppermute x3, waiting for transfers between devices, layer(): lax.ppermute(pair, FAR, [(i, (i + step) % far) for i in range(far)])  28.5 us
    all_to_all x4, starting transfers between devices, swap(): return lax.all_to_all(blocks, axes, split_axis=0, concat_axis=0, tiled=True)  27 us
    ppermute x3, starting transfers between devices, layer(): lax.ppermute(pair, FAR, [(i, (i + step) % far) for i in range(far)])  25.7 us
    all_to_all x4, waiting for transfers between devices, swap(): return lax.all_to_all(blocks, axes, split_axis=0, concat_axis=0, tiled=True)  11.8 us
    ppermute x1, starting transfers between devices, layer(): got = lax.ppermute(both[1 - side], RHO, [(0, 1), (1, 0)])  3.13 us
  transfers between devices with their start and end apart: 8, of which 4 were waited for; matrix products, arithmetic and copies ran while one was open for 7% of the time, Pallas kernels for 0%

commit v1 on v0

v1 whole, which is shorter than its diff:
```python
import jax
import jax.numpy as jnp
import numpy as np
from jax import lax
from jax.experimental import pallas as pl
from jax.experimental.pallas import tpu as pltpu
from jax.sharding import Mesh
from jax.sharding import PartitionSpec as P

D = 2048
HEADS = 16
HEAD_DIM = 64
EPS = 1e-06
THETA = 10000.0

KV = ("y", "xh", "xl")
TP = ("b3", "b2", "b1", "b0", "c")
KAPPA = ("y", "xh")
RHO = ("xl",)
PLANES = ("b1", "b0", "c")
FAR = ("b3", "b2")


def size_of(axes):
    return int(np.prod([lax.axis_size(a) for a in axes]))


def swap(blocks, axes):
    return lax.all_to_all(blocks, axes, split_axis=0, concat_axis=0, tiled=True)


def to_all(value, axes):
    return swap(jnp.broadcast_to(value, (size_of(axes), *value.shape)), axes)


def rotate(vectors, position):
    breadth = vectors.shape[-1]
    middle = breadth // 2
    inverse = THETA ** (-jnp.arange(middle, dtype=jnp.float32) * 2.0 / breadth)
    angles = position.astype(jnp.float32)[:, None] * inverse[None, :]
    cosine = jnp.cos(angles)
    sine = jnp.sin(angles)
    former = vectors[..., :middle]
    latter = vectors[..., middle:]
    return jnp.concatenate(
        [former * cosine - latter * sine, former * sine + latter * cosine], axis=-1
    )


def call(kernel, out, *operands, scalars=(), flops=1 << 20):
    moved = sum(o.size * o.dtype.itemsize for o in operands)
    moved += int(np.prod(out.shape)) * out.dtype.itemsize
    smem = pl.BlockSpec(memory_space=pltpu.SMEM)
    vmem = pl.BlockSpec(memory_space=pltpu.VMEM)
    return pl.pallas_call(
        kernel,
        out_shape=out,
        in_specs=[smem] * len(scalars) + [vmem] * len(operands),
        out_specs=vmem,
        compiler_params=pltpu.CompilerParams(vmem_limit_bytes=24 << 20),
        cost_estimate=pl.CostEstimate(flops=flops, bytes_accessed=moved, transcendentals=0),
    )(*(jnp.reshape(v, (1,)).astype(jnp.int32) for v in scalars), *operands)


def pack_kernel(up_ref, down_ref, gain_ref, out_ref):
    bf16, f32 = jnp.bfloat16, jnp.float32
    feats, units = up_ref.shape[0], up_ref.shape[1] // out_ref.shape[0]
    gain = gain_ref[...]
    first = gain.astype(bf16).astype(f32)
    second = (gain - first).astype(bf16).astype(f32)
    third = gain - first - second
    row = lax.broadcasted_iota(jnp.int32, (8, feats), 0)
    zero = jnp.zeros((8, feats), f32)
    rows = jnp.where(row == 0, first, jnp.where(row == 1, second, jnp.where(row == 2, third, zero)))
    for r in range(out_ref.shape[0]):
        out_ref[r, :feats] = up_ref[:, r * units : (r + 1) * units]
        out_ref[r, feats : feats + units] = down_ref[r * units : (r + 1) * units]
        out_ref[r, feats + units :] = rows.astype(bf16)


def pick_kernel(side_ref, *refs):
    *blocks, out_ref = refs
    for d, block in enumerate(blocks):
        out_ref[d] = block[1 - side_ref[0]]


def after_kernel(at_ref, parts_ref, tokens_ref, out_ref):
    f32 = jnp.float32
    feats = tokens_ref.shape[2]
    total = parts_ref[0].astype(f32)
    for k in range(1, parts_ref.shape[0]):
        total = total + parts_ref[k].astype(f32)
    rho = out_ref.shape[2] // feats
    for r in range(rho):
        own = tokens_ref[at_ref[0] + r].astype(f32)
        block = (own + total[:, r * feats : (r + 1) * feats]).astype(jnp.bfloat16)
        for p in range(out_ref.shape[0]):
            out_ref[p, :, r * feats : (r + 1) * feats] = block


def up_kernel(side_ref, rows_ref, got_ref, *refs):
    bf16, f32 = jnp.bfloat16, jnp.float32
    *blocks, out_ref = refs
    planes, served, wide = rows_ref.shape
    kappa, _, _ = out_ref.shape
    feats = wide // 2
    count = planes * served
    side = side_ref[0]
    rows = rows_ref[...].reshape(count, wide)
    x = rows.astype(f32)
    kept = jnp.where(side == 0, x[:, :feats], x[:, feats:])
    other = jnp.where(side == 0, x[:, feats:], x[:, :feats])
    bottom = blocks[0].shape[1] - 8

    def gain_of(pieces):
        p = pieces.astype(f32)
        return p[0:1] + p[1:2] + p[2:3]

    mine = blocks[0][side]
    kept = (kept * gain_of(mine[bottom:])).astype(bf16)
    other = (other * gain_of(got_ref[0, bottom:])).astype(bf16)
    for d, block in enumerate(blocks):
        part = jnp.dot(kept, block[side, :feats], preferred_element_type=f32)
        part = part + jnp.dot(other, got_ref[d, :feats], preferred_element_type=f32)
        units = part.shape[1]
        part = part.astype(bf16).reshape(kappa, count // kappa, units)
        out_ref[:, : count // kappa, d * units : (d + 1) * units] = part
    square = x * x
    high = square.astype(bf16)
    low = (square - high.astype(f32)).astype(bf16)
    ones = jnp.ones((8, wide), bf16)
    along = (((1,), (1,)), ((), ()))
    total = lax.dot_general(ones, high, along, preferred_element_type=f32)
    total = total + lax.dot_general(ones, low, along, preferred_element_type=f32)
    high = total.astype(bf16).astype(f32)
    low = total - high
    row = lax.broadcasted_iota(jnp.int32, total.shape, 0)
    extra = jnp.where(row == 0, high, jnp.where(row == 1, low, jnp.zeros_like(total))).astype(bf16)
    for k in range(kappa):
        out_ref[k, count // kappa :] = extra


def hidden_kernel(at_ref, parts_ref, out_ref):
    f32 = jnp.float32
    count = out_ref.shape[1]
    total = parts_ref[0].astype(f32)
    for k in range(1, parts_ref.shape[0]):
        total = total + parts_ref[k].astype(f32)
    squares = total[count : count + 1] + total[count + 1 : count + 2]
    shape = (count, total.shape[1])
    row = lax.broadcasted_iota(jnp.int32, shape, 0)
    lane = lax.broadcasted_iota(jnp.int32, shape, 1)
    mine = jnp.where(lane == row + at_ref[0] * count, squares, jnp.zeros(shape, f32))
    factor = lax.rsqrt(jnp.sum(mine, axis=1, keepdims=True) / D + EPS)
    raised = jnp.maximum(total[:count] * factor, 0.0)
    hidden = (raised * raised).astype(jnp.bfloat16)
    for k in range(out_ref.shape[0]):
        out_ref[k] = hidden


def down_kernel(side_ref, hidden_ref, got_ref, *refs):
    *blocks, out_ref = refs
    kappa, rows, units = hidden_ref.shape
    _, planes, served, feats = out_ref.shape
    start = feats
    stop = blocks[0].shape[1] - 8
    side = side_ref[0]
    hidden = hidden_ref[...].reshape(kappa * rows, units)
    kept = jnp.concatenate([b[side, start:stop] for b in blocks])
    other = jnp.concatenate([got_ref[d, start:stop] for d in range(len(blocks))])
    for at, weight in ((side, kept), (1 - side, other)):
        part = jnp.dot(hidden, weight, preferred_element_type=jnp.float32)
        out_ref[at] = part.astype(jnp.bfloat16).reshape(planes, served, feats)


def final_kernel(side_ref, parts_ref, after_ref, out_ref):
    f32 = jnp.float32
    feats = out_ref.shape[1]
    total = parts_ref[0].astype(f32)
    for k in range(1, parts_ref.shape[0]):
        total = total + parts_ref[k].astype(f32)
    after = after_ref[0].astype(f32)
    after = jnp.where(side_ref[0] == 0, after[:, :feats], after[:, feats:])
    out_ref[...] = (after + total).astype(out_ref.dtype)


def layer(
    tokens,
    lengths,
    query_weight,
    key_weight,
    value_weight,
    gate_weight,
    output_weight,
    mixer_gain,
    group_gain,
    channel_gain,
    up_weight,
    down_weight,
    memory_state,
):
    bf16, f32 = jnp.bfloat16, jnp.float32
    served, feats = tokens.shape
    kv, kappa, rho = size_of(KV), size_of(KAPPA), size_of(RHO)
    planes, far = size_of(PLANES), size_of(FAR)
    wide = feats * rho
    units = up_weight.shape[1] // rho

    like = jax.ShapeDtypeStruct
    both = call(
        pack_kernel,
        like((rho, feats + units + 8, feats), bf16),
        up_weight,
        down_weight,
        channel_gain.reshape(1, feats),
    )
    blocks_far = [both]
    for step in (2, 1, 3):
        ring = [(i, (i + step) % far) for i in range(far)]
        blocks_far.append(lax.ppermute(both, FAR, ring))
    side = lax.axis_index(RHO)
    given = call(
        pick_kernel, like((far, *both.shape[1:]), bf16), *blocks_far, scalars=(side,)
    )
    got = lax.ppermute(given, RHO, [(0, 1), (1, 0)])

    blocks = to_all(tokens, KV)
    whole_rows = jnp.moveaxis(blocks, 0, 1).reshape(served, kv * feats)
    widened = whole_rows.astype(f32)
    normed = (
        widened * lax.rsqrt(jnp.mean(widened * widened, axis=1, keepdims=True) + EPS) * mixer_gain
    ).astype(bf16)

    def project(weight):
        return jnp.dot(normed, weight, preferred_element_type=f32)

    queries = rotate(project(query_weight), lengths)
    keys_new = rotate(project(key_weight), lengths) * HEAD_DIM ** (-0.5)
    values_new = project(value_weight)
    gating = project(gate_weight)
    head = lax.axis_index(KV).astype(f32)
    decay = 1.0 - 2.0 ** (-5.0 - 5.0 * head / (HEADS - 1))
    new_state = decay * memory_state[:, 0] + keys_new[:, :, None] * values_new[:, None, :]
    readout = jnp.einsum("bkv,bk->bv", new_state, queries, precision=lax.Precision.HIGHEST)
    grouped = readout * lax.rsqrt(jnp.mean(readout * readout, axis=-1, keepdims=True) + EPS)
    merged = (grouped * group_gain * jax.nn.silu(gating)).astype(bf16)
    shares = jnp.dot(merged, output_weight, preferred_element_type=f32).astype(bf16)

    shares = jnp.moveaxis(shares.reshape(served, kappa, wide), 1, 0)
    shares = jnp.broadcast_to(shares[:, None], (kappa, rho, served, wide)).reshape(kv, served, wide)
    shares = swap(shares, KV)
    at = lax.axis_index(KAPPA) * rho
    after_wide = call(
        after_kernel, like((planes, served, wide), bf16), shares, blocks, scalars=(at,)
    )

    rows = swap(after_wide, PLANES)
    part = planes * served // kappa
    sent = call(
        up_kernel,
        like((kappa, part + 8, far * units), bf16),
        rows,
        got,
        *blocks_far,
        scalars=(side,),
        flops=2 * planes * served * wide * far * units,
    )
    hidden = call(
        hidden_kernel,
        like((kappa, part, far * units), bf16),
        swap(sent, KAPPA),
        scalars=(lax.axis_index(KAPPA),),
    )
    lowered = call(
        down_kernel,
        like((rho, planes, served, feats), bf16),
        swap(hidden, KAPPA),
        got,
        *blocks_far,
        scalars=(side,),
        flops=2 * planes * served * wide * far * units,
    )

    lowered = swap(lowered.reshape(rho * planes, served, feats), RHO + PLANES)
    mixed = call(final_kernel, like((served, feats), bf16), lowered, after_wide, scalars=(side,))
    return (mixed, new_state[:, None])


def solution(mesh):
    fine = Mesh(mesh.devices.reshape(4, 2, 2, 2, 2, 2, 2, 2), KV + TP)
    return jax.shard_map(
        layer,
        mesh=fine,
        in_specs=(
            P(TP, KV),
            P(TP),
            P(None, KV),
            P(None, KV),
            P(None, KV),
            P(None, KV),
            P(KV, None),
            P(None),
            P(KV),
            P(KV),
            P(KV, TP),
            P(TP, KV),
            P(TP, KV, None, None),
        ),
        out_specs=(P(TP, KV), P(TP, KV, None, None)),
        check_vma=False,
    )
```

time: 155 us -> 148 us (0.955)
  waiting for transfers between devices: 43.1 us -> 53.8 us
  local copies, waits for them, and re-layouts: 10.8 us -> 2.78 us
  blocking collectives: 29.5 us -> 24.8 us
  starting transfers between devices: 55.9 us -> 51.5 us
  Pallas kernels: 0 us -> 4.26 us
  other arithmetic: 6.9 us -> 3.63 us
    all_to_all x4, waiting for transfers between devices: 11.8 us -> 24.1 us  [swap(): return lax.all_to_all(blocks, axes, split_axis=0, concat_axis=0, tiled=True)]
    all_to_all x2, blocking collectives: 29.5 us -> 24.8 us  [swap(): return lax.all_to_all(blocks, axes, split_axis=0, concat_axis=0, tiled=True)]
    ppermute x4, starting transfers between devices: 28.9 us -> 24.2 us  [the longest x3 22.1 us: layer(): blocks_far.append(lax.ppermute(both, FAR, ring))]
    pallas_call x0 -> x7, Pallas kernels: none -> 4.26 us  [call(): pl.pallas_call(kernel, out_shape=out, in_specs=[smem] * len(scalars) + [v...]
    slice x9 -> x0, local copies, waits for them, and re-layouts: 3.58 us -> none  [the longest x4 2.43 us: layer(): p[:, half:2 * half]]
    reshape x3 -> x0, local copies, waits for them, and re-layouts: 1.77 us -> none  [the longest x1 0.96 us: layer(): down_cut = down_weight.reshape(rho, units, feats)]
    ppermute x4, waiting for transfers between devices: 31.3 us -> 29.7 us  [the longest x3 22.7 us: layer(): blocks_far.append(lax.ppermute(both, FAR, ring))]
    unnamed x22 -> x19, local copies, waits for them, and re-layouts: 1.68 us -> 0.11 us
  transfers between devices with their start and end apart: 8 -> 8, of which waited for: 4 -> 5; matrix products, arithmetic and copies ran while one was open for 7% -> 2% of each run, Pallas kernels for 0% -> 0%
where the time goes in v1:
time: 148 us; the launch traced here: 147 us
  waiting for transfers between devices  53.8 us (36%)
  starting transfers between devices  51.5 us (35%)
  blocking collectives  24.8 us (17%)
  matrix products  5.27 us (4%)
  Pallas kernels  4.26 us (3%)
  other arithmetic  3.63 us (2%)
  local copies, waits for them, and re-layouts  2.78 us (2%)
    all_to_all x4, starting transfers between devices, swap(): return lax.all_to_all(blocks, axes, split_axis=0, concat_axis=0, tiled=True)  27.2 us
    all_to_all x2, blocking collectives, swap(): return lax.all_to_all(blocks, axes, split_axis=0, concat_axis=0, tiled=True)  24.8 us
    all_to_all x4, waiting for transfers between devices, swap(): return lax.all_to_all(blocks, axes, split_axis=0, concat_axis=0, tiled=True)  24.1 us
    ppermute x3, waiting for transfers between devices, layer(): blocks_far.append(lax.ppermute(both, FAR, ring))  22.7 us
    ppermute x3, starting transfers between devices, layer(): blocks_far.append(lax.ppermute(both, FAR, ring))  22.1 us
    ppermute x1, waiting for transfers between devices, layer(): got = lax.ppermute(given, RHO, [(0, 1), (1, 0)])  7.02 us
    pallas_call x7, Pallas kernels, call(): pl.pallas_call(kernel, out_shape=out, in_specs=[smem] * len(scalars) + [v...  4.26 us
  transfers between devices with their start and end apart: 8, of which 5 were waited for; matrix products, arithmetic and copies ran while one was open for 2% of the time, Pallas kernels for 0%

profile of v1, /device:TPU:1, one launch (start us, length us, event | category | flops | bytes accessed | tf_op | source)
XLA Modules:
  0.0 147.1 jit_solution(7279352497478841703)
XLA Ops:
  0.6 0.0 copy-start
  0.7 0.0 copy-start.4
  0.7 1.6 %broadcast_in_dim.4 = bf16[16,64,128]{2,1,0:T(8,128)(2,1)} broadcast(bf16[64,128]{1,0:T(8,128)(2,1)} %param.13), dimensions={1,2} | broadcast | bytes 278528 | tf_op jit(solution)/shard_map/broadcast_in_dim | solution.py:33
  2.3 7.6 %all-to-all-start = ((bf16[16,64,128]{2,1,0:T(8,128)(2,1)}), bf16[16,64,128]{2,1,0:T(8,128)(2,1)S(1)}, u32[]{:S(2)}, u32[]{:S(2)}) async-start(bf16[16,64,128]{2,1,0:T(8,128)(2,1)} %broadcast_in_dim.4), calls=%async_computation | async-start | bytes 524288 | tf_op jit(solution)/shard_map/all_to_all | solution.py:29
  9.9 0.7 convert_element_type.35
  10.6 7.0 %all-to-all-done.tokens_ref = bf16[16,64,128]{2,1,0:T(8,128)(2,1)S(1)} async-done(((bf16[16,64,128]{2,1,0:T(8,128)(2,1)}), bf16[16,64,128]{2,1,0:T(8,128)(2,1)S(1)}, u32[]{:S(2)}, u32[]{:S(2)}) %all-to-all-start) | async-done | bytes 262176 | tf_op jit(solution)/shard_map/all_to_all | solution.py:29
  17.6 0.2 fusion.6
  17.7 0.8 fusion.8
  18.6 0.0 copy-start.6
  18.6 0.0 copy-start.8
  18.6 1.2 fusion.28
  19.8 0.0 copy-done.7
  19.8 0.2 fusion.29
  20.0 1.2 fusion.27
  21.2 0.2 fusion.17
  21.4 0.1 copy.19
  21.5 0.1 copy.22
  21.5 0.0 copy-done.4
  21.6 2.2 %fusion = f32[64,1,64]{2,1,0:T(1,128)S(1)} fusion(f32[64,64,1]{1,2,0:T(1,128)S(1)} %copy.22, f32[64,1,64,64]{3,2,1,0:T(8,128)S(1)} %copy-done.4, f32[64,64]{1,0:T(8,128)S(1)} %fusion.28, f32[64,64]{1,0:T(8,128)S(1)} %copy.19, f32[]{:T(128)S(6)} %sub.13), kind=kOutput, calls=%fused_computation.2 | convolution fusion | flops 3932160 | bytes 1114116 | tf_op jit(solution)/shard_map/bkv,bk->bv/dot_general | solution.py:244
  23.7 0.1 multiply_reduce_fusion
  23.9 0.5 convolution_convert_fusion
  24.4 0.1 copy.25
  24.5 0.0 copy-start.1
  24.5 0.0 copy-start.2
  24.5 0.0 copy-start.3
  24.6 0.9 broadcast_in_dim.5
  25.4 3.6 %all-to-all-start.1 = ((bf16[16,64,256]{2,1,0:T(8,128)(2,1)}), bf16[16,64,256]{2,1,0:T(8,128)(2,1)S(1)}, u32[]{:S(2)}, u32[]{:S(2)}) async-start(bf16[16,64,256]{2,1,0:T(8,128)(2,1)} %bitcast.9), calls=%async_computation.1 | async-start | bytes 1048576 | tf_op jit(solution)/shard_map/all_to_all | solution.py:29
  29.0 9.2 %all-to-all-done.1.parts_ref = bf16[16,64,256]{2,1,0:T(8,128)(2,1)S(1)} async-done(((bf16[16,64,256]{2,1,0:T(8,128)(2,1)}), bf16[16,64,256]{2,1,0:T(8,128)(2,1)S(1)}, u32[]{:S(2)}, u32[]{:S(2)}) %all-to-all-start.1) | async-done | bytes 524320 | tf_op jit(solution)/shard_map/all_to_all | solution.py:29
  38.2 0.8 shard_map.140.after_ref
  39.0 9.0 %all-to-all-start.2 = ((bf16[8,64,256]{2,1,0:T(8,128)(2,1)}), bf16[8,64,256]{2,1,0:T(8,128)(2,1)S(1)}, u32[]{:S(2)}, u32[]{:S(2)}) async-start(bf16[8,64,256]{2,1,0:T(8,128)(2,1)} %shard_map.140.after_ref), calls=%async_computation.2 | async-start | bytes 524288 | tf_op jit(solution)/shard_map/all_to_all | solution.py:29
  48.1 9.9 %collective-permute-start.2 = (bf16[2,264,128]{2,1,0:T(8,128)(2,1)S(1)}, bf16[2,264,128]{2,1,0:T(8,128)(2,1)S(1)}, u32[]{:S(2)}, u32[]{:S(2)}) collective-permute-start(bf16[2,264,128]{2,1,0:T(8,128)(2,1)S(1)} %shard_map.141.refs_0_), channel_id=1, source_target_pairs={{0,24},{8,0},{16,8},{24,16},{1,25},{9,1},{17,9},{25,17},{2,26},{10... | collective-permute-start | bytes 405512 | tf_op jit(solution)/shard_map/ppermute | solution.py:220
  58.0 1.9 %collective-permute-start.1 = (bf16[2,264,128]{2,1,0:T(8,128)(2,1)S(1)}, bf16[2,264,128]{2,1,0:T(8,128)(2,1)S(1)}, u32[]{:S(2)}, u32[]{:S(2)}) collective-permute-start(bf16[2,264,128]{2,1,0:T(8,128)(2,1)S(1)} %shard_map.141.refs_0_), channel_id=1, source_target_pairs={{0,8},{8,16},{16,24},{24,0},{1,9},{9,17},{17,25},{25,1},{2,10},{10... | collective-permute-start | bytes 405512 | tf_op jit(solution)/shard_map/ppermute | solution.py:220
  59.9 10.3 %collective-permute-start = (bf16[2,264,128]{2,1,0:T(8,128)(2,1)S(1)}, bf16[2,264,128]{2,1,0:T(8,128)(2,1)S(1)}, u32[]{:S(2)}, u32[]{:S(2)}) collective-permute-start(bf16[2,264,128]{2,1,0:T(8,128)(2,1)S(1)} %shard_map.141.refs_0_), channel_id=1, source_target_pairs={{0,16},{8,24},{16,0},{24,8},{1,17},{9,25},{17,1},{25,9},{2,18},{10... | collective-permute-start | bytes 405512 | tf_op jit(solution)/shard_map/ppermute | solution.py:220
  70.1 0.0 collective-permute-done.2.refs_3_
  70.2 0.0 collective-permute-done.1.refs_2_
  70.2 22.7 %collective-permute-done.refs_1_ = bf16[2,264,128]{2,1,0:T(8,128)(2,1)S(1)} collective-permute-done((bf16[2,264,128]{2,1,0:T(8,128)(2,1)S(1)}, bf16[2,264,128]{2,1,0:T(8,128)(2,1)S(1)}, u32[]{:S(2)}, u32[]{:S(2)}) %collective-permute-start) | collective-permute-done | bytes 135200 | tf_op jit(solution)/shard_map/ppermute | solution.py:220
  92.9 2.2 %collective-permute-start.3 = (bf16[4,264,128]{2,1,0:T(8,128)(2,1)S(1)}, bf16[4,264,128]{2,1,0:T(8,128)(2,1)S(1)}, u32[]{:S(2)}, u32[]{:S(2)}) collective-permute-start(bf16[4,264,128]{2,1,0:T(8,128)(2,1)S(1)} %shard_map.142), channel_id=1, source_target_pairs={{0,32},{32,0},{1,33},{33,1},{2,34},{34,2},{3,35},{35,3},{4,36},{36... | collective-permute-start | bytes 811016 | tf_op jit(solution)/shard_map/ppermute | solution.py:225
  95.1 7.0 %collective-permute-done.3.got_ref = bf16[4,264,128]{2,1,0:T(8,128)(2,1)S(1)} collective-permute-done((bf16[4,264,128]{2,1,0:T(8,128)(2,1)S(1)}, bf16[4,264,128]{2,1,0:T(8,128)(2,1)S(1)}, u32[]{:S(2)}, u32[]{:S(2)}) %collective-permute-start.3) | collective-permute-done | bytes 270368 | tf_op jit(solution)/shard_map/ppermute | solution.py:225
  102.1 0.0 all-to-all-done.2.rows_ref
  102.1 0.5 shard_map.143
  102.6 13.0 %all_to_all.30.parts_ref = bf16[8,72,512]{2,1,0:T(8,128)(2,1)S(1)} all-to-all(bf16[8,72,512]{2,1,0:T(8,128)(2,1)S(1)} %shard_map.143), channel_id=1, replica_groups=mesh['y'=4,'xh'=2,'xl'=2,'b3'=2,'b2'=2,'b1'=2,'b0'=2,'c'=2] {'y','xh'}, dimensions={0} | all-to-all | bytes 1179648 | tf_op jit(solution)/shard_map/all_to_all | solution.py:29
  115.7 0.2 shard_map.144
  115.8 11.8 %all_to_all.31.hidden_ref = bf16[8,64,512]{2,1,0:T(8,128)(2,1)S(1)} all-to-all(bf16[8,64,512]{2,1,0:T(8,128)(2,1)S(1)} %shard_map.144), channel_id=1, replica_groups=mesh['y'=4,'xh'=2,'xl'=2,'b3'=2,'b2'=2,'b1'=2,'b0'=2,'c'=2] {'y','xh'}, dimensions={0} | all-to-all | bytes 1048576 | tf_op jit(solution)/shard_map/all_to_all | solution.py:29
  127.7 1.2 shard_map.145
  128.8 7.1 %all-to-all-start.5 = ((bf16[16,64,128]{2,1,0:T(8,128)(2,1)}), bf16[16,64,128]{2,1,0:T(8,128)(2,1)S(1)}, u32[]{:S(2)}, u32[]{:S(2)}) async-start(bf16[16,64,128]{2,1,0:T(8,128)(2,1)} %bitcast.11), calls=%async_computation.5 | async-start | bytes 524288 | tf_op jit(solution)/shard_map/all_to_all | solution.py:29
  135.9 1.7 %multiply_add_fusion = f32[64,1,64,64]{3,2,1,0:T(8,128)} fusion(f32[64,1,64,64]{3,2,1,0:T(8,128)S(1)} %copy-done.5, f32[64,64]{1,0:T(8,128)S(1)} %fusion.28, f32[64,64]{1,0:T(8,128)S(1)} %copy.19, f32[]{:T(128)S(6)} %sub.13), kind=kLoop, calls=%fused_computation.3 | loop fusion | flops 786432 | bytes 2129924 | tf_op jit(solution)/shard_map/add | solution.py:243
  137.6 7.9 %all-to-all-done.5.parts_ref = bf16[16,64,128]{2,1,0:T(8,128)(2,1)S(1)} async-done(((bf16[16,64,128]{2,1,0:T(8,128)(2,1)}), bf16[16,64,128]{2,1,0:T(8,128)(2,1)S(1)}, u32[]{:S(2)}, u32[]{:S(2)}) %all-to-all-start.5) | async-done | bytes 262176 | tf_op jit(solution)/shard_map/all_to_all | solution.py:29
  145.5 1.6 %shard_map.146 = bf16[64,128]{1,0:T(8,128)(2,1)} custom-call(s32[1]{0:T(128)} %bitcast.side_ref, bf16[16,64,128]{2,1,0:T(8,128)(2,1)S(1)} %all-to-all-done.5.parts_ref, bf16[8,64,256]{2,1,0:T(8,128)(2,1)} %shard_map.140.after_ref), custom_call_target="tpu_custom_call" | custom-call | flops 1048576 | bytes 540672 | tf_op jit(solution)/shard_map/pallas_call | solution.py:55
  (17 shorter events, 0.1 us)
Async XLA Ops:
  0.6 23.2 %copy-start = (bf16[64,2048]{1,0:T(8,128)(2,1)S(1)}, bf16[64,2048]{1,0:T(8,128)(2,1)}, u32[]{:S(2)}) copy-start(bf16[64,2048]{1,0:T(8,128)(2,1)} %param.19) | copy-start | bytes 786436
  0.6 19.2 %copy-start.7 = (bf16[2048,64]{0,1:T(8,128)(2,1)S(1)}, bf16[2048,64]{0,1:T(8,128)(2,1)}, u32[]{:S(2)}) copy-start(bf16[2048,64]{0,1:T(8,128)(2,1)} %param.15) | copy-start | bytes 786436
  0.7 20.9 %copy-start.4 = (f32[64,1,64,64]{3,2,1,0:T(8,128)S(1)}, f32[64,1,64,64]{3,2,1,0:T(8,128)}, u32[]{:S(2)}) copy-start(f32[64,1,64,64]{3,2,1,0:T(8,128)} %param.25) | copy-start | bytes 3145732
  2.3 15.3 %all-to-all-start = ((bf16[16,64,128]{2,1,0:T(8,128)(2,1)}), bf16[16,64,128]{2,1,0:T(8,128)(2,1)S(1)}, u32[]{:S(2)}, u32[]{:S(2)}) async-start(bf16[16,64,128]{2,1,0:T(8,128)(2,1)} %broadcast_in_dim.4), calls=%async_computation | async-start | bytes 524288 | tf_op jit(solution)/shard_map/all_to_all | solution.py:29
  18.6 5.3 %copy-start.6 = (bf16[2048,64]{0,1:T(8,128)(2,1)S(1)}, bf16[2048,64]{0,1:T(8,128)(2,1)}, u32[]{:S(2)}) copy-start(bf16[2048,64]{0,1:T(8,128)(2,1)} %param.18) | copy-start | bytes 786436
  18.6 5.3 %copy-start.8 = (f32[64]{0:T(128)S(1)}, f32[64]{0:T(128)}, u32[]{:S(2)}) copy-start(f32[64]{0:T(128)} %param.21) | copy-start | bytes 772
  24.5 23.6 %copy-start.1 = (bf16[128,256]{1,0:T(8,128)(2,1)S(1)}, bf16[128,256]{1,0:T(8,128)(2,1)}, u32[]{:S(2)}) copy-start(bf16[128,256]{1,0:T(8,128)(2,1)} %up_ref.1) | copy-start | bytes 196612
  24.5 23.6 %copy-start.2 = (bf16[256,128]{1,0:T(8,128)(2,1)S(1)}, bf16[256,128]{1,0:T(8,128)(2,1)}, u32[]{:S(2)}) copy-start(bf16[256,128]{1,0:T(8,128)(2,1)} %down_ref.1) | copy-start | bytes 196612
  24.5 23.5 %copy-start.3 = (f32[128]{0:T(128)S(1)}, f32[128]{0:T(128)}, u32[]{:S(2)}) copy-start(f32[128]{0:T(128)} %param.22) | copy-start | bytes 1540
  25.4 12.8 %all-to-all-start.1 = ((bf16[16,64,256]{2,1,0:T(8,128)(2,1)}), bf16[16,64,256]{2,1,0:T(8,128)(2,1)S(1)}, u32[]{:S(2)}, u32[]{:S(2)}) async-start(bf16[16,64,256]{2,1,0:T(8,128)(2,1)} %bitcast.9), calls=%async_computation.1 | async-start | bytes 1048576 | tf_op jit(solution)/shard_map/all_to_all | solution.py:29
  39.0 63.1 %all-to-all-start.2 = ((bf16[8,64,256]{2,1,0:T(8,128)(2,1)}), bf16[8,64,256]{2,1,0:T(8,128)(2,1)S(1)}, u32[]{:S(2)}, u32[]{:S(2)}) async-start(bf16[8,64,256]{2,1,0:T(8,128)(2,1)} %shard_map.140.after_ref), calls=%async_computation.2 | async-start | bytes 524288 | tf_op jit(solution)/shard_map/all_to_all | solution.py:29
  48.1 22.1 %collective-permute-start.2 = (bf16[2,264,128]{2,1,0:T(8,128)(2,1)S(1)}, bf16[2,264,128]{2,1,0:T(8,128)(2,1)S(1)}, u32[]{:S(2)}, u32[]{:S(2)}) collective-permute-start(bf16[2,264,128]{2,1,0:T(8,128)(2,1)S(1)} %shard_map.141.refs_0_), channel_id=1, source_target_pairs={{0,24},{8,0},{16,8},{24,16},{1,25},{9,1},{17,9},{25,17},{2,26},{10... | collective-permute-start | bytes 405512 | tf_op jit(solution)/shard_map/ppermute | solution.py:220
  58.0 12.2 %collective-permute-start.1 = (bf16[2,264,128]{2,1,0:T(8,128)(2,1)S(1)}, bf16[2,264,128]{2,1,0:T(8,128)(2,1)S(1)}, u32[]{:S(2)}, u32[]{:S(2)}) collective-permute-start(bf16[2,264,128]{2,1,0:T(8,128)(2,1)S(1)} %shard_map.141.refs_0_), channel_id=1, source_target_pairs={{0,8},{8,16},{16,24},{24,0},{1,9},{9,17},{17,25},{25,1},{2,10},{10... | collective-permute-start | bytes 405512 | tf_op jit(solution)/shard_map/ppermute | solution.py:220
  59.9 33.0 %collective-permute-start = (bf16[2,264,128]{2,1,0:T(8,128)(2,1)S(1)}, bf16[2,264,128]{2,1,0:T(8,128)(2,1)S(1)}, u32[]{:S(2)}, u32[]{:S(2)}) collective-permute-start(bf16[2,264,128]{2,1,0:T(8,128)(2,1)S(1)} %shard_map.141.refs_0_), channel_id=1, source_target_pairs={{0,16},{8,24},{16,0},{24,8},{1,17},{9,25},{17,1},{25,9},{2,18},{10... | collective-permute-start | bytes 405512 | tf_op jit(solution)/shard_map/ppermute | solution.py:220
  92.9 9.2 %collective-permute-start.3 = (bf16[4,264,128]{2,1,0:T(8,128)(2,1)S(1)}, bf16[4,264,128]{2,1,0:T(8,128)(2,1)S(1)}, u32[]{:S(2)}, u32[]{:S(2)}) collective-permute-start(bf16[4,264,128]{2,1,0:T(8,128)(2,1)S(1)} %shard_map.142), channel_id=1, source_target_pairs={{0,32},{32,0},{1,33},{33,1},{2,34},{34,2},{3,35},{35,3},{4,36},{36... | collective-permute-start | bytes 811016 | tf_op jit(solution)/shard_map/ppermute | solution.py:225
  115.7 20.2 %copy-start.5 = (f32[64,1,64,64]{3,2,1,0:T(8,128)S(1)}, f32[64,1,64,64]{3,2,1,0:T(8,128)}, u32[]{:S(2)}) copy-start(f32[64,1,64,64]{3,2,1,0:T(8,128)} %param.25) | copy-start | bytes 3145732
  128.8 16.7 %all-to-all-start.5 = ((bf16[16,64,128]{2,1,0:T(8,128)(2,1)}), bf16[16,64,128]{2,1,0:T(8,128)(2,1)S(1)}, u32[]{:S(2)}, u32[]{:S(2)}) async-start(bf16[16,64,128]{2,1,0:T(8,128)(2,1)} %bitcast.11), calls=%async_computation.5 | async-start | bytes 524288 | tf_op jit(solution)/shard_map/all_to_all | solution.py:29

commit v2 on v0

v2 whole, which is shorter than its diff:
```python
import jax
import jax.numpy as jnp
import numpy as np
from jax import lax
from jax.experimental import pallas as pl
from jax.experimental.pallas import tpu as pltpu
from jax.sharding import Mesh
from jax.sharding import PartitionSpec as P

D = 2048
HEADS = 16
HEAD_DIM = 64
EPS = 1e-06
THETA = 10000.0

KV = ("y", "xh", "xl")
TP = ("b3", "b2", "b1", "b0", "c")
HALF = "xl"
COLS = ("y", "xh")
PLANES = ("b0", "c")
FAR = ("b3", "b2", "b1")

bf16, f32 = jnp.bfloat16, jnp.float32
NT = (((1,), (1,)), ((), ()))


def size_of(axes):
    return int(np.prod([lax.axis_size(a) for a in axes]))


def swap(blocks, axes):
    return lax.all_to_all(blocks, axes, split_axis=0, concat_axis=0, tiled=True)


def call(kernel, out, *operands, scalars=(), flops=1 << 20):
    outs = out if isinstance(out, tuple) else (out,)
    moved = sum(o.size * o.dtype.itemsize for o in operands)
    moved += sum(int(np.prod(o.shape)) * o.dtype.itemsize for o in outs)
    smem = pl.BlockSpec(memory_space=pltpu.SMEM)
    vmem = pl.BlockSpec(memory_space=pltpu.VMEM)
    return pl.pallas_call(
        kernel,
        out_shape=out,
        in_specs=[smem] * len(scalars) + [vmem] * len(operands),
        out_specs=(vmem,) * len(out) if isinstance(out, tuple) else vmem,
        compiler_params=pltpu.CompilerParams(vmem_limit_bytes=32 << 20),
        cost_estimate=pl.CostEstimate(flops=flops, bytes_accessed=moved, transcendentals=0),
    )(*(jnp.reshape(v, (1,)) for v in scalars), *operands)


def pack_kernel(tokens_ref, up_ref, down_ref, gain_ref, out_ref):
    served, feats = tokens_ref.shape
    cols = out_ref.shape[0] // 2
    units = up_ref.shape[1] // cols
    gain = gain_ref[...]
    first = gain.astype(bf16).astype(f32)
    second = (gain - first).astype(bf16).astype(f32)
    third = gain - first - second
    row = lax.broadcasted_iota(jnp.int32, (8, feats), 0)
    zero = jnp.zeros((8, feats), f32)
    rows = jnp.where(row == 0, first, jnp.where(row == 1, second, jnp.where(row == 2, third, zero)))
    rows = rows.astype(bf16)
    up = up_ref[...].astype(f32).T.astype(bf16)
    tokens = tokens_ref[...]
    at = served + 2 * units
    for j in range(cols):
        for half in range(2):
            k = 2 * j + half
            out_ref[k, :served] = tokens
            out_ref[k, served : served + units] = up[j * units : (j + 1) * units]
            out_ref[k, served + units : at] = down_ref[j * units : (j + 1) * units]
            out_ref[k, at:] = rows


def unpack_kernel(side_ref, arrived_ref, gain_ref, mine_ref, normed_ref):
    feats = arrived_ref.shape[2]
    served = normed_ref.shape[0]
    both = mine_ref.shape[0]
    for j in range(arrived_ref.shape[0] // 2):
        mine_ref[:, j * feats : (j + 1) * feats] = arrived_ref[
            2 * j + side_ref[0], served : served + both
        ]
    total = jnp.zeros((served, feats), f32)
    for k in range(arrived_ref.shape[0]):
        x = arrived_ref[k, :served].astype(f32)
        total = total + x * x
    factor = lax.rsqrt(jnp.sum(total, axis=1, keepdims=True) / D + EPS)
    for k in range(arrived_ref.shape[0]):
        at = slice(k * feats, (k + 1) * feats)
        x = arrived_ref[k, :served].astype(f32)
        normed_ref[:, at] = (x * factor * gain_ref[:, at]).astype(bf16)


def retention_kernel(
    decay_ref,
    normed_ref,
    query_ref,
    key_ref,
    value_ref,
    gate_ref,
    output_ref,
    cosine_ref,
    sine_ref,
    state_ref,
    gain_ref,
    shares_ref,
    keys_ref,
    values_ref,
    readout_ref,
):
    normed = normed_ref[...]
    middle = HEAD_DIM // 2

    def project(weight):
        return lax.dot_general(normed, weight, NT, preferred_element_type=f32)

    def rotated(ref):
        plain = project(ref[...])
        turned = project(jnp.concatenate([ref[middle:], ref[:middle]]))
        return plain * cosine_ref[...] + turned * sine_ref[...]

    queries = rotated(query_ref)
    keys = rotated(key_ref) * HEAD_DIM ** (-0.5)
    values = project(value_ref[...])
    gating = project(gate_ref[...])
    keys_ref[...] = keys
    values_ref[...] = values
    columns = queries.T
    for b in range(state_ref.shape[0]):
        readout_ref[b : b + 1] = jnp.sum(state_ref[b] * columns[:, b : b + 1], axis=0, keepdims=True)
    matched = jnp.sum(keys * queries, axis=1, keepdims=True)
    readout = decay_ref[0] * readout_ref[...] + matched * values
    square = jnp.sum(readout * readout, axis=1, keepdims=True) / HEAD_DIM
    grouped = readout * lax.rsqrt(square + EPS) * gain_ref[...]
    merged = (grouped * (gating * jax.nn.sigmoid(gating))).astype(bf16)
    shares = jnp.dot(merged, output_ref[...], preferred_element_type=f32).astype(bf16)
    feats = shares_ref.shape[2]
    for k in range(shares_ref.shape[0]):
        shares_ref[k] = shares[:, k * feats : (k + 1) * feats]


def sum_of(parts_ref):
    total = parts_ref[0].astype(f32)
    for k in range(1, parts_ref.shape[0]):
        total = total + parts_ref[k].astype(f32)
    return total


def after_kernel(parts_ref, tokens_ref, out_ref):
    block = (tokens_ref[...].astype(f32) + sum_of(parts_ref)).astype(bf16)
    for p in range(out_ref.shape[0]):
        out_ref[p] = block


def up_kernel(side_ref, rows_ref, arrived_ref, weights_ref, own_ref, sent_ref):
    cols, count, feats = rows_ref.shape
    lines = arrived_ref.shape[1]
    far = weights_ref.shape[0] // 64
    units = weights_ref.shape[0] // (2 * far)
    ones = jnp.ones((8, feats), bf16)
    total = jnp.zeros((8, count), f32)
    scaled = []
    for j in range(cols):
        x = rows_ref[j].astype(f32)
        pieces = arrived_ref[2 * j + side_ref[0], lines - 8 :].astype(f32)
        scaled.append((x * (pieces[0:1] + pieces[1:2] + pieces[2:3])).astype(bf16))
        square = x * x
        high = square.astype(bf16)
        low = (square - high.astype(f32)).astype(bf16)
        total = total + lax.dot_general(ones, high, NT, preferred_element_type=f32)
        total = total + lax.dot_general(ones, low, NT, preferred_element_type=f32)
    weight = jnp.concatenate(
        [weights_ref[2 * f * units : (2 * f + 1) * units] for f in range(far)]
    )
    part = lax.dot_general(
        jnp.concatenate(scaled, axis=1), weight, NT, preferred_element_type=f32
    )
    own_ref[:count] = part
    sent_ref[:count] = part.astype(bf16)
    high = total.astype(bf16).astype(f32)
    low = total - high
    row = lax.broadcasted_iota(jnp.int32, total.shape, 0)
    extra = jnp.where(row == 0, high, jnp.where(row == 1, low, jnp.zeros_like(total)))
    own_ref[count:] = extra
    sent_ref[count:] = extra.astype(bf16)


def down_kernel(own_ref, other_ref, weights_ref, out_ref):
    cols, count, feats = out_ref.shape
    far = weights_ref.shape[0] // 64
    units = weights_ref.shape[0] // (2 * far)
    total = own_ref[...] + other_ref[...].astype(f32)
    squares = total[count : count + 1] + total[count + 1 : count + 2]
    row = lax.broadcasted_iota(jnp.int32, (count, count), 0)
    lane = lax.broadcasted_iota(jnp.int32, (count, count), 1)
    mine = jnp.where(lane == row, squares, jnp.zeros((count, count), f32))
    factor = lax.rsqrt(jnp.sum(mine, axis=1, keepdims=True) / D + EPS)
    raised = jnp.maximum(total[:count] * factor, 0.0)
    hidden = (raised * raised).astype(bf16)
    weight = jnp.concatenate(
        [weights_ref[(2 * f + 1) * units : (2 * f + 2) * units] for f in range(far)]
    )
    part = jnp.dot(hidden, weight, preferred_element_type=f32).astype(bf16)
    for j in range(cols):
        out_ref[j] = part[:, j * feats : (j + 1) * feats]


def final_kernel(parts_ref, after_ref, out_ref):
    out_ref[...] = (after_ref[0].astype(f32) + sum_of(parts_ref)).astype(out_ref.dtype)


def layer(
    tokens,
    lengths,
    query_weight,
    key_weight,
    value_weight,
    gate_weight,
    output_weight,
    mixer_gain,
    group_gain,
    channel_gain,
    up_weight,
    down_weight,
    memory_state,
):
    like = jax.ShapeDtypeStruct
    served, feats = tokens.shape
    kv, cols, planes, far = size_of(KV), size_of(COLS), size_of(PLANES), size_of(FAR)
    units = up_weight.shape[1] // cols
    count = planes * served
    side = lax.axis_index(HALF)

    sent = call(
        pack_kernel,
        like((kv, served + 2 * units + 8, feats), bf16),
        tokens,
        up_weight,
        down_weight,
        channel_gain.reshape(1, feats),
    )
    arrived = swap(sent, KV)
    mine, normed = call(
        unpack_kernel,
        (like((2 * units, cols * feats), bf16), like((served, kv * feats), bf16)),
        arrived,
        mixer_gain.reshape(1, kv * feats),
        scalars=(side,),
    )
    weights = lax.all_gather(mine, FAR, axis=0, tiled=True)

    middle = HEAD_DIM // 2
    inverse = THETA ** (-jnp.arange(middle, dtype=f32) * 2.0 / HEAD_DIM)
    angles = lengths.astype(f32)[:, None] * inverse[None, :]
    cosine, sine = jnp.cos(angles), jnp.sin(angles)
    head = lax.axis_index(KV).astype(f32)
    decay = 1.0 - 2.0 ** (-5.0 - 5.0 * head / (HEADS - 1))
    state = memory_state[:, 0]
    shares, keys_new, values_new, _ = call(
        retention_kernel,
        (
            like((kv, served, feats), bf16),
            like((served, HEAD_DIM), f32),
            like((served, HEAD_DIM), f32),
            like((served, HEAD_DIM), f32),
        ),
        normed,
        query_weight.T,
        key_weight.T,
        value_weight.T,
        gate_weight.T,
        output_weight,
        jnp.concatenate([cosine, cosine], axis=1),
        jnp.concatenate([-sine, sine], axis=1),
        state,
        group_gain.reshape(1, HEAD_DIM),
        scalars=(decay,),
        flops=2 * served * D * 6 * HEAD_DIM,
    )
    shares = swap(shares, KV)
    after = call(after_kernel, like((cols * planes, served, feats), bf16), shares, tokens)

    rows = swap(after, COLS + PLANES).reshape(cols, count, feats)
    own, given = call(
        up_kernel,
        (like((count + 8, far * units), f32), like((count + 8, far * units), bf16)),
        rows,
        arrived,
        weights,
        scalars=(side,),
        flops=2 * count * cols * feats * far * units,
    )
    other = lax.ppermute(given, HALF, [(0, 1), (1, 0)])
    lowered = call(
        down_kernel,
        like((cols, count, feats), bf16),
        own,
        other,
        weights,
        flops=2 * count * cols * feats * far * units,
    )

    lowered = swap(lowered.reshape(cols * planes, served, feats), COLS + PLANES)
    mixed = call(final_kernel, like((served, feats), bf16), lowered, after)
    new_state = decay * state + keys_new[:, :, None] * values_new[:, None, :]
    return (mixed, new_state[:, None])


def solution(mesh):
    fine = Mesh(mesh.devices.reshape(4, 2, 2, 2, 2, 2, 2, 2), KV + TP)
    return jax.shard_map(
        layer,
        mesh=fine,
        in_specs=(
            P(TP, KV),
            P(TP),
            P(None, KV),
            P(None, KV),
            P(None, KV),
            P(None, KV),
            P(KV, None),
            P(None),
            P(KV),
            P(KV),
            P(KV, TP),
            P(TP, KV),
            P(TP, KV, None, None),
        ),
        out_specs=(P(TP, KV), P(TP, KV, None, None)),
        check_vma=False,
    )
```

time: 155 us -> 156 us (level)
  waiting for transfers between devices: 43.1 us -> 79.6 us
  starting transfers between devices: 55.9 us -> 32 us
  blocking collectives: 29.5 us -> 10.1 us
  between operations: 1.17 us -> 14.2 us
  Pallas kernels: 0 us -> 7.91 us
  matrix products: 6.81 us -> 0 us
  other arithmetic: 6.9 us -> 2.63 us
  local copies, waits for them, and re-layouts: 10.8 us -> 8.63 us
    all_gather x0 -> x1, waiting for transfers between devices: none -> 56.1 us  [layer(): weights = lax.all_gather(mine, FAR, axis=0, tiled=True)]
    ppermute x4 -> x1, waiting for transfers between devices: 31.3 us -> 3.61 us  [layer(): other = lax.ppermute(given, HALF, [(0, 1), (1, 0)])]
    ppermute x4 -> x1, starting transfers between devices: 28.9 us -> 2.14 us  [layer(): other = lax.ppermute(given, HALF, [(0, 1), (1, 0)])]
    all_to_all x2 -> x1, blocking collectives: 29.5 us -> 10.1 us  [swap(): return lax.all_to_all(blocks, axes, split_axis=0, concat_axis=0, tiled=True)]
    pallas_call x0 -> x7, Pallas kernels: none -> 7.91 us  [call(): pl.pallas_call(kernel, out_shape=out, in_specs=[smem] * len(scalars) + [v...]
    all_to_all x4 -> x3, waiting for transfers between devices: 11.8 us -> 19.2 us  [swap(): return lax.all_to_all(blocks, axes, split_axis=0, concat_axis=0, tiled=True)]
    unnamed x22 -> x30, local copies, waits for them, and re-layouts: 1.68 us -> 8.63 us
    dot_general x7 -> x0, matrix products: 6.81 us -> none  [the longest x3 2.55 us: project(): return jnp.dot(normed, weight, preferred_element_type=f32)]
  transfers between devices with their start and end apart: 8 -> 5, of which waited for: 4 -> 4; matrix products, arithmetic and copies ran while one was open for 7% -> 2% of each run, Pallas kernels for 0% -> 0%
where the time goes in v2:
time: 156 us; the launch traced here: 155 us
  waiting for transfers between devices  79.6 us (51%)
  starting transfers between devices  32 us (21%)
  between operations  14.2 us (9%)
  blocking collectives  10.1 us (6%)
  local copies, waits for them, and re-layouts  8.63 us (6%)
  Pallas kernels  7.91 us (5%)
  other arithmetic  2.63 us (2%)
    all_gather x1, waiting for transfers between devices, layer(): weights = lax.all_gather(mine, FAR, axis=0, tiled=True)  56.1 us
    all_to_all x3, starting transfers between devices, swap(): return lax.all_to_all(blocks, axes, split_axis=0, concat_axis=0, tiled=True)  29.8 us
    all_to_all x3, waiting for transfers between devices, swap(): return lax.all_to_all(blocks, axes, split_axis=0, concat_axis=0, tiled=True)  19.2 us
    all_to_all x1, blocking collectives, swap(): return lax.all_to_all(blocks, axes, split_axis=0, concat_axis=0, tiled=True)  10.1 us
    unnamed x30, local copies, waits for them, and re-layouts  8.63 us
    pallas_call x7, Pallas kernels, call(): pl.pallas_call(kernel, out_shape=out, in_specs=[smem] * len(scalars) + [v...  7.91 us
    ppermute x1, waiting for transfers between devices, layer(): other = lax.ppermute(given, HALF, [(0, 1), (1, 0)])  3.61 us
  transfers between devices with their start and end apart: 5, of which 4 were waited for; matrix products, arithmetic and copies ran while one was open for 2% of the time, Pallas kernels for 0%

profile of v2, /device:TPU:1, one launch (start us, length us, event | category | flops | bytes accessed | tf_op | source)
XLA Modules:
  0.0 155.1 jit_solution(178730417832031816)
XLA Ops:
  7.2 0.0 copy-start
  7.2 0.0 copy-start.4
  7.2 0.0 copy-start.3
  7.2 0.0 copy-start.8
  7.2 1.0 copy-done.8
  8.2 0.0 copy-start.9
  8.2 0.8 copy-done.9
  9.0 0.0 copy-start.10
  9.0 0.7 copy-done.10
  9.7 0.0 copy-start.13
  9.7 0.7 copy-done.13
  10.4 0.9 shard_map.140
  11.3 7.6 %all-to-all-start = ((bf16[16,136,128]{2,1,0:T(8,128)(2,1)}), bf16[16,136,128]{2,1,0:T(8,128)(2,1)S(1)}, u32[]{:S(2)}, u32[]{:S(2)}) async-start(bf16[16,136,128]{2,1,0:T(8,128)(2,1)} %shard_map.140), calls=%async_computation | async-start | bytes 1114112 | tf_op jit(solution)/shard_map/all_to_all | solution.py:32
  18.9 0.7 convert_element_type.7
  19.6 0.2 fusion
  19.8 0.1 pad_maximum_fusion
  19.9 8.3 %all-to-all-done.arrived_ref = bf16[16,136,128]{2,1,0:T(8,128)(2,1)S(1)} async-done(((bf16[16,136,128]{2,1,0:T(8,128)(2,1)}), bf16[16,136,128]{2,1,0:T(8,128)(2,1)S(1)}, u32[]{:S(2)}, u32[]{:S(2)}) %all-to-all-start) | async-done | bytes 557088 | tf_op jit(solution)/shard_map/all_to_all | solution.py:32
  28.2 0.0 copy-start.12
  28.2 0.7 copy-done.12
  28.9 0.7 shard_map.141
  29.6 0.0 copy-done
  29.6 0.0 copy-done.4
  29.6 0.0 copy-done.3
  29.6 0.0 copy-start.5
  29.6 0.9 copy-done.5
  30.6 0.0 copy-start.6
  30.6 0.9 copy-done.6
  31.5 0.9 copy-done.7
  32.5 0.7 copy-done.14
  33.2 1.9 %shard_map.142 = (bf16[16,64,128]{2,1,0:T(8,128)(2,1)S(1)}, f32[64,64]{1,0:T(8,128)S(1)}, f32[64,64]{1,0:T(8,128)S(1)}, f32[64,64]{1,0:T(8,128)}) custom-call(f32[1]{0:T(128)} %bitcast.1.decay_ref, bf16[64,2048]{1,0:T(8,128)(2,1)S(1)} %get-tuple-element.9.normed_ref, bf16[64,2048]{1,0:T(8,128)(2,1)S(1)} %bitcast.14, bf16[64,2048]{1,0:T(8,128)(2,1)S(1)} %bitcast.15, ...), custom_call_target="tpu_custom_call" | custom-call | flops 100663296 | bytes 2965760 | tf_op jit(solution)/shard_map/pallas_call | solution.py:41
  35.0 10.1 %all_to_all.20.parts_ref = bf16[16,64,128]{2,1,0:T(8,128)(2,1)S(1)} all-to-all(bf16[16,64,128]{2,1,0:T(8,128)(2,1)S(1)} %get-tuple-element.10), channel_id=1, replica_groups=mesh['y'=4,'xh'=2,'xl'=2,'b3'=2,'b2'=2,'b1'=2,'b0'=2,'c'=2] {'y','xh','xl'}, dimensions={0} | all-to-all | bytes 524288 | tf_op jit(solution)/shard_map/all_to_all | solution.py:32
  45.2 0.0 copy-done.11
  45.2 0.9 shard_map.143.after_ref
  46.1 9.5 %all-to-all-start.2 = ((bf16[32,64,128]{2,1,0:T(8,128)(2,1)}), bf16[32,64,128]{2,1,0:T(8,128)(2,1)S(1)}, u32[]{:S(2)}, u32[]{:S(2)}) async-start(bf16[32,64,128]{2,1,0:T(8,128)(2,1)} %shard_map.143.after_ref), calls=%async_computation.2 | async-start | bytes 1048576 | tf_op jit(solution)/shard_map/all_to_all | solution.py:32
  55.6 0.0 all-gather.2.cloned.1.call-start
  55.7 0.7 all-gather.2.cloned.1.call-update
  56.3 56.1 %all-gather.2.cloned.1.call-done.weights_ref = bf16[512,1024]{1,0:T(8,128)(2,1)} async-done(((bf16[64,1024]{1,0:T(8,128)(2,1)}), bf16[512,1024]{1,0:T(8,128)(2,1)}) %all-gather.2.cloned.1.call-update) | async-done | bytes 1048592 | tf_op jit(solution)/shard_map/all_gather | solution.py:250
  112.4 0.0 all-to-all-done.2
  112.4 1.2 copy-done.1
  113.6 0.6 shard_map.144
  114.2 2.1 %collective-permute-start = (bf16[264,256]{1,0:T(8,128)(2,1)S(1)}, bf16[264,256]{1,0:T(8,128)(2,1)S(1)}, u32[]{:S(2)}, u32[]{:S(2)}) collective-permute-start(bf16[264,256]{1,0:T(8,128)(2,1)S(1)} %get-tuple-element.13), channel_id=1, source_target_pairs={{0,32},{32,0},{1,33},{33,1},{2,34},{34,2},{3,35},{35,3},{4,36},{36... | collective-permute-start | bytes 405512 | tf_op jit(solution)/shard_map/ppermute | solution.py:293
  116.4 3.6 %collective-permute-done.other_ref = bf16[264,256]{1,0:T(8,128)(2,1)S(1)} collective-permute-done((bf16[264,256]{1,0:T(8,128)(2,1)S(1)}, bf16[264,256]{1,0:T(8,128)(2,1)S(1)}, u32[]{:S(2)}, u32[]{:S(2)}) %collective-permute-start) | collective-permute-done | bytes 135200 | tf_op jit(solution)/shard_map/ppermute | solution.py:293
  120.0 0.0 copy-done.2
  120.0 1.2 shard_map.145
  121.2 12.7 %all-to-all-start.3 = ((bf16[32,64,128]{2,1,0:T(8,128)(2,1)}), bf16[32,64,128]{2,1,0:T(8,128)(2,1)S(1)}, u32[]{:S(2)}, u32[]{:S(2)}) async-start(bf16[32,64,128]{2,1,0:T(8,128)(2,1)} %bitcast.11), calls=%async_computation.3 | async-start | bytes 1048576 | tf_op jit(solution)/shard_map/all_to_all | solution.py:32
  133.9 1.7 %multiply_add_fusion = f32[64,1,64,64]{3,2,1,0:T(8,128)} fusion(f32[64,1,64,64]{3,2,1,0:T(8,128)S(1)} %copy-done, f32[64,64]{1,0:T(8,128)S(1)} %get-tuple-element.15, f32[64,64]{1,0:T(8,128)S(1)} %get-tuple-element.14, f32[]{:T(128)} %sub.7), kind=kLoop, calls=%fused_computation | loop fusion | flops 786432 | bytes 2129924 | tf_op jit(solution)/shard_map/add | solution.py:305
  135.6 10.9 %all-to-all-done.3.parts_ref = bf16[32,64,128]{2,1,0:T(8,128)(2,1)S(1)} async-done(((bf16[32,64,128]{2,1,0:T(8,128)(2,1)}), bf16[32,64,128]{2,1,0:T(8,128)(2,1)S(1)}, u32[]{:S(2)}, u32[]{:S(2)}) %all-to-all-start.3) | async-done | bytes 524320 | tf_op jit(solution)/shard_map/all_to_all | solution.py:32
  146.5 1.7 %shard_map.146 = bf16[64,128]{1,0:T(8,128)(2,1)} custom-call(bf16[32,64,128]{2,1,0:T(8,128)(2,1)S(1)} %all-to-all-done.3.parts_ref, bf16[32,64,128]{2,1,0:T(8,128)(2,1)} %shard_map.143.after_ref), custom_call_target="tpu_custom_call" | custom-call | flops 1048576 | bytes 1064960 | tf_op jit(solution)/shard_map/pallas_call | solution.py:41
  (6 shorter events, 0.0 us)
Async XLA Ops:
  7.2 22.5 %copy-start = (f32[64,1,64,64]{3,2,1,0:T(8,128)S(1)}, f32[64,1,64,64]{3,2,1,0:T(8,128)}, u32[]{:S(2)}) copy-start(f32[64,1,64,64]{3,2,1,0:T(8,128)} %param.25) | copy-start | bytes 3145732
  7.2 22.5 %copy-start.4 = (bf16[2048,64]{0,1:T(8,128)(2,1)S(1)}, bf16[2048,64]{0,1:T(8,128)(2,1)}, u32[]{:S(2)}) copy-start(bf16[2048,64]{0,1:T(8,128)(2,1)} %param.16) | copy-start | bytes 786436
  7.2 22.5 %copy-start.3 = (bf16[2048,64]{0,1:T(8,128)(2,1)S(1)}, bf16[2048,64]{0,1:T(8,128)(2,1)}, u32[]{:S(2)}) copy-start(bf16[2048,64]{0,1:T(8,128)(2,1)} %param.15) | copy-start | bytes 786436
  7.2 1.0 copy-start.8
  8.2 0.8 copy-start.9
  9.0 0.7 copy-start.10
  9.7 0.7 copy-start.13
  11.3 16.9 %all-to-all-start = ((bf16[16,136,128]{2,1,0:T(8,128)(2,1)}), bf16[16,136,128]{2,1,0:T(8,128)(2,1)S(1)}, u32[]{:S(2)}, u32[]{:S(2)}) async-start(bf16[16,136,128]{2,1,0:T(8,128)(2,1)} %shard_map.140), calls=%async_computation | async-start | bytes 1114112 | tf_op jit(solution)/shard_map/all_to_all | solution.py:32
  28.2 0.7 copy-start.12
  29.6 1.0 copy-start.5
  30.6 0.9 copy-start.6
  31.5 0.9 copy-start.7
  32.5 0.7 copy-start.14
  33.1 12.0 %copy-start.11 = (bf16[64,128]{1,0:T(8,128)(2,1)S(1)}, bf16[64,128]{1,0:T(8,128)(2,1)}, u32[]{:S(2)}) copy-start(bf16[64,128]{1,0:T(8,128)(2,1)} %tokens_ref.3) | copy-start | bytes 49156
  46.1 66.4 %all-to-all-start.2 = ((bf16[32,64,128]{2,1,0:T(8,128)(2,1)}), bf16[32,64,128]{2,1,0:T(8,128)(2,1)S(1)}, u32[]{:S(2)}, u32[]{:S(2)}) async-start(bf16[32,64,128]{2,1,0:T(8,128)(2,1)} %shard_map.143.after_ref), calls=%async_computation.2 | async-start | bytes 1048576 | tf_op jit(solution)/shard_map/all_to_all | solution.py:32
  55.6 56.8 %all-gather.2.cloned.1.call-start = ((), (), s32[]{:S(2)}) async-start(), calls=%async_computation.4 | async-start | bytes 1179648 | tf_op jit(solution)/shard_map/all_gather | solution.py:250
  112.4 1.2 copy-start.1
  113.6 6.4 %copy-start.2 = (bf16[512,1024]{1,0:T(8,128)(2,1)S(1)}, bf16[512,1024]{1,0:T(8,128)(2,1)}, u32[]{:S(2)}) copy-start(bf16[512,1024]{1,0:T(8,128)(2,1)} %all-gather.2.cloned.1.call-done.weights_ref) | copy-start | bytes 3145732
  114.2 5.8 %collective-permute-start = (bf16[264,256]{1,0:T(8,128)(2,1)S(1)}, bf16[264,256]{1,0:T(8,128)(2,1)S(1)}, u32[]{:S(2)}, u32[]{:S(2)}) collective-permute-start(bf16[264,256]{1,0:T(8,128)(2,1)S(1)} %get-tuple-element.13), channel_id=1, source_target_pairs={{0,32},{32,0},{1,33},{33,1},{2,34},{34,2},{3,35},{35,3},{4,36},{36... | collective-permute-start | bytes 405512 | tf_op jit(solution)/shard_map/ppermute | solution.py:293
  121.2 25.3 %all-to-all-start.3 = ((bf16[32,64,128]{2,1,0:T(8,128)(2,1)}), bf16[32,64,128]{2,1,0:T(8,128)(2,1)S(1)}, u32[]{:S(2)}, u32[]{:S(2)}) async-start(bf16[32,64,128]{2,1,0:T(8,128)(2,1)} %bitcast.11), calls=%async_computation.3 | async-start | bytes 1048576 | tf_op jit(solution)/shard_map/all_to_all | solution.py:32
Sparse Core Ops, SparseCore 0:
  59.1 53.2 all-gather.1

commit v3 on v2

--- a/solution.py
+++ b/solution.py
@@ -32,26 +32,47 @@
     return lax.all_to_all(blocks, axes, split_axis=0, concat_axis=0, tiled=True)
 
 
-def call(kernel, out, *operands, scalars=(), flops=1 << 20):
+def call(kernel, out, *operands, scalars=(), hbm=(), scratch=(), limit=16 << 20, flops=1 << 20):
     outs = out if isinstance(out, tuple) else (out,)
     moved = sum(o.size * o.dtype.itemsize for o in operands)
     moved += sum(int(np.prod(o.shape)) * o.dtype.itemsize for o in outs)
     smem = pl.BlockSpec(memory_space=pltpu.SMEM)
     vmem = pl.BlockSpec(memory_space=pltpu.VMEM)
+    far = pl.BlockSpec(memory_space=pltpu.HBM)
     return pl.pallas_call(
         kernel,
         out_shape=out,
-        in_specs=[smem] * len(scalars) + [vmem] * len(operands),
+        in_specs=[smem] * len(scalars)
+        + [far if n in hbm else vmem for n in range(len(operands))],
         out_specs=(vmem,) * len(out) if isinstance(out, tuple) else vmem,
-        compiler_params=pltpu.CompilerParams(vmem_limit_bytes=32 << 20),
+        scratch_shapes=scratch,
+        compiler_params=pltpu.CompilerParams(vmem_limit_bytes=limit),
         cost_estimate=pl.CostEstimate(flops=flops, bytes_accessed=moved, transcendentals=0),
     )(*(jnp.reshape(v, (1,)) for v in scalars), *operands)
 
 
-def pack_kernel(tokens_ref, up_ref, down_ref, gain_ref, out_ref):
-    served, feats = tokens_ref.shape
-    cols = out_ref.shape[0] // 2
-    units = up_ref.shape[1] // cols
+def fetch(pairs, sems):
+    copies = [pltpu.make_async_copy(a, b, sems.at[n]) for n, (a, b) in enumerate(pairs)]
+    for copy in copies:
+        copy.start()
+    for copy in copies:
+        copy.wait()
+
+
+def pack_kernel(tokens_hbm, up_hbm, down_hbm, gain_hbm, out_ref, copies_ref, *scratch):
+    tokens_ref, up_ref, down_ref, gain_ref, sems = scratch
+    fetch(
+        (
+            (up_hbm, up_ref),
+            (down_hbm, down_ref),
+            (gain_hbm, gain_ref),
+            (tokens_hbm, tokens_ref),
+        ),
+        sems,
+    )
+    cols = out_ref.shape[0]
+    feats, width = up_ref.shape
+    units = width // cols
     gain = gain_ref[...]
     first = gain.astype(bf16).astype(f32)
     second = (gain - first).astype(bf16).astype(f32)
@@ -61,53 +82,43 @@
     rows = jnp.where(row == 0, first, jnp.where(row == 1, second, jnp.where(row == 2, third, zero)))
     rows = rows.astype(bf16)
     up = up_ref[...].astype(f32).T.astype(bf16)
+    for j in range(cols):
+        out_ref[j, :units] = up[j * units : (j + 1) * units]
+        out_ref[j, units : 2 * units] = down_ref[j * units : (j + 1) * units]
+        out_ref[j, 2 * units :] = rows
     tokens = tokens_ref[...]
-    at = served + 2 * units
-    for j in range(cols):
-        for half in range(2):
-            k = 2 * j + half
-            out_ref[k, :served] = tokens
-            out_ref[k, served : served + units] = up[j * units : (j + 1) * units]
-            out_ref[k, served + units : at] = down_ref[j * units : (j + 1) * units]
-            out_ref[k, at:] = rows
-
-
-def unpack_kernel(side_ref, arrived_ref, gain_ref, mine_ref, normed_ref):
+    for k in range(copies_ref.shape[0]):
+        copies_ref[k] = tokens
+
+
+def unpack_kernel(arrived_ref, mine_ref):
     feats = arrived_ref.shape[2]
-    served = normed_ref.shape[0]
     both = mine_ref.shape[0]
-    for j in range(arrived_ref.shape[0] // 2):
-        mine_ref[:, j * feats : (j + 1) * feats] = arrived_ref[
-            2 * j + side_ref[0], served : served + both
-        ]
+    for j in range(arrived_ref.shape[0]):
+        mine_ref[:, j * feats : (j + 1) * feats] = arrived_ref[j, :both]
+
+
+def retention_kernel(decay_ref, *refs):
+    sources, (shares_ref, keys_ref, values_ref) = refs[:11], refs[11:14]
+    targets, (normed_ref, readout_ref, sems) = refs[14:25], refs[25:]
+    copies = [
+        pltpu.make_async_copy(a, b, sems.at[n]) for n, (a, b) in enumerate(zip(sources, targets))
+    ]
+    for copy in copies:
+        copy.start()
+    blocks_ref, mixer_ref, query_ref, key_ref, value_ref, gate_ref = targets[:6]
+    cosine_ref, sine_ref, state_ref, output_ref, gain_ref = targets[6:]
+    kv, served, feats = blocks_ref.shape
+    for copy in copies[:2]:
+        copy.wait()
     total = jnp.zeros((served, feats), f32)
-    for k in range(arrived_ref.shape[0]):
-        x = arrived_ref[k, :served].astype(f32)
+    for k in range(kv):
+        x = blocks_ref[k].astype(f32)
         total = total + x * x
     factor = lax.rsqrt(jnp.sum(total, axis=1, keepdims=True) / D + EPS)
-    for k in range(arrived_ref.shape[0]):
+    for k in range(kv):
         at = slice(k * feats, (k + 1) * feats)
-        x = arrived_ref[k, :served].astype(f32)
-        normed_ref[:, at] = (x * factor * gain_ref[:, at]).astype(bf16)
-
-
-def retention_kernel(
-    decay_ref,
-    normed_ref,
-    query_ref,
-    key_ref,
-    value_ref,
-    gate_ref,
-    output_ref,
-    cosine_ref,
-    sine_ref,
-    state_ref,
-    gain_ref,
-    shares_ref,
-    keys_ref,
-    values_ref,
-    readout_ref,
-):
+        normed_ref[:, at] = (blocks_ref[k].astype(f32) * factor * mixer_ref[:, at]).astype(bf16)
     normed = normed_ref[...]
     middle = HEAD_DIM // 2
 
@@ -119,6 +130,8 @@
         turned = project(jnp.concatenate([ref[middle:], ref[:middle]]))
         return plain * cosine_ref[...] + turned * sine_ref[...]
 
+    for copy in copies[2:]:
+        copy.wait()
     queries = rotated(query_ref)
     keys = rotated(key_ref) * HEAD_DIM ** (-0.5)
     values = project(value_ref[...])
@@ -152,28 +165,27 @@
         out_ref[p] = block
 
 
-def up_kernel(side_ref, rows_ref, arrived_ref, weights_ref, own_ref, sent_ref):
+def up_kernel(rows_ref, arrived_ref, weights_ref, own_ref, sent_ref):
     cols, count, feats = rows_ref.shape
     lines = arrived_ref.shape[1]
-    far = weights_ref.shape[0] // 64
-    units = weights_ref.shape[0] // (2 * far)
+    far, _, units, width = weights_ref.shape
     ones = jnp.ones((8, feats), bf16)
     total = jnp.zeros((8, count), f32)
     scaled = []
     for j in range(cols):
         x = rows_ref[j].astype(f32)
-        pieces = arrived_ref[2 * j + side_ref[0], lines - 8 :].astype(f32)
+        pieces = arrived_ref[j, lines - 8 :].astype(f32)
         scaled.append((x * (pieces[0:1] + pieces[1:2] + pieces[2:3])).astype(bf16))
         square = x * x
         high = square.astype(bf16)
         low = (square - high.astype(f32)).astype(bf16)
         total = total + lax.dot_general(ones, high, NT, preferred_element_type=f32)
         total = total + lax.dot_general(ones, low, NT, preferred_element_type=f32)
-    weight = jnp.concatenate(
-        [weights_ref[2 * f * units : (2 * f + 1) * units] for f in range(far)]
-    )
     part = lax.dot_general(
-        jnp.concatenate(scaled, axis=1), weight, NT, preferred_element_type=f32
+        jnp.concatenate(scaled, axis=1),
+        weights_ref[:, 0].reshape(far * units, width),
+        NT,
+        preferred_element_type=f32,
     )
     own_ref[:count] = part
     sent_ref[:count] = part.astype(bf16)
@@ -187,8 +199,6 @@
 
 def down_kernel(own_ref, other_ref, weights_ref, out_ref):
     cols, count, feats = out_ref.shape
-    far = weights_ref.shape[0] // 64
-    units = weights_ref.shape[0] // (2 * far)
     total = own_ref[...] + other_ref[...].astype(f32)
     squares = total[count : count + 1] + total[count + 1 : count + 2]
     row = lax.broadcasted_iota(jnp.int32, (count, count), 0)
@@ -197,9 +207,7 @@
     factor = lax.rsqrt(jnp.sum(mine, axis=1, keepdims=True) / D + EPS)
     raised = jnp.maximum(total[:count] * factor, 0.0)
     hidden = (raised * raised).astype(bf16)
-    weight = jnp.concatenate(
-        [weights_ref[(2 * f + 1) * units : (2 * f + 2) * units] for f in range(far)]
-    )
+    weight = weights_ref[:, 1].reshape(-1, weights_ref.shape[3])
     part = jnp.dot(hidden, weight, preferred_element_type=f32).astype(bf16)
     for j in range(cols):
         out_ref[j] = part[:, j * feats : (j + 1) * feats]
@@ -229,65 +237,83 @@
     kv, cols, planes, far = size_of(KV), size_of(COLS), size_of(PLANES), size_of(FAR)
     units = up_weight.shape[1] // cols
     count = planes * served
-    side = lax.axis_index(HALF)
-
-    sent = call(
+    sent, copies = call(
         pack_kernel,
-        like((kv, served + 2 * units + 8, feats), bf16),
+        (like((cols, 2 * units + 8, feats), bf16), like((kv, served, feats), bf16)),
         tokens,
         up_weight,
         down_weight,
         channel_gain.reshape(1, feats),
-    )
-    arrived = swap(sent, KV)
-    mine, normed = call(
-        unpack_kernel,
-        (like((2 * units, cols * feats), bf16), like((served, kv * feats), bf16)),
-        arrived,
-        mixer_gain.reshape(1, kv * feats),
-        scalars=(side,),
-    )
+        hbm=(0, 1, 2, 3),
+        limit=63 << 20,
+        scratch=(
+            pltpu.VMEM(tokens.shape, bf16),
+            pltpu.VMEM(up_weight.shape, bf16),
+            pltpu.VMEM(down_weight.shape, bf16),
+            pltpu.VMEM((1, feats), f32),
+            pltpu.SemaphoreType.DMA((4,)),
+        ),
+    )
+    arrived = swap(sent, COLS)
+    mine = call(unpack_kernel, like((2 * units, cols * feats), bf16), arrived)
     weights = lax.all_gather(mine, FAR, axis=0, tiled=True)
 
+    blocks = swap(copies, KV)
     middle = HEAD_DIM // 2
     inverse = THETA ** (-jnp.arange(middle, dtype=f32) * 2.0 / HEAD_DIM)
     angles = lengths.astype(f32)[:, None] * inverse[None, :]
     cosine, sine = jnp.cos(angles), jnp.sin(angles)
+    both_cosine = jnp.concatenate([cosine, cosine], axis=1)
+    both_sine = jnp.concatenate([-sine, sine], axis=1)
     head = lax.axis_index(KV).astype(f32)
     decay = 1.0 - 2.0 ** (-5.0 - 5.0 * head / (HEADS - 1))
     state = memory_state[:, 0]
-    shares, keys_new, values_new, _ = call(
+    operands = (
+        blocks,
+        mixer_gain.reshape(1, kv * feats),
+        query_weight.T,
+        key_weight.T,
+        value_weight.T,
+        gate_weight.T,
+        both_cosine,
+        both_sine,
+        state,
+        output_weight,
+        group_gain.reshape(1, HEAD_DIM),
+    )
+    shares, keys_new, values_new = call(
         retention_kernel,
         (
             like((kv, served, feats), bf16),
             like((served, HEAD_DIM), f32),
             like((served, HEAD_DIM), f32),
-            like((served, HEAD_DIM), f32),
-        ),
-        normed,
-        query_weight.T,
-        key_weight.T,
-        value_weight.T,
-        gate_weight.T,
-        output_weight,
-        jnp.concatenate([cosine, cosine], axis=1),
-        jnp.concatenate([-sine, sine], axis=1),
-        state,
-        group_gain.reshape(1, HEAD_DIM),
+        ),
+        *operands,
         scalars=(decay,),
+        hbm=tuple(range(len(operands))),
+        scratch=(
+            *(pltpu.VMEM(a.shape, a.dtype) for a in operands),
+            pltpu.VMEM((served, kv * feats), bf16),
+            pltpu.VMEM((served, HEAD_DIM), f32),
+            pltpu.SemaphoreType.DMA((len(operands),)),
+        ),
+        limit=63 << 20,
         flops=2 * served * D * 6 * HEAD_DIM,
     )
     shares = swap(shares, KV)
     after = call(after_kernel, like((cols * planes, served, feats), bf16), shares, tokens)
 
     rows = swap(after, COLS + PLANES).reshape(cols, count, feats)
+    weights = weights.reshape(far, 2, units, cols * feats)
     own, given = call(
         up_kernel,
-        (like((count + 8, far * units), f32), like((count + 8, far * units), bf16)),
+        (
+            like((count + 8, far * units), f32),
+            like((count + 8, far * units), bf16),
+        ),
         rows,
         arrived,
         weights,
-        scalars=(side,),
         flops=2 * count * cols * feats * far * units,
     )
     other = lax.ppermute(given, HALF, [(0, 1), (1, 0)])

time: 156 us -> 160 us (1.026)
  local copies, waits for them, and re-layouts: 8.63 us -> 1.95 us
  starting transfers between devices: 32 us -> 35.6 us
  Pallas kernels: 7.91 us -> 11.2 us
  waiting for transfers between devices: 79.6 us -> 81.9 us
    unnamed x30 -> x14, local copies, waits for them, and re-layouts: 8.63 us -> 1.95 us
    all_to_all x3 -> x4, waiting for transfers between devices: 19.2 us -> 23.1 us  [swap(): return lax.all_to_all(blocks, axes, split_axis=0, concat_axis=0, tiled=True)]
    all_to_all x3 -> x4, starting transfers between devices: 29.8 us -> 33.3 us  [swap(): return lax.all_to_all(blocks, axes, split_axis=0, concat_axis=0, tiled=True)]
    pallas_call x7, Pallas kernels: 7.91 us -> 11.2 us  [call(): pl.pallas_call(kernel, out_shape=out, in_specs=[smem] * len(scalars) + [f...]
  transfers between devices with their start and end apart: 5 -> 6, of which waited for: 4 -> 5; matrix products, arithmetic and copies ran while one was open for 2% -> 2% of each run, Pallas kernels for 0% -> 1%
where the time goes in v3:
time: 160 us; the launch traced here: 159 us
  waiting for transfers between devices  81.9 us (51%)
  starting transfers between devices  35.6 us (22%)
  between operations  14.2 us (9%)
  Pallas kernels  11.2 us (7%)
  blocking collectives  11 us (7%)
  other arithmetic  3.27 us (2%)
  local copies, waits for them, and re-layouts  1.95 us (1%)
    all_gather x1, waiting for transfers between devices, layer(): weights = lax.all_gather(mine, FAR, axis=0, tiled=True)  55.2 us
    all_to_all x4, starting transfers between devices, swap(): return lax.all_to_all(blocks, axes, split_axis=0, concat_axis=0, tiled=True)  33.3 us
    all_to_all x4, waiting for transfers between devices, swap(): return lax.all_to_all(blocks, axes, split_axis=0, concat_axis=0, tiled=True)  23.1 us
    pallas_call x7, Pallas kernels, call(): pl.pallas_call(kernel, out_shape=out, in_specs=[smem] * len(scalars) + [f...  11.2 us
    all_to_all x1, blocking collectives, swap(): return lax.all_to_all(blocks, axes, split_axis=0, concat_axis=0, tiled=True)  11 us
    ppermute x1, waiting for transfers between devices, layer(): other = lax.ppermute(given, HALF, [(0, 1), (1, 0)])  3.61 us
  transfers between devices with their start and end apart: 6, of which 5 were waited for; matrix products, arithmetic and copies ran while one was open for 2% of the time, Pallas kernels for 1%

profile of v3, /device:TPU:1, one launch (start us, length us, event | category | flops | bytes accessed | tf_op | source)
XLA Modules:
  0.0 159.1 jit_solution(15303617228891504317)
XLA Ops:
  7.2 1.7 %shard_map.140 = (bf16[8,72,128]{2,1,0:T(8,128)(2,1)}, bf16[16,64,128]{2,1,0:T(8,128)(2,1)}) custom-call(bf16[64,128]{1,0:T(8,128)(2,1)} %tokens_ref.1, bf16[128,256]{1,0:T(8,128)(2,1)} %up_hbm.1, bf16[256,128]{1,0:T(8,128)(2,1)} %down_hbm.1, f32[1,128]{1,0:T(1,128)} %bitcast.21), custom_call_target="tpu_custom_call" | custom-call | flops 1048576 | bytes 557568 | tf_op jit(solution)/shard_map/pallas_call | solution.py:42
  8.9 7.6 %all-to-all-start = ((bf16[16,64,128]{2,1,0:T(8,128)(2,1)}), bf16[16,64,128]{2,1,0:T(8,128)(2,1)S(1)}, u32[]{:S(2)}, u32[]{:S(2)}) async-start(bf16[16,64,128]{2,1,0:T(8,128)(2,1)} %get-tuple-element.9), calls=%async_computation | async-start | bytes 524288 | tf_op jit(solution)/shard_map/all_to_all | solution.py:32
  16.5 0.7 convert_element_type.7
  17.2 0.2 fusion
  17.4 0.7 pad_maximum_fusion
  18.1 6.0 %all-to-all-done.refs_0_ = bf16[16,64,128]{2,1,0:T(8,128)(2,1)S(1)} async-done(((bf16[16,64,128]{2,1,0:T(8,128)(2,1)}), bf16[16,64,128]{2,1,0:T(8,128)(2,1)S(1)}, u32[]{:S(2)}, u32[]{:S(2)}) %all-to-all-start) | async-done | bytes 262176 | tf_op jit(solution)/shard_map/all_to_all | solution.py:32
  24.2 0.0 copy-start.4
  24.2 0.7 copy-done.4
  24.9 0.0 copy-start.2
  24.9 4.4 %shard_map.141 = (bf16[16,64,128]{2,1,0:T(8,128)(2,1)}, f32[64,64]{1,0:T(8,128)}, f32[64,64]{1,0:T(8,128)}) custom-call(f32[1]{0:T(128)} %bitcast.decay_ref, bf16[16,64,128]{2,1,0:T(8,128)(2,1)} %copy-done.4, f32[1,2048]{1,0:T(1,128)} %bitcast.20, bf16[64,2048]{1,0:T(8,128)(2,1)} %bitcast.16, bf16[64,2048]{1,0:T(8,128)(2,1)} %bitcast.17, ...), custom_call_target="tpu_custom_call" | custom-call | flops 100663296 | bytes 2957568 | tf_op jit(solution)/shard_map/pallas_call | solution.py:42
  29.3 11.0 %all_to_all.25.parts_ref = bf16[16,64,128]{2,1,0:T(8,128)(2,1)S(1)} all-to-all(bf16[16,64,128]{2,1,0:T(8,128)(2,1)} %get-tuple-element.10), channel_id=1, replica_groups=mesh['y'=4,'xh'=2,'xl'=2,'b3'=2,'b2'=2,'b1'=2,'b0'=2,'c'=2] {'y','xh','xl'}, dimensions={0} | all-to-all | bytes 524288 | tf_op jit(solution)/shard_map/all_to_all | solution.py:32
  40.3 3.4 %all-to-all-start.3 = ((bf16[8,72,128]{2,1,0:T(8,128)(2,1)}), bf16[8,72,128]{2,1,0:T(8,128)(2,1)S(1)}, u32[]{:S(2)}, u32[]{:S(2)}) async-start(bf16[8,72,128]{2,1,0:T(8,128)(2,1)} %get-tuple-element.11), calls=%async_computation.3 | async-start | bytes 294912 | tf_op jit(solution)/shard_map/all_to_all | solution.py:32
  43.7 0.0 copy-done.2
  43.7 0.9 shard_map.142.after_ref
  44.6 6.1 %all-to-all-done.3.arrived_ref = bf16[8,72,128]{2,1,0:T(8,128)(2,1)S(1)} async-done(((bf16[8,72,128]{2,1,0:T(8,128)(2,1)}), bf16[8,72,128]{2,1,0:T(8,128)(2,1)S(1)}, u32[]{:S(2)}, u32[]{:S(2)}) %all-to-all-start.3) | async-done | bytes 147488 | tf_op jit(solution)/shard_map/all_to_all | solution.py:32
  50.8 9.6 %all-to-all-start.2 = ((bf16[32,64,128]{2,1,0:T(8,128)(2,1)}), bf16[32,64,128]{2,1,0:T(8,128)(2,1)S(1)}, u32[]{:S(2)}, u32[]{:S(2)}) async-start(bf16[32,64,128]{2,1,0:T(8,128)(2,1)} %shard_map.142.after_ref), calls=%async_computation.2 | async-start | bytes 1048576 | tf_op jit(solution)/shard_map/all_to_all | solution.py:32
  60.4 0.0 all-gather.2.cloned.1.call-start
  60.4 0.7 shard_map.143
  61.1 0.0 all-gather.2.cloned.1.call-update
  61.1 55.2 %all-gather.2.cloned.1.call-done = bf16[512,1024]{1,0:T(8,128)(2,1)} async-done(((bf16[64,1024]{1,0:T(8,128)(2,1)}), bf16[512,1024]{1,0:T(8,128)(2,1)}) %all-gather.2.cloned.1.call-update) | async-done | bytes 1048592 | tf_op jit(solution)/shard_map/all_gather | solution.py:259
  116.3 0.0 all-to-all-done.2
  116.3 0.0 copy-start
  116.3 1.2 copy-done
  117.5 0.0 copy-start.1
  117.5 0.0 copy-start.3
  117.6 0.0 copy-start.5
  117.6 0.0 copy-start.6
  117.6 0.6 shard_map.144
  118.1 2.3 %collective-permute-start = (bf16[264,256]{1,0:T(8,128)(2,1)S(1)}, bf16[264,256]{1,0:T(8,128)(2,1)S(1)}, u32[]{:S(2)}, u32[]{:S(2)}) collective-permute-start(bf16[264,256]{1,0:T(8,128)(2,1)S(1)} %get-tuple-element.13), channel_id=1, source_target_pairs={{0,32},{32,0},{1,33},{33,1},{2,34},{34,2},{3,35},{35,3},{4,36},{36... | collective-permute-start | bytes 405512 | tf_op jit(solution)/shard_map/ppermute | solution.py:319
  120.4 3.6 %collective-permute-done.other_ref = bf16[264,256]{1,0:T(8,128)(2,1)S(1)} collective-permute-done((bf16[264,256]{1,0:T(8,128)(2,1)S(1)}, bf16[264,256]{1,0:T(8,128)(2,1)S(1)}, u32[]{:S(2)}, u32[]{:S(2)}) %collective-permute-start) | collective-permute-done | bytes 135200 | tf_op jit(solution)/shard_map/ppermute | solution.py:319
  124.0 0.0 copy-done.1
  124.0 1.2 shard_map.145
  125.2 12.7 %all-to-all-start.4 = ((bf16[32,64,128]{2,1,0:T(8,128)(2,1)}), bf16[32,64,128]{2,1,0:T(8,128)(2,1)S(1)}, u32[]{:S(2)}, u32[]{:S(2)}) async-start(bf16[32,64,128]{2,1,0:T(8,128)(2,1)} %bitcast.11), calls=%async_computation.4 | async-start | bytes 1048576 | tf_op jit(solution)/shard_map/all_to_all | solution.py:32
  137.9 0.0 copy-done.3
  137.9 0.0 copy-done.5
  138.0 0.0 copy-done.6
  138.0 1.7 %multiply_add_fusion = f32[64,1,64,64]{3,2,1,0:T(8,128)} fusion(f32[64,1,64,64]{3,2,1,0:T(8,128)S(1)} %copy-done.3, f32[64,64]{1,0:T(8,128)S(1)} %copy-done.6, f32[64,64]{1,0:T(8,128)S(1)} %copy-done.5, f32[]{:T(128)} %sub.7), kind=kLoop, calls=%fused_computation | loop fusion | flops 786432 | bytes 2129924 | tf_op jit(solution)/shard_map/add | solution.py:331
  139.6 10.9 %all-to-all-done.4.parts_ref = bf16[32,64,128]{2,1,0:T(8,128)(2,1)S(1)} async-done(((bf16[32,64,128]{2,1,0:T(8,128)(2,1)}), bf16[32,64,128]{2,1,0:T(8,128)(2,1)S(1)}, u32[]{:S(2)}, u32[]{:S(2)}) %all-to-all-start.4) | async-done | bytes 524320 | tf_op jit(solution)/shard_map/all_to_all | solution.py:32
  150.6 1.7 %shard_map.146 = bf16[64,128]{1,0:T(8,128)(2,1)} custom-call(bf16[32,64,128]{2,1,0:T(8,128)(2,1)S(1)} %all-to-all-done.4.parts_ref, bf16[32,64,128]{2,1,0:T(8,128)(2,1)} %shard_map.142.after_ref), custom_call_target="tpu_custom_call" | custom-call | flops 1048576 | bytes 1064960 | tf_op jit(solution)/shard_map/pallas_call | solution.py:42
  (1 shorter events, 0.0 us)
Async XLA Ops:
  8.9 15.3 %all-to-all-start = ((bf16[16,64,128]{2,1,0:T(8,128)(2,1)}), bf16[16,64,128]{2,1,0:T(8,128)(2,1)S(1)}, u32[]{:S(2)}, u32[]{:S(2)}) async-start(bf16[16,64,128]{2,1,0:T(8,128)(2,1)} %get-tuple-element.9), calls=%async_computation | async-start | bytes 524288 | tf_op jit(solution)/shard_map/all_to_all | solution.py:32
  24.2 0.7 copy-start.4
  24.9 18.9 %copy-start.2 = (bf16[64,128]{1,0:T(8,128)(2,1)S(1)}, bf16[64,128]{1,0:T(8,128)(2,1)}, u32[]{:S(2)}) copy-start(bf16[64,128]{1,0:T(8,128)(2,1)} %tokens_ref.1) | copy-start | bytes 49156
  40.3 10.4 %all-to-all-start.3 = ((bf16[8,72,128]{2,1,0:T(8,128)(2,1)}), bf16[8,72,128]{2,1,0:T(8,128)(2,1)S(1)}, u32[]{:S(2)}, u32[]{:S(2)}) async-start(bf16[8,72,128]{2,1,0:T(8,128)(2,1)} %get-tuple-element.11), calls=%async_computation.3 | async-start | bytes 294912 | tf_op jit(solution)/shard_map/all_to_all | solution.py:32
  50.8 65.6 %all-to-all-start.2 = ((bf16[32,64,128]{2,1,0:T(8,128)(2,1)}), bf16[32,64,128]{2,1,0:T(8,128)(2,1)S(1)}, u32[]{:S(2)}, u32[]{:S(2)}) async-start(bf16[32,64,128]{2,1,0:T(8,128)(2,1)} %shard_map.142.after_ref), calls=%async_computation.2 | async-start | bytes 1048576 | tf_op jit(solution)/shard_map/all_to_all | solution.py:32
  60.4 55.9 %all-gather.2.cloned.1.call-start = ((), (), s32[]{:S(2)}) async-start(), calls=%async_computation.5 | async-start | bytes 1179648 | tf_op jit(solution)/shard_map/all_gather | solution.py:259
  116.3 1.2 copy-start
  117.5 6.5 %copy-start.1 = (bf16[512,1024]{1,0:T(8,128)(2,1)S(1)}, bf16[512,1024]{1,0:T(8,128)(2,1)}, u32[]{:S(2)}) copy-start(bf16[512,1024]{1,0:T(8,128)(2,1)} %all-gather.2.cloned.1.call-done) | copy-start | bytes 3145732
  117.5 20.4 %copy-start.3 = (f32[64,1,64,64]{3,2,1,0:T(8,128)S(1)}, f32[64,1,64,64]{3,2,1,0:T(8,128)}, u32[]{:S(2)}) copy-start(f32[64,1,64,64]{3,2,1,0:T(8,128)} %param.25) | copy-start | bytes 3145732
  117.6 20.4 %copy-start.5 = (f32[64,64]{1,0:T(8,128)S(1)}, f32[64,64]{1,0:T(8,128)}, u32[]{:S(2)}) copy-start(f32[64,64]{1,0:T(8,128)} %get-tuple-element.14) | copy-start | bytes 49156
  117.6 20.4 %copy-start.6 = (f32[64,64]{1,0:T(8,128)S(1)}, f32[64,64]{1,0:T(8,128)}, u32[]{:S(2)}) copy-start(f32[64,64]{1,0:T(8,128)} %get-tuple-element.15) | copy-start | bytes 49156
  118.1 5.9 %collective-permute-start = (bf16[264,256]{1,0:T(8,128)(2,1)S(1)}, bf16[264,256]{1,0:T(8,128)(2,1)S(1)}, u32[]{:S(2)}, u32[]{:S(2)}) collective-permute-start(bf16[264,256]{1,0:T(8,128)(2,1)S(1)} %get-tuple-element.13), channel_id=1, source_target_pairs={{0,32},{32,0},{1,33},{33,1},{2,34},{34,2},{3,35},{35,3},{4,36},{36... | collective-permute-start | bytes 405512 | tf_op jit(solution)/shard_map/ppermute | solution.py:319
  125.2 25.3 %all-to-all-start.4 = ((bf16[32,64,128]{2,1,0:T(8,128)(2,1)}), bf16[32,64,128]{2,1,0:T(8,128)(2,1)S(1)}, u32[]{:S(2)}, u32[]{:S(2)}) async-start(bf16[32,64,128]{2,1,0:T(8,128)(2,1)} %bitcast.11), calls=%async_computation.4 | async-start | bytes 1048576 | tf_op jit(solution)/shard_map/all_to_all | solution.py:32
Sparse Core Ops, SparseCore 0:
  63.8 52.4 all-gather.1

commit v4 on v3

--- a/solution.py
+++ b/solution.py
@@ -17,7 +17,8 @@
 TP = ("b3", "b2", "b1", "b0", "c")
 HALF = "xl"
 COLS = ("y", "xh")
-PLANES = ("b0", "c")
+NEAR = "b0"
+CORE = "c"
 FAR = ("b3", "b2", "b1")
 
 bf16, f32 = jnp.bfloat16, jnp.float32
@@ -59,14 +60,13 @@
         copy.wait()
 
 
-def pack_kernel(tokens_hbm, up_hbm, down_hbm, gain_hbm, out_ref, copies_ref, *scratch):
-    tokens_ref, up_ref, down_ref, gain_ref, sems = scratch
+def pack_kernel(decay_ref, up_hbm, down_hbm, gain_hbm, out_ref, *scratch):
+    up_ref, down_ref, gain_ref, sems = scratch
     fetch(
         (
             (up_hbm, up_ref),
             (down_hbm, down_ref),
             (gain_hbm, gain_ref),
-            (tokens_hbm, tokens_ref),
         ),
         sems,
     )
@@ -86,6 +86,9 @@
         out_ref[j, :units] = up[j * units : (j + 1) * units]
         out_ref[j, units : 2 * units] = down_ref[j * units : (j + 1) * units]
         out_ref[j, 2 * units :] = rows
+
+
+def copies_kernel(tokens_ref, copies_ref):
     tokens = tokens_ref[...]
     for k in range(copies_ref.shape[0]):
         copies_ref[k] = tokens
@@ -130,7 +133,7 @@
         turned = project(jnp.concatenate([ref[middle:], ref[:middle]]))
         return plain * cosine_ref[...] + turned * sine_ref[...]
 
-    for copy in copies[2:]:
+    for copy in copies[2:8]:
         copy.wait()
     queries = rotated(query_ref)
     keys = rotated(key_ref) * HEAD_DIM ** (-0.5)
@@ -139,6 +142,8 @@
     keys_ref[...] = keys
     values_ref[...] = values
     columns = queries.T
+    for copy in copies[8:]:
+        copy.wait()
     for b in range(state_ref.shape[0]):
         readout_ref[b : b + 1] = jnp.sum(state_ref[b] * columns[:, b : b + 1], axis=0, keepdims=True)
     matched = jnp.sum(keys * queries, axis=1, keepdims=True)
@@ -160,9 +165,15 @@
 
 
 def after_kernel(parts_ref, tokens_ref, out_ref):
-    block = (tokens_ref[...].astype(f32) + sum_of(parts_ref)).astype(bf16)
-    for p in range(out_ref.shape[0]):
-        out_ref[p] = block
+    out_ref[...] = (tokens_ref[...].astype(f32) + sum_of(parts_ref)).astype(bf16)
+
+
+def rows_kernel(near_ref, own_ref, other_ref, out_ref):
+    served = own_ref.shape[0]
+    for n in range(2):
+        block = jnp.where(near_ref[0] == n, own_ref[...], other_ref[...])
+        for p in range(out_ref.shape[0]):
+            out_ref[p, n * served : (n + 1) * served] = block
 
 
 def up_kernel(rows_ref, arrived_ref, weights_ref, own_ref, sent_ref):
@@ -213,8 +224,17 @@
         out_ref[j] = part[:, j * feats : (j + 1) * feats]
 
 
-def final_kernel(parts_ref, after_ref, out_ref):
-    out_ref[...] = (after_ref[0].astype(f32) + sum_of(parts_ref)).astype(out_ref.dtype)
+def halves_kernel(near_ref, parts_ref, own_ref, sent_ref):
+    served = own_ref.shape[0]
+    total = sum_of(parts_ref)
+    first, second = total[:served], total[served:]
+    own_ref[...] = jnp.where(near_ref[0] == 0, first, second)
+    sent_ref[...] = jnp.where(near_ref[0] == 0, second, first).astype(bf16)
+
+
+def final_kernel(own_ref, other_ref, after_ref, out_ref):
+    total = own_ref[...] + other_ref[...].astype(f32)
+    out_ref[...] = (after_ref[...].astype(f32) + total).astype(out_ref.dtype)
 
 
 def layer(
@@ -234,30 +254,35 @@
 ):
     like = jax.ShapeDtypeStruct
     served, feats = tokens.shape
-    kv, cols, planes, far = size_of(KV), size_of(COLS), size_of(PLANES), size_of(FAR)
+    kv, cols, far = size_of(KV), size_of(COLS), size_of(FAR)
+    cores = lax.axis_size(CORE)
     units = up_weight.shape[1] // cols
-    count = planes * served
-    sent, copies = call(
+    count = 2 * cores * served
+    near = lax.axis_index(NEAR)
+    turn = [(0, 1), (1, 0)]
+    head = lax.axis_index(KV).astype(f32)
+    decay = 1.0 - 2.0 ** (-5.0 - 5.0 * head / (HEADS - 1))
+    sent = call(
         pack_kernel,
-        (like((cols, 2 * units + 8, feats), bf16), like((kv, served, feats), bf16)),
-        tokens,
+        like((cols, 2 * units + 8, feats), bf16),
         up_weight,
         down_weight,
         channel_gain.reshape(1, feats),
-        hbm=(0, 1, 2, 3),
+        scalars=(decay,),
+        hbm=(0, 1, 2),
         limit=63 << 20,
         scratch=(
-            pltpu.VMEM(tokens.shape, bf16),
             pltpu.VMEM(up_weight.shape, bf16),
             pltpu.VMEM(down_weight.shape, bf16),
             pltpu.VMEM((1, feats), f32),
-            pltpu.SemaphoreType.DMA((4,)),
+            pltpu.SemaphoreType.DMA((3,)),
         ),
     )
     arrived = swap(sent, COLS)
     mine = call(unpack_kernel, like((2 * units, cols * feats), bf16), arrived)
     weights = lax.all_gather(mine, FAR, axis=0, tiled=True)
 
+    copies = call(copies_kernel, like((kv, served, feats), bf16), tokens)
     blocks = swap(copies, KV)
     middle = HEAD_DIM // 2
     inverse = THETA ** (-jnp.arange(middle, dtype=f32) * 2.0 / HEAD_DIM)
@@ -265,8 +290,6 @@
     cosine, sine = jnp.cos(angles), jnp.sin(angles)
     both_cosine = jnp.concatenate([cosine, cosine], axis=1)
     both_sine = jnp.concatenate([-sine, sine], axis=1)
-    head = lax.axis_index(KV).astype(f32)
-    decay = 1.0 - 2.0 ** (-5.0 - 5.0 * head / (HEADS - 1))
     state = memory_state[:, 0]
     operands = (
         blocks,
@@ -301,9 +324,17 @@
         flops=2 * served * D * 6 * HEAD_DIM,
     )
     shares = swap(shares, KV)
-    after = call(after_kernel, like((cols * planes, served, feats), bf16), shares, tokens)
-
-    rows = swap(after, COLS + PLANES).reshape(cols, count, feats)
+    after = call(after_kernel, like((served, feats), bf16), shares, tokens)
+
+    passed = lax.ppermute(after, NEAR, turn)
+    copies = call(
+        rows_kernel,
+        like((cols * cores, 2 * served, feats), bf16),
+        after,
+        passed,
+        scalars=(near,),
+    )
+    rows = swap(copies, COLS + (CORE,)).reshape(cols, count, feats)
     weights = weights.reshape(far, 2, units, cols * feats)
     own, given = call(
         up_kernel,
@@ -316,7 +347,7 @@
         weights,
         flops=2 * count * cols * feats * far * units,
     )
-    other = lax.ppermute(given, HALF, [(0, 1), (1, 0)])
+    other = lax.ppermute(given, HALF, turn)
     lowered = call(
         down_kernel,
         like((cols, count, feats), bf16),
@@ -326,8 +357,15 @@
         flops=2 * count * cols * feats * far * units,
     )
 
-    lowered = swap(lowered.reshape(cols * planes, served, feats), COLS + PLANES)
-    mixed = call(final_kernel, like((served, feats), bf16), lowered, after)
+    lowered = swap(lowered.reshape(cols * cores, 2 * served, feats), COLS + (CORE,))
+    kept, back = call(
+        halves_kernel,
+        (like((served, feats), f32), like((served, feats), bf16)),
+        lowered,
+        scalars=(near,),
+    )
+    returned = lax.ppermute(back, NEAR, turn)
+    mixed = call(final_kernel, like((served, feats), bf16), kept, returned, after)
     new_state = decay * state + keys_new[:, :, None] * values_new[:, None, :]
     return (mixed, new_state[:, None])
 

time: 160 us -> 121 us (0.76)
  waiting for transfers between devices: 81.9 us -> 11.3 us
  blocking collectives: 11 us -> 66.4 us
  starting transfers between devices: 35.6 us -> 12.7 us
  Pallas kernels: 11.2 us -> 8.86 us
    all_to_all x1 -> x4, blocking collectives: 11 us -> 66.4 us  [swap(): return lax.all_to_all(blocks, axes, split_axis=0, concat_axis=0, tiled=True)]
    all_gather x1, waiting for transfers between devices: 55.2 us -> 0.01 us  [layer(): weights = lax.all_gather(mine, FAR, axis=0, tiled=True)]
    all_to_all x4 -> x1, starting transfers between devices: 33.3 us -> 3.53 us  [swap(): return lax.all_to_all(blocks, axes, split_axis=0, concat_axis=0, tiled=True)]
    all_to_all x4 -> x1, waiting for transfers between devices: 23.1 us -> 5.92 us  [swap(): return lax.all_to_all(blocks, axes, split_axis=0, concat_axis=0, tiled=True)]
    ppermute x1 -> x3, starting transfers between devices: 2.27 us -> 9.12 us  [the longest x1 3.54 us: layer(): passed = lax.ppermute(after, NEAR, turn)]
    pallas_call x7 -> x10, Pallas kernels: 11.2 us -> 8.86 us  [call(): pl.pallas_call(kernel, out_shape=out, in_specs=[smem] * len(scalars) + [f...]
    ppermute x1 -> x3, waiting for transfers between devices: 3.61 us -> 5.33 us  [the longest x1 3.59 us: layer(): other = lax.ppermute(given, HALF, turn)]
  transfers between devices with their start and end apart: 6 -> 5, of which waited for: 5 -> 3; matrix products, arithmetic and copies ran while one was open for 2% -> 3% of each run, Pallas kernels for 1% -> 4%
where the time goes in v4:
time: 121 us; the launch traced here: 119 us
  blocking collectives  66.4 us (55%)
  between operations  14.2 us (12%)
  starting transfers between devices  12.7 us (10%)
  waiting for transfers between devices  11.3 us (9%)
  Pallas kernels  8.86 us (7%)
  other arithmetic  3.27 us (3%)
  local copies, waits for them, and re-layouts  2.66 us (2%)
    all_to_all x4, blocking collectives, swap(): return lax.all_to_all(blocks, axes, split_axis=0, concat_axis=0, tiled=True)  66.4 us
    pallas_call x10, Pallas kernels, call(): pl.pallas_call(kernel, out_shape=out, in_specs=[smem] * len(scalars) + [f...  8.86 us
    all_to_all x1, waiting for transfers between devices, swap(): return lax.all_to_all(blocks, axes, split_axis=0, concat_axis=0, tiled=True)  5.92 us
    ppermute x1, waiting for transfers between devices, layer(): other = lax.ppermute(given, HALF, turn)  3.59 us
    ppermute x1, starting transfers between devices, layer(): passed = lax.ppermute(after, NEAR, turn)  3.54 us
    all_to_all x1, starting transfers between devices, swap(): return lax.all_to_all(blocks, axes, split_axis=0, concat_axis=0, tiled=True)  3.53 us
    ppermute x1, starting transfers between devices, layer(): returned = lax.ppermute(back, NEAR, turn)  3.29 us
    unnamed x16, local copies, waits for them, and re-layouts  2.66 us
  transfers between devices with their start and end apart: 5, of which 3 were waited for; matrix products, arithmetic and copies ran while one was open for 3% of the time, Pallas kernels for 4%

profile of v4, /device:TPU:1, one launch (start us, length us, event | category | flops | bytes accessed | tf_op | source)
XLA Modules:
  0.0 119.4 jit_solution(18377343954003932934)
XLA Ops:
  7.2 0.0 all-gather.2.cloned.1.call-start
  7.3 1.7 %shard_map.144 = bf16[8,72,128]{2,1,0:T(8,128)(2,1)} custom-call(f32[1]{0:T(128)} %bitcast.1.decay_ref, bf16[128,256]{1,0:T(8,128)(2,1)} %up_hbm.1, bf16[256,128]{1,0:T(8,128)(2,1)} %down_hbm.1, f32[1,128]{1,0:T(1,128)} %bitcast.23), custom_call_target="tpu_custom_call" | custom-call | flops 1048576 | bytes 279040 | tf_op jit(solution)/shard_map/pallas_call | solution.py:43
  8.9 14.6 %all_to_all.25.arrived_ref = bf16[8,72,128]{2,1,0:T(8,128)(2,1)S(1)} all-to-all(bf16[8,72,128]{2,1,0:T(8,128)(2,1)} %shard_map.144), channel_id=1, replica_groups=mesh['y'=4,'xh'=2,'xl'=2,'b3'=2,'b2'=2,'b1'=2,'b0'=2,'c'=2] {'y','xh'}, dimensions={0} | all-to-all | bytes 294912 | tf_op jit(solution)/shard_map/all_to_all | solution.py:33
  23.5 0.7 shard_map.145
  24.2 0.0 all-gather.2.cloned.1.call-update
  24.2 0.0 copy-start.2
  24.3 0.7 copy-done.2
  25.0 0.8 shard_map.140
  25.7 3.5 %all-to-all-start = ((bf16[16,64,128]{2,1,0:T(8,128)(2,1)}), bf16[16,64,128]{2,1,0:T(8,128)(2,1)S(1)}, u32[]{:S(2)}, u32[]{:S(2)}) async-start(bf16[16,64,128]{2,1,0:T(8,128)(2,1)} %shard_map.140), calls=%async_computation | async-start | bytes 524288 | tf_op jit(solution)/shard_map/all_to_all | solution.py:33
  29.3 0.7 convert_element_type.7
  29.9 0.2 fusion
  30.1 0.7 pad_maximum_fusion
  30.9 5.9 %all-to-all-done.refs_0_ = bf16[16,64,128]{2,1,0:T(8,128)(2,1)S(1)} async-done(((bf16[16,64,128]{2,1,0:T(8,128)(2,1)}), bf16[16,64,128]{2,1,0:T(8,128)(2,1)S(1)}, u32[]{:S(2)}, u32[]{:S(2)}) %all-to-all-start) | async-done | bytes 262176 | tf_op jit(solution)/shard_map/all_to_all | solution.py:33
  36.8 0.0 copy-start.5
  36.8 0.7 copy-done.5
  37.5 0.0 copy-start.3
  37.5 4.0 %shard_map.141 = (bf16[16,64,128]{2,1,0:T(8,128)(2,1)}, f32[64,64]{1,0:T(8,128)}, f32[64,64]{1,0:T(8,128)}) custom-call(f32[1]{0:T(128)} %bitcast.1.decay_ref, bf16[16,64,128]{2,1,0:T(8,128)(2,1)} %copy-done.5, f32[1,2048]{1,0:T(1,128)} %bitcast.22, bf16[64,2048]{1,0:T(8,128)(2,1)} %bitcast.18, bf16[64,2048]{1,0:T(8,128)(2,1)} %bitcast.19, ...), custom_call_target="tpu_custom_call" | custom-call | flops 100663296 | bytes 2957568 | tf_op jit(solution)/shard_map/pallas_call | solution.py:43
  41.5 11.0 %all_to_all.26.parts_ref = bf16[16,64,128]{2,1,0:T(8,128)(2,1)S(1)} all-to-all(bf16[16,64,128]{2,1,0:T(8,128)(2,1)} %get-tuple-element.9), channel_id=1, replica_groups=mesh['y'=4,'xh'=2,'xl'=2,'b3'=2,'b2'=2,'b1'=2,'b0'=2,'c'=2] {'y','xh','xl'}, dimensions={0} | all-to-all | bytes 524288 | tf_op jit(solution)/shard_map/all_to_all | solution.py:33
  52.5 0.0 copy-done.3
  52.5 3.5 %collective-permute-start = (bf16[64,128]{1,0:T(8,128)(2,1)S(1)}, bf16[64,128]{1,0:T(8,128)(2,1)S(1)}, u32[]{:S(2)}, u32[]{:S(2)}) collective-permute-start(bf16[64,128]{1,0:T(8,128)(2,1)S(1)} %shard_map.142.own_ref.after_ref), channel_id=1, source_target_pairs={{0,2},{2,0},{1,3},{3,1},{4,6},{6,4},{5,7},{7,5},{8,10},{10,8},{9,1... | collective-permute-start | bytes 49160 | tf_op jit(solution)/shard_map/ppermute | solution.py:329
  56.1 1.7 %collective-permute-done.other_ref = bf16[64,128]{1,0:T(8,128)(2,1)S(1)} collective-permute-done((bf16[64,128]{1,0:T(8,128)(2,1)S(1)}, bf16[64,128]{1,0:T(8,128)(2,1)S(1)}, u32[]{:S(2)}, u32[]{:S(2)}) %collective-permute-start) | collective-permute-done | bytes 16416 | tf_op jit(solution)/shard_map/ppermute | solution.py:329
  57.8 0.1 shard_map.143
  57.9 20.7 %all_to_all.27 = bf16[16,128,128]{2,1,0:T(8,128)(2,1)S(1)} all-to-all(bf16[16,128,128]{2,1,0:T(8,128)(2,1)S(1)} %shard_map.143), channel_id=1, replica_groups=mesh['y'=4,'xh'=2,'xl'=2,'b3'=2,'b2'=2,'b1'=2,'b0'=2,'c'=2] {'y','xh','c'}, dimensions={0} | all-to-all | bytes 1048576 | tf_op jit(solution)/shard_map/all_to_all | solution.py:33
  78.6 0.0 all-gather.2.cloned.1.call-done
  78.6 0.0 copy-start
  78.6 1.2 %copy-done = bf16[512,1024]{1,0:T(8,128)(2,1)S(1)} copy-done((bf16[512,1024]{1,0:T(8,128)(2,1)S(1)}, bf16[512,1024]{1,0:T(8,128)(2,1)}, u32[]{:S(2)}) %copy-start) | copy-done | bytes 1048600
  79.9 0.0 copy-start.1
  79.9 0.6 shard_map.146
  80.5 0.0 copy-start.4
  80.5 0.0 copy-start.6
  80.5 0.0 copy-start.7
  80.5 2.3 %collective-permute-start.1 = (bf16[264,256]{1,0:T(8,128)(2,1)S(1)}, bf16[264,256]{1,0:T(8,128)(2,1)S(1)}, u32[]{:S(2)}, u32[]{:S(2)}) collective-permute-start(bf16[264,256]{1,0:T(8,128)(2,1)S(1)} %get-tuple-element.11), channel_id=1, source_target_pairs={{0,32},{32,0},{1,33},{33,1},{2,34},{34,2},{3,35},{35,3},{4,36},{36... | collective-permute-start | bytes 405512 | tf_op jit(solution)/shard_map/ppermute | solution.py:350
  82.8 3.6 %collective-permute-done.1.other_ref = bf16[264,256]{1,0:T(8,128)(2,1)S(1)} collective-permute-done((bf16[264,256]{1,0:T(8,128)(2,1)S(1)}, bf16[264,256]{1,0:T(8,128)(2,1)S(1)}, u32[]{:S(2)}, u32[]{:S(2)}) %collective-permute-start.1) | collective-permute-done | bytes 135200 | tf_op jit(solution)/shard_map/ppermute | solution.py:350
  86.4 0.0 copy-done.1
  86.4 0.4 shard_map.147
  86.8 20.1 %all_to_all.28.parts_ref = bf16[16,128,128]{2,1,0:T(8,128)(2,1)S(1)} all-to-all(bf16[16,128,128]{2,1,0:T(8,128)(2,1)S(1)} %bitcast.16), channel_id=1, replica_groups=mesh['y'=4,'xh'=2,'xl'=2,'b3'=2,'b2'=2,'b1'=2,'b0'=2,'c'=2] {'y','xh','c'}, dimensions={0} | all-to-all | bytes 1048576 | tf_op jit(solution)/shard_map/all_to_all | solution.py:33
  106.8 0.1 shard_map.148
  106.9 3.3 %collective-permute-start.2 = (bf16[64,128]{1,0:T(8,128)(2,1)S(1)}, bf16[64,128]{1,0:T(8,128)(2,1)S(1)}, u32[]{:S(2)}, u32[]{:S(2)}) collective-permute-start(bf16[64,128]{1,0:T(8,128)(2,1)S(1)} %get-tuple-element.13), channel_id=1, source_target_pairs={{0,2},{2,0},{1,3},{3,1},{4,6},{6,4},{5,7},{7,5},{8,10},{10,8},{9,1... | collective-permute-start | bytes 49160 | tf_op jit(solution)/shard_map/ppermute | solution.py:367
  110.2 0.0 copy-done.4
  110.2 0.0 copy-done.6
  110.2 0.0 copy-done.7
  110.2 1.7 %multiply_add_fusion = f32[64,1,64,64]{3,2,1,0:T(8,128)} fusion(f32[64,1,64,64]{3,2,1,0:T(8,128)S(1)} %copy-done.4, f32[64,64]{1,0:T(8,128)S(1)} %copy-done.7, f32[64,64]{1,0:T(8,128)S(1)} %copy-done.6, f32[]{:T(128)} %sub.7), kind=kLoop, calls=%fused_computation | loop fusion | flops 786432 | bytes 2129924 | tf_op jit(solution)/shard_map/add | solution.py:369
  111.9 0.0 collective-permute-done.2.other_ref
  111.9 0.6 shard_map.149
  (2 shorter events, 0.1 us)
Async XLA Ops:
  7.2 71.5 %all-gather.2.cloned.1.call-start = ((), (), s32[]{:S(2)}) async-start(), calls=%async_computation.5 | async-start | bytes 1179648 | tf_op jit(solution)/shard_map/all_gather | solution.py:283
  24.2 0.7 copy-start.2
  25.7 11.0 %all-to-all-start = ((bf16[16,64,128]{2,1,0:T(8,128)(2,1)}), bf16[16,64,128]{2,1,0:T(8,128)(2,1)S(1)}, u32[]{:S(2)}, u32[]{:S(2)}) async-start(bf16[16,64,128]{2,1,0:T(8,128)(2,1)} %shard_map.140), calls=%async_computation | async-start | bytes 524288 | tf_op jit(solution)/shard_map/all_to_all | solution.py:33
  36.8 0.7 copy-start.5
  37.5 15.0 %copy-start.3 = (bf16[64,128]{1,0:T(8,128)(2,1)S(1)}, bf16[64,128]{1,0:T(8,128)(2,1)}, u32[]{:S(2)}) copy-start(bf16[64,128]{1,0:T(8,128)(2,1)} %tokens_ref.3) | copy-start | bytes 49156
  52.5 5.3 %collective-permute-start = (bf16[64,128]{1,0:T(8,128)(2,1)S(1)}, bf16[64,128]{1,0:T(8,128)(2,1)S(1)}, u32[]{:S(2)}, u32[]{:S(2)}) collective-permute-start(bf16[64,128]{1,0:T(8,128)(2,1)S(1)} %shard_map.142.own_ref.after_ref), channel_id=1, source_target_pairs={{0,2},{2,0},{1,3},{3,1},{4,6},{6,4},{5,7},{7,5},{8,10},{10,8},{9,1... | collective-permute-start | bytes 49160 | tf_op jit(solution)/shard_map/ppermute | solution.py:329
  78.6 1.2 %copy-start = (bf16[512,1024]{1,0:T(8,128)(2,1)S(1)}, bf16[512,1024]{1,0:T(8,128)(2,1)}, u32[]{:S(2)}) copy-start(bf16[512,1024]{1,0:T(8,128)(2,1)} %all-gather.2.cloned.1.call-done) | copy-start | bytes 3145732
  79.9 6.5 %copy-start.1 = (bf16[512,1024]{1,0:T(8,128)(2,1)S(1)}, bf16[512,1024]{1,0:T(8,128)(2,1)}, u32[]{:S(2)}) copy-start(bf16[512,1024]{1,0:T(8,128)(2,1)} %all-gather.2.cloned.1.call-done) | copy-start | bytes 3145732
  80.5 29.8 %copy-start.4 = (f32[64,1,64,64]{3,2,1,0:T(8,128)S(1)}, f32[64,1,64,64]{3,2,1,0:T(8,128)}, u32[]{:S(2)}) copy-start(f32[64,1,64,64]{3,2,1,0:T(8,128)} %param.25) | copy-start | bytes 3145732
  80.5 29.8 %copy-start.6 = (f32[64,64]{1,0:T(8,128)S(1)}, f32[64,64]{1,0:T(8,128)}, u32[]{:S(2)}) copy-start(f32[64,64]{1,0:T(8,128)} %get-tuple-element.14) | copy-start | bytes 49156
  80.5 29.8 %copy-start.7 = (f32[64,64]{1,0:T(8,128)S(1)}, f32[64,64]{1,0:T(8,128)}, u32[]{:S(2)}) copy-start(f32[64,64]{1,0:T(8,128)} %get-tuple-element.15) | copy-start | bytes 49156
  80.5 5.9 %collective-permute-start.1 = (bf16[264,256]{1,0:T(8,128)(2,1)S(1)}, bf16[264,256]{1,0:T(8,128)(2,1)S(1)}, u32[]{:S(2)}, u32[]{:S(2)}) collective-permute-start(bf16[264,256]{1,0:T(8,128)(2,1)S(1)} %get-tuple-element.11), channel_id=1, source_target_pairs={{0,32},{32,0},{1,33},{33,1},{2,34},{34,2},{3,35},{35,3},{4,36},{36... | collective-permute-start | bytes 405512 | tf_op jit(solution)/shard_map/ppermute | solution.py:350
  106.9 5.0 %collective-permute-start.2 = (bf16[64,128]{1,0:T(8,128)(2,1)S(1)}, bf16[64,128]{1,0:T(8,128)(2,1)S(1)}, u32[]{:S(2)}, u32[]{:S(2)}) collective-permute-start(bf16[64,128]{1,0:T(8,128)(2,1)S(1)} %get-tuple-element.13), channel_id=1, source_target_pairs={{0,2},{2,0},{1,3},{3,1},{4,6},{6,4},{5,7},{7,5},{8,10},{10,8},{9,1... | collective-permute-start | bytes 49160 | tf_op jit(solution)/shard_map/ppermute | solution.py:367
Sparse Core Ops, SparseCore 0:
  24.4 51.2 all-gather.1

commit v5 on v3

--- a/solution.py
+++ b/solution.py
@@ -15,8 +15,8 @@
 
 KV = ("y", "xh", "xl")
 TP = ("b3", "b2", "b1", "b0", "c")
-HALF = "xl"
-COLS = ("y", "xh")
+HALF = "xh"
+COLS = ("y", "xl")
 PLANES = ("b0", "c")
 FAR = ("b3", "b2", "b1")
 
@@ -59,14 +59,13 @@
         copy.wait()
 
 
-def pack_kernel(tokens_hbm, up_hbm, down_hbm, gain_hbm, out_ref, copies_ref, *scratch):
-    tokens_ref, up_ref, down_ref, gain_ref, sems = scratch
+def pack_kernel(decay_ref, up_hbm, down_hbm, gain_hbm, out_ref, *scratch):
+    up_ref, down_ref, gain_ref, sems = scratch
     fetch(
         (
             (up_hbm, up_ref),
             (down_hbm, down_ref),
             (gain_hbm, gain_ref),
-            (tokens_hbm, tokens_ref),
         ),
         sems,
     )
@@ -86,6 +85,9 @@
         out_ref[j, :units] = up[j * units : (j + 1) * units]
         out_ref[j, units : 2 * units] = down_ref[j * units : (j + 1) * units]
         out_ref[j, 2 * units :] = rows
+
+
+def copies_kernel(tokens_ref, copies_ref):
     tokens = tokens_ref[...]
     for k in range(copies_ref.shape[0]):
         copies_ref[k] = tokens
@@ -130,7 +132,7 @@
         turned = project(jnp.concatenate([ref[middle:], ref[:middle]]))
         return plain * cosine_ref[...] + turned * sine_ref[...]
 
-    for copy in copies[2:]:
+    for copy in copies[2:8]:
         copy.wait()
     queries = rotated(query_ref)
     keys = rotated(key_ref) * HEAD_DIM ** (-0.5)
@@ -139,6 +141,8 @@
     keys_ref[...] = keys
     values_ref[...] = values
     columns = queries.T
+    for copy in copies[8:]:
+        copy.wait()
     for b in range(state_ref.shape[0]):
         readout_ref[b : b + 1] = jnp.sum(state_ref[b] * columns[:, b : b + 1], axis=0, keepdims=True)
     matched = jnp.sum(keys * queries, axis=1, keepdims=True)
@@ -159,8 +163,9 @@
     return total
 
 
-def after_kernel(parts_ref, tokens_ref, out_ref):
+def after_kernel(parts_ref, tokens_ref, out_ref, one_ref):
     block = (tokens_ref[...].astype(f32) + sum_of(parts_ref)).astype(bf16)
+    one_ref[...] = block
     for p in range(out_ref.shape[0]):
         out_ref[p] = block
 
@@ -214,7 +219,7 @@
 
 
 def final_kernel(parts_ref, after_ref, out_ref):
-    out_ref[...] = (after_ref[0].astype(f32) + sum_of(parts_ref)).astype(out_ref.dtype)
+    out_ref[...] = (after_ref[...].astype(f32) + sum_of(parts_ref)).astype(out_ref.dtype)
 
 
 def layer(
@@ -237,27 +242,29 @@
     kv, cols, planes, far = size_of(KV), size_of(COLS), size_of(PLANES), size_of(FAR)
     units = up_weight.shape[1] // cols
     count = planes * served
-    sent, copies = call(
+    head = lax.axis_index(KV).astype(f32)
+    decay = 1.0 - 2.0 ** (-5.0 - 5.0 * head / (HEADS - 1))
+    sent = call(
         pack_kernel,
-        (like((cols, 2 * units + 8, feats), bf16), like((kv, served, feats), bf16)),
-        tokens,
+        like((cols, 2 * units + 8, feats), bf16),
         up_weight,
         down_weight,
         channel_gain.reshape(1, feats),
-        hbm=(0, 1, 2, 3),
+        scalars=(decay,),
+        hbm=(0, 1, 2),
         limit=63 << 20,
         scratch=(
-            pltpu.VMEM(tokens.shape, bf16),
             pltpu.VMEM(up_weight.shape, bf16),
             pltpu.VMEM(down_weight.shape, bf16),
             pltpu.VMEM((1, feats), f32),
-            pltpu.SemaphoreType.DMA((4,)),
+            pltpu.SemaphoreType.DMA((3,)),
         ),
     )
     arrived = swap(sent, COLS)
     mine = call(unpack_kernel, like((2 * units, cols * feats), bf16), arrived)
     weights = lax.all_gather(mine, FAR, axis=0, tiled=True)
 
+    copies = call(copies_kernel, like((kv, served, feats), bf16), tokens)
     blocks = swap(copies, KV)
     middle = HEAD_DIM // 2
     inverse = THETA ** (-jnp.arange(middle, dtype=f32) * 2.0 / HEAD_DIM)
@@ -265,8 +272,6 @@
     cosine, sine = jnp.cos(angles), jnp.sin(angles)
     both_cosine = jnp.concatenate([cosine, cosine], axis=1)
     both_sine = jnp.concatenate([-sine, sine], axis=1)
-    head = lax.axis_index(KV).astype(f32)
-    decay = 1.0 - 2.0 ** (-5.0 - 5.0 * head / (HEADS - 1))
     state = memory_state[:, 0]
     operands = (
         blocks,
@@ -301,9 +306,14 @@
         flops=2 * served * D * 6 * HEAD_DIM,
     )
     shares = swap(shares, KV)
-    after = call(after_kernel, like((cols * planes, served, feats), bf16), shares, tokens)
-
-    rows = swap(after, COLS + PLANES).reshape(cols, count, feats)
+    copies, after = call(
+        after_kernel,
+        (like((cols * planes, served, feats), bf16), like((served, feats), bf16)),
+        shares,
+        tokens,
+    )
+
+    rows = swap(copies, COLS + PLANES).reshape(cols, count, feats)
     weights = weights.reshape(far, 2, units, cols * feats)
     own, given = call(
         up_kernel,

time: 160 us -> 153 us (0.956)
  blocking collectives: 11 us -> 0 us
  starting transfers between devices: 35.6 us -> 38.9 us
    all_to_all x1 -> x0, blocking collectives: 11 us -> none  [swap(): return lax.all_to_all(blocks, axes, split_axis=0, concat_axis=0, tiled=True)]
    all_to_all x4 -> x5, waiting for transfers between devices: 23.1 us -> 25.9 us  [swap(): return lax.all_to_all(blocks, axes, split_axis=0, concat_axis=0, tiled=True)]
    all_to_all x4 -> x5, starting transfers between devices: 33.3 us -> 35.3 us  [swap(): return lax.all_to_all(blocks, axes, split_axis=0, concat_axis=0, tiled=True)]
    all_gather x1, waiting for transfers between devices: 55.2 us -> 53.1 us  [layer(): weights = lax.all_gather(mine, FAR, axis=0, tiled=True)]
    pallas_call x7 -> x8, Pallas kernels: 11.2 us -> 10.4 us  [call(): pl.pallas_call(kernel, out_shape=out, in_specs=[smem] * len(scalars) + [f...]
  transfers between devices with their start and end apart: 6 -> 7, of which waited for: 5 -> 6; matrix products, arithmetic and copies ran while one was open for 2% -> 2% of each run, Pallas kernels for 1% -> 2%
where the time goes in v5:
time: 153 us; the launch traced here: 152 us
  waiting for transfers between devices  83 us (54%)
  starting transfers between devices  38.9 us (25%)
  between operations  14.2 us (9%)
  Pallas kernels  10.4 us (7%)
  other arithmetic  3.26 us (2%)
  local copies, waits for them, and re-layouts  2.66 us (2%)
    all_gather x1, waiting for transfers between devices, layer(): weights = lax.all_gather(mine, FAR, axis=0, tiled=True)  53.1 us
    all_to_all x5, starting transfers between devices, swap(): return lax.all_to_all(blocks, axes, split_axis=0, concat_axis=0, tiled=True)  35.3 us
    all_to_all x5, waiting for transfers between devices, swap(): return lax.all_to_all(blocks, axes, split_axis=0, concat_axis=0, tiled=True)  25.9 us
    pallas_call x8, Pallas kernels, call(): pl.pallas_call(kernel, out_shape=out, in_specs=[smem] * len(scalars) + [f...  10.4 us
    ppermute x1, waiting for transfers between devices, layer(): other = lax.ppermute(given, HALF, [(0, 1), (1, 0)])  3.92 us
    ppermute x1, starting transfers between devices, layer(): other = lax.ppermute(given, HALF, [(0, 1), (1, 0)])  3.47 us
  transfers between devices with their start and end apart: 7, of which 6 were waited for; matrix products, arithmetic and copies ran while one was open for 2% of the time, Pallas kernels for 2%

profile of v5, /device:TPU:1, one launch (start us, length us, event | category | flops | bytes accessed | tf_op | source)
XLA Modules:
  0.0 152.4 jit_solution(2134388346899446437)
XLA Ops:
  7.2 0.0 copy-start.2
  7.2 0.7 copy-done.2
  7.9 0.8 shard_map.140
  8.6 7.6 %all-to-all-start = ((bf16[16,64,128]{2,1,0:T(8,128)(2,1)}), bf16[16,64,128]{2,1,0:T(8,128)(2,1)S(1)}, u32[]{:S(2)}, u32[]{:S(2)}) async-start(bf16[16,64,128]{2,1,0:T(8,128)(2,1)} %shard_map.140), calls=%async_computation | async-start | bytes 524288 | tf_op jit(solution)/shard_map/all_to_all | solution.py:32
  16.2 0.7 convert_element_type.7
  17.0 0.2 fusion
  17.2 0.7 pad_maximum_fusion
  17.9 6.0 %all-to-all-done.refs_0_ = bf16[16,64,128]{2,1,0:T(8,128)(2,1)S(1)} async-done(((bf16[16,64,128]{2,1,0:T(8,128)(2,1)}), bf16[16,64,128]{2,1,0:T(8,128)(2,1)S(1)}, u32[]{:S(2)}, u32[]{:S(2)}) %all-to-all-start) | async-done | bytes 262176 | tf_op jit(solution)/shard_map/all_to_all | solution.py:32
  23.9 0.0 copy-start.5
  23.9 0.7 copy-done.5
  24.6 0.0 copy-start.3
  24.6 4.0 %shard_map.141 = (bf16[16,64,128]{2,1,0:T(8,128)(2,1)}, f32[64,64]{1,0:T(8,128)}, f32[64,64]{1,0:T(8,128)}) custom-call(f32[1]{0:T(128)} %bitcast.decay_ref, bf16[16,64,128]{2,1,0:T(8,128)(2,1)} %copy-done.5, f32[1,2048]{1,0:T(1,128)} %bitcast.20, bf16[64,2048]{1,0:T(8,128)(2,1)} %bitcast.16, bf16[64,2048]{1,0:T(8,128)(2,1)} %bitcast.17, ...), custom_call_target="tpu_custom_call" | custom-call | flops 100663296 | bytes 2957568 | tf_op jit(solution)/shard_map/pallas_call | solution.py:42
  28.6 3.5 %all-to-all-start.1 = ((bf16[16,64,128]{2,1,0:T(8,128)(2,1)}), bf16[16,64,128]{2,1,0:T(8,128)(2,1)S(1)}, u32[]{:S(2)}, u32[]{:S(2)}) async-start(bf16[16,64,128]{2,1,0:T(8,128)(2,1)} %get-tuple-element.9), calls=%async_computation.1 | async-start | bytes 524288 | tf_op jit(solution)/shard_map/all_to_all | solution.py:32
  32.1 1.7 %shard_map.143 = bf16[8,72,128]{2,1,0:T(8,128)(2,1)} custom-call(f32[1]{0:T(128)} %bitcast.decay_ref, bf16[128,256]{1,0:T(8,128)(2,1)} %up_hbm.1, bf16[256,128]{1,0:T(8,128)(2,1)} %down_hbm.1, f32[1,128]{1,0:T(1,128)} %bitcast.22), custom_call_target="tpu_custom_call" | custom-call | flops 1048576 | bytes 279040 | tf_op jit(solution)/shard_map/pallas_call | solution.py:42
  33.8 5.8 %all-to-all-done.1.parts_ref = bf16[16,64,128]{2,1,0:T(8,128)(2,1)S(1)} async-done(((bf16[16,64,128]{2,1,0:T(8,128)(2,1)}), bf16[16,64,128]{2,1,0:T(8,128)(2,1)S(1)}, u32[]{:S(2)}, u32[]{:S(2)}) %all-to-all-start.1) | async-done | bytes 262176 | tf_op jit(solution)/shard_map/all_to_all | solution.py:32
  39.7 3.4 %all-to-all-start.3 = ((bf16[8,72,128]{2,1,0:T(8,128)(2,1)}), bf16[8,72,128]{2,1,0:T(8,128)(2,1)S(1)}, u32[]{:S(2)}, u32[]{:S(2)}) async-start(bf16[8,72,128]{2,1,0:T(8,128)(2,1)} %shard_map.143), calls=%async_computation.3 | async-start | bytes 294912 | tf_op jit(solution)/shard_map/all_to_all | solution.py:32
  43.0 0.0 copy-done.3
  43.0 0.9 shard_map.142
  43.9 4.6 %all-to-all-done.3.arrived_ref = bf16[8,72,128]{2,1,0:T(8,128)(2,1)S(1)} async-done(((bf16[8,72,128]{2,1,0:T(8,128)(2,1)}), bf16[8,72,128]{2,1,0:T(8,128)(2,1)S(1)}, u32[]{:S(2)}, u32[]{:S(2)}) %all-to-all-start.3) | async-done | bytes 147488 | tf_op jit(solution)/shard_map/all_to_all | solution.py:32
  48.6 9.6 %all-to-all-start.2 = ((bf16[32,64,128]{2,1,0:T(8,128)(2,1)}), bf16[32,64,128]{2,1,0:T(8,128)(2,1)S(1)}, u32[]{:S(2)}, u32[]{:S(2)}) async-start(bf16[32,64,128]{2,1,0:T(8,128)(2,1)} %get-tuple-element.10), calls=%async_computation.2 | async-start | bytes 1048576 | tf_op jit(solution)/shard_map/all_to_all | solution.py:32
  58.2 0.0 all-gather.2.cloned.1.call-start
  58.2 0.7 shard_map.144
  58.9 0.0 all-gather.2.cloned.1.call-update
  58.9 53.1 %all-gather.2.cloned.1.call-done = bf16[512,1024]{1,0:T(8,128)(2,1)} async-done(((bf16[64,1024]{1,0:T(8,128)(2,1)}), bf16[512,1024]{1,0:T(8,128)(2,1)}) %all-gather.2.cloned.1.call-update) | async-done | bytes 1048592 | tf_op jit(solution)/shard_map/all_gather | solution.py:265
  112.0 0.0 all-to-all-done.2
  112.1 0.0 copy-start
  112.1 1.2 copy-done
  113.3 0.0 copy-start.1
  113.3 0.0 copy-start.4
  113.3 0.0 copy-start.6
  113.3 0.0 copy-start.7
  113.3 0.6 shard_map.145
  113.9 3.5 %collective-permute-start = (bf16[264,256]{1,0:T(8,128)(2,1)S(1)}, bf16[264,256]{1,0:T(8,128)(2,1)S(1)}, u32[]{:S(2)}, u32[]{:S(2)}) collective-permute-start(bf16[264,256]{1,0:T(8,128)(2,1)S(1)} %get-tuple-element.12), channel_id=1, source_target_pairs={{0,64},{64,0},{1,65},{65,1},{2,66},{66,2},{3,67},{67,3},{4,68},{68... | collective-permute-start | bytes 405512 | tf_op jit(solution)/shard_map/ppermute | solution.py:329
  117.4 3.9 %collective-permute-done.other_ref = bf16[264,256]{1,0:T(8,128)(2,1)S(1)} collective-permute-done((bf16[264,256]{1,0:T(8,128)(2,1)S(1)}, bf16[264,256]{1,0:T(8,128)(2,1)S(1)}, u32[]{:S(2)}, u32[]{:S(2)}) %collective-permute-start) | collective-permute-done | bytes 135200 | tf_op jit(solution)/shard_map/ppermute | solution.py:329
  121.3 0.0 copy-done.1
  121.3 1.2 shard_map.146
  122.4 11.3 %all-to-all-start.4 = ((bf16[32,64,128]{2,1,0:T(8,128)(2,1)}), bf16[32,64,128]{2,1,0:T(8,128)(2,1)S(1)}, u32[]{:S(2)}, u32[]{:S(2)}) async-start(bf16[32,64,128]{2,1,0:T(8,128)(2,1)} %bitcast.11), calls=%async_computation.4 | async-start | bytes 1048576 | tf_op jit(solution)/shard_map/all_to_all | solution.py:32
  133.7 0.0 copy-done.4
  133.7 0.0 copy-done.6
  133.7 0.0 copy-done.7
  133.7 1.7 %multiply_add_fusion = f32[64,1,64,64]{3,2,1,0:T(8,128)} fusion(f32[64,1,64,64]{3,2,1,0:T(8,128)S(1)} %copy-done.4, f32[64,64]{1,0:T(8,128)S(1)} %copy-done.7, f32[64,64]{1,0:T(8,128)S(1)} %copy-done.6, f32[]{:T(128)} %sub.7), kind=kLoop, calls=%fused_computation | loop fusion | flops 786432 | bytes 2129924 | tf_op jit(solution)/shard_map/add | solution.py:341
  135.4 9.4 %all-to-all-done.4.parts_ref = bf16[32,64,128]{2,1,0:T(8,128)(2,1)S(1)} async-done(((bf16[32,64,128]{2,1,0:T(8,128)(2,1)}), bf16[32,64,128]{2,1,0:T(8,128)(2,1)S(1)}, u32[]{:S(2)}, u32[]{:S(2)}) %all-to-all-start.4) | async-done | bytes 524320 | tf_op jit(solution)/shard_map/all_to_all | solution.py:32
  144.8 0.7 shard_map.147
  (1 shorter events, 0.0 us)
Async XLA Ops:
  7.2 0.7 copy-start.2
  8.6 15.3 %all-to-all-start = ((bf16[16,64,128]{2,1,0:T(8,128)(2,1)}), bf16[16,64,128]{2,1,0:T(8,128)(2,1)S(1)}, u32[]{:S(2)}, u32[]{:S(2)}) async-start(bf16[16,64,128]{2,1,0:T(8,128)(2,1)} %shard_map.140), calls=%async_computation | async-start | bytes 524288 | tf_op jit(solution)/shard_map/all_to_all | solution.py:32
  23.9 0.7 copy-start.5
  24.6 18.4 %copy-start.3 = (bf16[64,128]{1,0:T(8,128)(2,1)S(1)}, bf16[64,128]{1,0:T(8,128)(2,1)}, u32[]{:S(2)}) copy-start(bf16[64,128]{1,0:T(8,128)(2,1)} %tokens_ref.3) | copy-start | bytes 49156
  28.6 11.1 %all-to-all-start.1 = ((bf16[16,64,128]{2,1,0:T(8,128)(2,1)}), bf16[16,64,128]{2,1,0:T(8,128)(2,1)S(1)}, u32[]{:S(2)}, u32[]{:S(2)}) async-start(bf16[16,64,128]{2,1,0:T(8,128)(2,1)} %get-tuple-element.9), calls=%async_computation.1 | async-start | bytes 524288 | tf_op jit(solution)/shard_map/all_to_all | solution.py:32
  39.7 8.9 %all-to-all-start.3 = ((bf16[8,72,128]{2,1,0:T(8,128)(2,1)}), bf16[8,72,128]{2,1,0:T(8,128)(2,1)S(1)}, u32[]{:S(2)}, u32[]{:S(2)}) async-start(bf16[8,72,128]{2,1,0:T(8,128)(2,1)} %shard_map.143), calls=%async_computation.3 | async-start | bytes 294912 | tf_op jit(solution)/shard_map/all_to_all | solution.py:32
  48.6 63.5 %all-to-all-start.2 = ((bf16[32,64,128]{2,1,0:T(8,128)(2,1)}), bf16[32,64,128]{2,1,0:T(8,128)(2,1)S(1)}, u32[]{:S(2)}, u32[]{:S(2)}) async-start(bf16[32,64,128]{2,1,0:T(8,128)(2,1)} %get-tuple-element.10), calls=%async_computation.2 | async-start | bytes 1048576 | tf_op jit(solution)/shard_map/all_to_all | solution.py:32
  58.2 53.9 %all-gather.2.cloned.1.call-start = ((), (), s32[]{:S(2)}) async-start(), calls=%async_computation.5 | async-start | bytes 1179648 | tf_op jit(solution)/shard_map/all_gather | solution.py:265
  112.1 1.2 copy-start
  113.3 8.0 %copy-start.1 = (bf16[512,1024]{1,0:T(8,128)(2,1)S(1)}, bf16[512,1024]{1,0:T(8,128)(2,1)}, u32[]{:S(2)}) copy-start(bf16[512,1024]{1,0:T(8,128)(2,1)} %all-gather.2.cloned.1.call-done) | copy-start | bytes 3145732
  113.3 20.4 %copy-start.4 = (f32[64,1,64,64]{3,2,1,0:T(8,128)S(1)}, f32[64,1,64,64]{3,2,1,0:T(8,128)}, u32[]{:S(2)}) copy-start(f32[64,1,64,64]{3,2,1,0:T(8,128)} %param.25) | copy-start | bytes 3145732
  113.3 20.4 %copy-start.6 = (f32[64,64]{1,0:T(8,128)S(1)}, f32[64,64]{1,0:T(8,128)}, u32[]{:S(2)}) copy-start(f32[64,64]{1,0:T(8,128)} %get-tuple-element.14) | copy-start | bytes 49156
  113.3 20.4 %copy-start.7 = (f32[64,64]{1,0:T(8,128)S(1)}, f32[64,64]{1,0:T(8,128)}, u32[]{:S(2)}) copy-start(f32[64,64]{1,0:T(8,128)} %get-tuple-element.15) | copy-start | bytes 49156
  113.9 7.4 %collective-permute-start = (bf16[264,256]{1,0:T(8,128)(2,1)S(1)}, bf16[264,256]{1,0:T(8,128)(2,1)S(1)}, u32[]{:S(2)}, u32[]{:S(2)}) collective-permute-start(bf16[264,256]{1,0:T(8,128)(2,1)S(1)} %get-tuple-element.12), channel_id=1, source_target_pairs={{0,64},{64,0},{1,65},{65,1},{2,66},{66,2},{3,67},{67,3},{4,68},{68... | collective-permute-start | bytes 405512 | tf_op jit(solution)/shard_map/ppermute | solution.py:329
  122.4 22.4 %all-to-all-start.4 = ((bf16[32,64,128]{2,1,0:T(8,128)(2,1)}), bf16[32,64,128]{2,1,0:T(8,128)(2,1)S(1)}, u32[]{:S(2)}, u32[]{:S(2)}) async-start(bf16[32,64,128]{2,1,0:T(8,128)(2,1)} %bitcast.11), calls=%async_computation.4 | async-start | bytes 1048576 | tf_op jit(solution)/shard_map/all_to_all | solution.py:32
Sparse Core Ops, SparseCore 0:
  61.1 50.9 all-gather.1

commit v6 on v4

--- a/solution.py
+++ b/solution.py
@@ -15,8 +15,8 @@
 
 KV = ("y", "xh", "xl")
 TP = ("b3", "b2", "b1", "b0", "c")
-HALF = "xl"
-COLS = ("y", "xh")
+HALF = "xh"
+COLS = ("y", "xl")
 NEAR = "b0"
 CORE = "c"
 FAR = ("b3", "b2", "b1")
@@ -33,7 +33,7 @@
     return lax.all_to_all(blocks, axes, split_axis=0, concat_axis=0, tiled=True)
 
 
-def call(kernel, out, *operands, scalars=(), hbm=(), scratch=(), limit=16 << 20, flops=1 << 20):
+def call(kernel, out, *operands, scalars=(), hbm=(), out_hbm=(), scratch=(), limit=16 << 20, flops=1 << 20):
     outs = out if isinstance(out, tuple) else (out,)
     moved = sum(o.size * o.dtype.itemsize for o in operands)
     moved += sum(int(np.prod(o.shape)) * o.dtype.itemsize for o in outs)
@@ -45,7 +45,9 @@
         out_shape=out,
         in_specs=[smem] * len(scalars)
         + [far if n in hbm else vmem for n in range(len(operands))],
-        out_specs=(vmem,) * len(out) if isinstance(out, tuple) else vmem,
+        out_specs=tuple(far if n in out_hbm else vmem for n in range(len(out)))
+        if isinstance(out, tuple)
+        else vmem,
         scratch_shapes=scratch,
         compiler_params=pltpu.CompilerParams(vmem_limit_bytes=limit),
         cost_estimate=pl.CostEstimate(flops=flops, bytes_accessed=moved, transcendentals=0),
@@ -102,8 +104,8 @@
 
 
 def retention_kernel(decay_ref, *refs):
-    sources, (shares_ref, keys_ref, values_ref) = refs[:11], refs[11:14]
-    targets, (normed_ref, readout_ref, sems) = refs[14:25], refs[25:]
+    sources, (shares_ref, new_hbm) = refs[:11], refs[11:13]
+    targets, (normed_ref, readout_ref, new_ref, sems, out_sems) = refs[13:24], refs[24:]
     copies = [
         pltpu.make_async_copy(a, b, sems.at[n]) for n, (a, b) in enumerate(zip(sources, targets))
     ]
@@ -139,11 +141,21 @@
     keys = rotated(key_ref) * HEAD_DIM ** (-0.5)
     values = project(value_ref[...])
     gating = project(gate_ref[...])
-    keys_ref[...] = keys
-    values_ref[...] = values
-    columns = queries.T
+    columns, key_columns = queries.T, keys.T
     for copy in copies[8:]:
         copy.wait()
+    step = served // out_sems.shape[0]
+    given = [
+        pltpu.make_async_copy(
+            new_ref.at[pl.ds(n * step, step)], new_hbm.at[pl.ds(n * step, step)], out_sems.at[n]
+        )
+        for n in range(out_sems.shape[0])
+    ]
+    for b in range(served):
+        added = key_columns[:, b : b + 1] * values[b : b + 1]
+        new_ref[b] = decay_ref[0] * state_ref[b] + added
+        if b % step == step - 1 and b > step:
+            given[b // step - 1].start()
     for b in range(state_ref.shape[0]):
         readout_ref[b : b + 1] = jnp.sum(state_ref[b] * columns[:, b : b + 1], axis=0, keepdims=True)
     matched = jnp.sum(keys * queries, axis=1, keepdims=True)
@@ -152,9 +164,11 @@
     grouped = readout * lax.rsqrt(square + EPS) * gain_ref[...]
     merged = (grouped * (gating * jax.nn.sigmoid(gating))).astype(bf16)
     shares = jnp.dot(merged, output_ref[...], preferred_element_type=f32).astype(bf16)
-    feats = shares_ref.shape[2]
     for k in range(shares_ref.shape[0]):
         shares_ref[k] = shares[:, k * feats : (k + 1) * feats]
+    given[-1].start()
+    for copy in given:
+        copy.wait()
 
 
 def sum_of(parts_ref):
@@ -224,17 +238,8 @@
         out_ref[j] = part[:, j * feats : (j + 1) * feats]
 
 
-def halves_kernel(near_ref, parts_ref, own_ref, sent_ref):
-    served = own_ref.shape[0]
-    total = sum_of(parts_ref)
-    first, second = total[:served], total[served:]
-    own_ref[...] = jnp.where(near_ref[0] == 0, first, second)
-    sent_ref[...] = jnp.where(near_ref[0] == 0, second, first).astype(bf16)
-
-
-def final_kernel(own_ref, other_ref, after_ref, out_ref):
-    total = own_ref[...] + other_ref[...].astype(f32)
-    out_ref[...] = (after_ref[...].astype(f32) + total).astype(out_ref.dtype)
+def final_kernel(parts_ref, after_ref, out_ref):
+    out_ref[...] = (after_ref[...].astype(f32) + sum_of(parts_ref)).astype(out_ref.dtype)
 
 
 def layer(
@@ -304,21 +309,20 @@
         output_weight,
         group_gain.reshape(1, HEAD_DIM),
     )
-    shares, keys_new, values_new = call(
+    shares, new_state = call(
         retention_kernel,
-        (
-            like((kv, served, feats), bf16),
-            like((served, HEAD_DIM), f32),
-            like((served, HEAD_DIM), f32),
-        ),
+        (like((kv, served, feats), bf16), like(state.shape, f32)),
         *operands,
         scalars=(decay,),
         hbm=tuple(range(len(operands))),
+        out_hbm=(1,),
         scratch=(
             *(pltpu.VMEM(a.shape, a.dtype) for a in operands),
             pltpu.VMEM((served, kv * feats), bf16),
             pltpu.VMEM((served, HEAD_DIM), f32),
+            pltpu.VMEM(state.shape, f32),
             pltpu.SemaphoreType.DMA((len(operands),)),
+            pltpu.SemaphoreType.DMA((4,)),
         ),
         limit=63 << 20,
         flops=2 * served * D * 6 * HEAD_DIM,
@@ -357,16 +361,9 @@
         flops=2 * count * cols * feats * far * units,
     )
 
-    lowered = swap(lowered.reshape(cols * cores, 2 * served, feats), COLS + (CORE,))
-    kept, back = call(
-        halves_kernel,
-        (like((served, feats), f32), like((served, feats), bf16)),
-        lowered,
-        scalars=(near,),
-    )
-    returned = lax.ppermute(back, NEAR, turn)
-    mixed = call(final_kernel, like((served, feats), bf16), kept, returned, after)
-    new_state = decay * state + keys_new[:, :, None] * values_new[:, None, :]
+    lowered = lowered.reshape(cols * 2 * cores, served, feats)
+    lowered = swap(lowered, COLS + (CORE, NEAR))
+    mixed = call(final_kernel, like((served, feats), bf16), lowered, after)
     return (mixed, new_state[:, None])
 
 

time: 121 us -> 115 us (0.950)
  blocking collectives: 66.4 us -> 62.5 us
  other arithmetic: 3.27 us -> 1.58 us
  starting transfers between devices: 12.7 us -> 11.3 us
  Pallas kernels: 8.86 us -> 10.1 us
    all_to_all x4, blocking collectives: 66.4 us -> 62.5 us  [swap(): return lax.all_to_all(blocks, axes, split_axis=0, concat_axis=0, tiled=True)]
    ppermute x1 -> x0, starting transfers between devices: 3.29 us -> none  [layer(): returned = lax.ppermute(back, NEAR, turn)]
    add x1 -> x0, other arithmetic: 1.69 us -> none  [layer(): new_state = decay * state + keys_new[:, :, None] * values_new[:, None, :]]
    pallas_call x10 -> x9, Pallas kernels: 8.86 us -> 10.1 us  [call(): pl.pallas_call(kernel, out_shape=out, in_specs=[smem] * len(scalars) + [f...]
    unnamed x16 -> x10, local copies, waits for them, and re-layouts: 2.66 us -> 2.66 us
  transfers between devices with their start and end apart: 5 -> 4, of which waited for: 3 -> 3; matrix products, arithmetic and copies ran while one was open for 3% -> 1% of each run, Pallas kernels for 4% -> 5%
where the time goes in v6:
time: 115 us; the launch traced here: 114 us
  blocking collectives  62.5 us (54%)
  between operations  14.2 us (12%)
  waiting for transfers between devices  11.6 us (10%)
  starting transfers between devices  11.3 us (10%)
  Pallas kernels  10.1 us (9%)
  local copies, waits for them, and re-layouts  2.66 us (2%)
  other arithmetic  1.58 us (1%)
    all_to_all x4, blocking collectives, swap(): return lax.all_to_all(blocks, axes, split_axis=0, concat_axis=0, tiled=True)  62.5 us
    pallas_call x9, Pallas kernels, call(): pl.pallas_call(kernel, out_shape=out, in_specs=[smem] * len(scalars) + [f...  10.1 us
    all_to_all x1, waiting for transfers between devices, swap(): return lax.all_to_all(blocks, axes, split_axis=0, concat_axis=0, tiled=True)  5.95 us
    all_to_all x1, starting transfers between devices, swap(): return lax.all_to_all(blocks, axes, split_axis=0, concat_axis=0, tiled=True)  4.44 us
    ppermute x1, waiting for transfers between devices, layer(): other = lax.ppermute(given, HALF, turn)  4.01 us
    ppermute x1, starting transfers between devices, layer(): passed = lax.ppermute(after, NEAR, turn)  3.55 us
    ppermute x1, starting transfers between devices, layer(): other = lax.ppermute(given, HALF, turn)  3.24 us
    unnamed x10, local copies, waits for them, and re-layouts  2.66 us
  transfers between devices with their start and end apart: 4, of which 3 were waited for; matrix products, arithmetic and copies ran while one was open for 1% of the time, Pallas kernels for 5%

profile of v6, /device:TPU:1, one launch (start us, length us, event | category | flops | bytes accessed | tf_op | source)
XLA Modules:
  0.0 113.9 jit_solution(941075352709074478)
XLA Ops:
  7.2 0.0 all-gather.2.cloned.1.call-start
  7.3 1.7 %shard_map.144 = bf16[8,72,128]{2,1,0:T(8,128)(2,1)} custom-call(f32[1]{0:T(128)} %bitcast.1.decay_ref, bf16[128,256]{1,0:T(8,128)(2,1)} %up_hbm.1, bf16[256,128]{1,0:T(8,128)(2,1)} %down_hbm.1, f32[1,128]{1,0:T(1,128)} %bitcast.26), custom_call_target="tpu_custom_call" | custom-call | flops 1048576 | bytes 279040 | tf_op jit(solution)/shard_map/pallas_call | solution.py:43
  8.9 11.6 %all_to_all.25.arrived_ref = bf16[8,72,128]{2,1,0:T(8,128)(2,1)S(1)} all-to-all(bf16[8,72,128]{2,1,0:T(8,128)(2,1)} %shard_map.144), channel_id=1, replica_groups=mesh['y'=4,'xh'=2,'xl'=2,'b3'=2,'b2'=2,'b1'=2,'b0'=2,'c'=2] {'y','xl'}, dimensions={0} | all-to-all | bytes 294912 | tf_op jit(solution)/shard_map/all_to_all | solution.py:33
  20.5 0.7 shard_map.145
  21.2 0.0 all-gather.2.cloned.1.call-update
  21.2 0.0 copy-start.2
  21.2 0.7 copy-done.2
  21.9 0.8 shard_map.140
  22.7 4.4 %all-to-all-start = ((bf16[16,64,128]{2,1,0:T(8,128)(2,1)}), bf16[16,64,128]{2,1,0:T(8,128)(2,1)S(1)}, u32[]{:S(2)}, u32[]{:S(2)}) async-start(bf16[16,64,128]{2,1,0:T(8,128)(2,1)} %shard_map.140), calls=%async_computation | async-start | bytes 524288 | tf_op jit(solution)/shard_map/all_to_all | solution.py:33
  27.1 0.7 convert_element_type.7
  27.8 0.2 fusion
  28.0 0.7 pad_maximum_fusion
  28.7 6.0 %all-to-all-done.refs_0_ = bf16[16,64,128]{2,1,0:T(8,128)(2,1)S(1)} async-done(((bf16[16,64,128]{2,1,0:T(8,128)(2,1)}), bf16[16,64,128]{2,1,0:T(8,128)(2,1)S(1)}, u32[]{:S(2)}, u32[]{:S(2)}) %all-to-all-start) | async-done | bytes 262176 | tf_op jit(solution)/shard_map/all_to_all | solution.py:33
  34.6 0.0 copy-start.4
  34.6 0.7 copy-done.4
  35.4 0.0 copy-start.3
  35.4 5.2 %shard_map.141 = (bf16[16,64,128]{2,1,0:T(8,128)(2,1)}, f32[64,64,64]{2,1,0:T(8,128)}) custom-call(f32[1]{0:T(128)} %bitcast.1.decay_ref, bf16[16,64,128]{2,1,0:T(8,128)(2,1)} %copy-done.4, f32[1,2048]{1,0:T(1,128)} %bitcast.25, bf16[64,2048]{1,0:T(8,128)(2,1)} %bitcast.21, bf16[64,2048]{1,0:T(8,128)(2,1)} %bitcast.22, bf16[64,2048]{1,0:T(8,128)(2,1)} %bitcast.23, ...), custom_call_target="tpu_custom_call" | custom-call | flops 100663296 | bytes 3973376 | tf_op jit(solution)/shard_map/pallas_call | solution.py:43
  40.6 11.0 %all_to_all.26.parts_ref = bf16[16,64,128]{2,1,0:T(8,128)(2,1)S(1)} all-to-all(bf16[16,64,128]{2,1,0:T(8,128)(2,1)} %get-tuple-element.6), channel_id=1, replica_groups=mesh['y'=4,'xh'=2,'xl'=2,'b3'=2,'b2'=2,'b1'=2,'b0'=2,'c'=2] {'y','xh','xl'}, dimensions={0} | all-to-all | bytes 524288 | tf_op jit(solution)/shard_map/all_to_all | solution.py:33
  51.6 0.0 copy-done.3
  51.7 3.5 %collective-permute-start = (bf16[64,128]{1,0:T(8,128)(2,1)S(1)}, bf16[64,128]{1,0:T(8,128)(2,1)S(1)}, u32[]{:S(2)}, u32[]{:S(2)}) collective-permute-start(bf16[64,128]{1,0:T(8,128)(2,1)S(1)} %shard_map.142.own_ref.after_ref), channel_id=1, source_target_pairs={{0,2},{2,0},{1,3},{3,1},{4,6},{6,4},{5,7},{7,5},{8,10},{10,8},{9,1... | collective-permute-start | bytes 49160 | tf_op jit(solution)/shard_map/ppermute | solution.py:333
  55.3 1.6 %collective-permute-done.other_ref = bf16[64,128]{1,0:T(8,128)(2,1)S(1)} collective-permute-done((bf16[64,128]{1,0:T(8,128)(2,1)S(1)}, bf16[64,128]{1,0:T(8,128)(2,1)S(1)}, u32[]{:S(2)}, u32[]{:S(2)}) %collective-permute-start) | collective-permute-done | bytes 16416 | tf_op jit(solution)/shard_map/ppermute | solution.py:333
  56.8 0.1 shard_map.143
  56.9 19.5 %all_to_all.27 = bf16[16,128,128]{2,1,0:T(8,128)(2,1)S(1)} all-to-all(bf16[16,128,128]{2,1,0:T(8,128)(2,1)S(1)} %shard_map.143), channel_id=1, replica_groups=mesh['y'=4,'xh'=2,'xl'=2,'b3'=2,'b2'=2,'b1'=2,'b0'=2,'c'=2] {'y','xl','c'}, dimensions={0} | all-to-all | bytes 1048576 | tf_op jit(solution)/shard_map/all_to_all | solution.py:33
  76.4 0.0 all-gather.2.cloned.1.call-done
  76.4 0.0 copy-start
  76.4 1.2 %copy-done = bf16[512,1024]{1,0:T(8,128)(2,1)S(1)} copy-done((bf16[512,1024]{1,0:T(8,128)(2,1)S(1)}, bf16[512,1024]{1,0:T(8,128)(2,1)}, u32[]{:S(2)}) %copy-start) | copy-done | bytes 1048600
  77.6 0.0 copy-start.1
  77.6 0.6 shard_map.146
  78.2 3.2 %collective-permute-start.1 = (bf16[264,256]{1,0:T(8,128)(2,1)S(1)}, bf16[264,256]{1,0:T(8,128)(2,1)S(1)}, u32[]{:S(2)}, u32[]{:S(2)}) collective-permute-start(bf16[264,256]{1,0:T(8,128)(2,1)S(1)} %get-tuple-element.8), channel_id=1, source_target_pairs={{0,64},{64,0},{1,65},{65,1},{2,66},{66,2},{3,67},{67,3},{4,68},{68... | collective-permute-start | bytes 405512 | tf_op jit(solution)/shard_map/ppermute | solution.py:354
  81.5 4.0 %collective-permute-done.1.other_ref = bf16[264,256]{1,0:T(8,128)(2,1)S(1)} collective-permute-done((bf16[264,256]{1,0:T(8,128)(2,1)S(1)}, bf16[264,256]{1,0:T(8,128)(2,1)S(1)}, u32[]{:S(2)}, u32[]{:S(2)}) %collective-permute-start.1) | collective-permute-done | bytes 135200 | tf_op jit(solution)/shard_map/ppermute | solution.py:354
  85.5 0.0 copy-done.1
  85.5 0.4 shard_map.147
  85.9 20.5 %all_to_all.28.parts_ref = bf16[32,64,128]{2,1,0:T(8,128)(2,1)S(1)} all-to-all(bf16[32,64,128]{2,1,0:T(8,128)(2,1)S(1)} %bitcast.19), channel_id=1, replica_groups=mesh['y'=4,'xh'=2,'xl'=2,'b3'=2,'b2'=2,'b1'=2,'b0'=2,'c'=2] {'y','xl','c..., dimensions={0} | all-to-all | bytes 1048576 | tf_op jit(solution)/shard_map/all_to_all | solution.py:33
  106.3 0.7 shard_map.148
  (2 shorter events, 0.1 us)
Async XLA Ops:
  7.2 69.2 %all-gather.2.cloned.1.call-start = ((), (), s32[]{:S(2)}) async-start(), calls=%async_computation.5 | async-start | bytes 1179648 | tf_op jit(solution)/shard_map/all_gather | solution.py:288
  21.2 0.7 copy-start.2
  22.7 12.0 %all-to-all-start = ((bf16[16,64,128]{2,1,0:T(8,128)(2,1)}), bf16[16,64,128]{2,1,0:T(8,128)(2,1)S(1)}, u32[]{:S(2)}, u32[]{:S(2)}) async-start(bf16[16,64,128]{2,1,0:T(8,128)(2,1)} %shard_map.140), calls=%async_computation | async-start | bytes 524288 | tf_op jit(solution)/shard_map/all_to_all | solution.py:33
  34.6 0.7 copy-start.4
  35.4 16.3 %copy-start.3 = (bf16[64,128]{1,0:T(8,128)(2,1)S(1)}, bf16[64,128]{1,0:T(8,128)(2,1)}, u32[]{:S(2)}) copy-start(bf16[64,128]{1,0:T(8,128)(2,1)} %tokens_ref.3) | copy-start | bytes 49156
  51.7 5.1 %collective-permute-start = (bf16[64,128]{1,0:T(8,128)(2,1)S(1)}, bf16[64,128]{1,0:T(8,128)(2,1)S(1)}, u32[]{:S(2)}, u32[]{:S(2)}) collective-permute-start(bf16[64,128]{1,0:T(8,128)(2,1)S(1)} %shard_map.142.own_ref.after_ref), channel_id=1, source_target_pairs={{0,2},{2,0},{1,3},{3,1},{4,6},{6,4},{5,7},{7,5},{8,10},{10,8},{9,1... | collective-permute-start | bytes 49160 | tf_op jit(solution)/shard_map/ppermute | solution.py:333
  76.4 1.2 %copy-start = (bf16[512,1024]{1,0:T(8,128)(2,1)S(1)}, bf16[512,1024]{1,0:T(8,128)(2,1)}, u32[]{:S(2)}) copy-start(bf16[512,1024]{1,0:T(8,128)(2,1)} %all-gather.2.cloned.1.call-done) | copy-start | bytes 3145732
  77.6 7.9 %copy-start.1 = (bf16[512,1024]{1,0:T(8,128)(2,1)S(1)}, bf16[512,1024]{1,0:T(8,128)(2,1)}, u32[]{:S(2)}) copy-start(bf16[512,1024]{1,0:T(8,128)(2,1)} %all-gather.2.cloned.1.call-done) | copy-start | bytes 3145732
  78.2 7.3 %collective-permute-start.1 = (bf16[264,256]{1,0:T(8,128)(2,1)S(1)}, bf16[264,256]{1,0:T(8,128)(2,1)S(1)}, u32[]{:S(2)}, u32[]{:S(2)}) collective-permute-start(bf16[264,256]{1,0:T(8,128)(2,1)S(1)} %get-tuple-element.8), channel_id=1, source_target_pairs={{0,64},{64,0},{1,65},{65,1},{2,66},{66,2},{3,67},{67,3},{4,68},{68... | collective-permute-start | bytes 405512 | tf_op jit(solution)/shard_map/ppermute | solution.py:354
Sparse Core Ops, SparseCore 0:
  21.3 53.3 all-gather.1

commit v7 on v6

--- a/solution.py
+++ b/solution.py
@@ -17,6 +17,7 @@
 TP = ("b3", "b2", "b1", "b0", "c")
 HALF = "xh"
 COLS = ("y", "xl")
+RING = ("xh", "xl")
 NEAR = "b0"
 CORE = "c"
 FAR = ("b3", "b2", "b1")
@@ -62,7 +63,7 @@
         copy.wait()
 
 
-def pack_kernel(decay_ref, up_hbm, down_hbm, gain_hbm, out_ref, *scratch):
+def pack_kernel(decay_ref, half_ref, up_hbm, down_hbm, gain_hbm, out_ref, *scratch):
     up_ref, down_ref, gain_ref, sems = scratch
     fetch(
         (
@@ -84,9 +85,11 @@
     rows = jnp.where(row == 0, first, jnp.where(row == 1, second, jnp.where(row == 2, third, zero)))
     rows = rows.astype(bf16)
     up = up_ref[...].astype(f32).T.astype(bf16)
+    down = down_ref[...]
     for j in range(cols):
-        out_ref[j, :units] = up[j * units : (j + 1) * units]
-        out_ref[j, units : 2 * units] = down_ref[j * units : (j + 1) * units]
+        at, turned = slice(j * units, (j + 1) * units), slice((j ^ 1) * units, ((j ^ 1) + 1) * units)
+        out_ref[j, :units] = jnp.where(half_ref[0] == 0, up[at], up[turned])
+        out_ref[j, units : 2 * units] = jnp.where(half_ref[0] == 0, down[at], down[turned])
         out_ref[j, 2 * units :] = rows
 
 
@@ -94,13 +97,6 @@
     tokens = tokens_ref[...]
     for k in range(copies_ref.shape[0]):
         copies_ref[k] = tokens
-
-
-def unpack_kernel(arrived_ref, mine_ref):
-    feats = arrived_ref.shape[2]
-    both = mine_ref.shape[0]
-    for j in range(arrived_ref.shape[0]):
-        mine_ref[:, j * feats : (j + 1) * feats] = arrived_ref[j, :both]
 
 
 def retention_kernel(decay_ref, *refs):
@@ -193,25 +189,21 @@
 def up_kernel(rows_ref, arrived_ref, weights_ref, own_ref, sent_ref):
     cols, count, feats = rows_ref.shape
     lines = arrived_ref.shape[1]
-    far, _, units, width = weights_ref.shape
+    far = weights_ref.shape[0] // cols
+    part = jnp.zeros((count, sent_ref.shape[1]), f32)
     ones = jnp.ones((8, feats), bf16)
     total = jnp.zeros((8, count), f32)
-    scaled = []
     for j in range(cols):
         x = rows_ref[j].astype(f32)
         pieces = arrived_ref[j, lines - 8 :].astype(f32)
-        scaled.append((x * (pieces[0:1] + pieces[1:2] + pieces[2:3])).astype(bf16))
+        scaled = (x * (pieces[0:1] + pieces[1:2] + pieces[2:3])).astype(bf16)
+        weight = jnp.concatenate([weights_ref[f * cols + j] for f in range(far)])
+        part = part + lax.dot_general(scaled, weight, NT, preferred_element_type=f32)
         square = x * x
         high = square.astype(bf16)
         low = (square - high.astype(f32)).astype(bf16)
         total = total + lax.dot_general(ones, high, NT, preferred_element_type=f32)
         total = total + lax.dot_general(ones, low, NT, preferred_element_type=f32)
-    part = lax.dot_general(
-        jnp.concatenate(scaled, axis=1),
-        weights_ref[:, 0].reshape(far * units, width),
-        NT,
-        preferred_element_type=f32,
-    )
     own_ref[:count] = part
     sent_ref[:count] = part.astype(bf16)
     high = total.astype(bf16).astype(f32)
@@ -223,7 +215,7 @@
 
 
 def down_kernel(own_ref, other_ref, weights_ref, out_ref):
-    cols, count, feats = out_ref.shape
+    cols, count, _ = out_ref.shape
     total = own_ref[...] + other_ref[...].astype(f32)
     squares = total[count : count + 1] + total[count + 1 : count + 2]
     row = lax.broadcasted_iota(jnp.int32, (count, count), 0)
@@ -232,10 +224,10 @@
     factor = lax.rsqrt(jnp.sum(mine, axis=1, keepdims=True) / D + EPS)
     raised = jnp.maximum(total[:count] * factor, 0.0)
     hidden = (raised * raised).astype(bf16)
-    weight = weights_ref[:, 1].reshape(-1, weights_ref.shape[3])
-    part = jnp.dot(hidden, weight, preferred_element_type=f32).astype(bf16)
+    far = weights_ref.shape[0] // cols
     for j in range(cols):
-        out_ref[j] = part[:, j * feats : (j + 1) * feats]
+        weight = jnp.concatenate([weights_ref[f * cols + j] for f in range(far)])
+        out_ref[j] = jnp.dot(hidden, weight, preferred_element_type=f32).astype(bf16)
 
 
 def final_kernel(parts_ref, after_ref, out_ref):
@@ -273,7 +265,7 @@
         up_weight,
         down_weight,
         channel_gain.reshape(1, feats),
-        scalars=(decay,),
+        scalars=(decay, lax.axis_index(HALF)),
         hbm=(0, 1, 2),
         limit=63 << 20,
         scratch=(
@@ -284,8 +276,7 @@
         ),
     )
     arrived = swap(sent, COLS)
-    mine = call(unpack_kernel, like((2 * units, cols * feats), bf16), arrived)
-    weights = lax.all_gather(mine, FAR, axis=0, tiled=True)
+    weights = lax.all_gather(arrived, FAR, axis=0, tiled=True)
 
     copies = call(copies_kernel, like((kv, served, feats), bf16), tokens)
     blocks = swap(copies, KV)
@@ -339,7 +330,7 @@
         scalars=(near,),
     )
     rows = swap(copies, COLS + (CORE,)).reshape(cols, count, feats)
-    weights = weights.reshape(far, 2, units, cols * feats)
+    ups = weights[:, :units]
     own, given = call(
         up_kernel,
         (
@@ -348,16 +339,18 @@
         ),
         rows,
         arrived,
-        weights,
+        ups,
         flops=2 * count * cols * feats * far * units,
     )
-    other = lax.ppermute(given, HALF, turn)
+    weights, given = lax.optimization_barrier((weights, given))
+    downs = weights[:, units : 2 * units]
+    other = lax.ppermute(given, RING, [(0, 3), (1, 2), (2, 1), (3, 0)])
     lowered = call(
         down_kernel,
         like((cols, count, feats), bf16),
         own,
         other,
-        weights,
+        downs,
         flops=2 * count * cols * feats * far * units,
     )
 

time: 115 us -> 115 us (level)
  blocking collectives: 62.5 us -> 42.9 us
  starting transfers between devices: 11.3 us -> 21.9 us
  waiting for transfers between devices: 11.6 us -> 19.4 us
    all_to_all x4 -> x3, blocking collectives: 62.5 us -> 42.9 us  [swap(): return lax.all_to_all(blocks, axes, split_axis=0, concat_axis=0, tiled=True)]
    all_to_all x1 -> x2, starting transfers between devices: 4.44 us -> 15.6 us  [swap(): return lax.all_to_all(blocks, axes, split_axis=0, concat_axis=0, tiled=True)]
    all_gather x1, waiting for transfers between devices: 0.01 us -> 6.74 us  [layer(): weights = lax.all_gather(arrived, FAR, axis=0, tiled=True)]
    slice x0 -> x2, local copies, waits for them, and re-layouts: none -> 2.17 us  [the longest x1 1.09 us: layer(): downs = weights[:, units:2 * units]]
    all_to_all x1 -> x2, waiting for transfers between devices: 5.95 us -> 7.88 us  [swap(): return lax.all_to_all(blocks, axes, split_axis=0, concat_axis=0, tiled=True)]
    unnamed x10 -> x8, local copies, waits for them, and re-layouts: 2.66 us -> 1.42 us
    pallas_call x9 -> x8, Pallas kernels: 10.1 us -> 10.5 us  [call(): pl.pallas_call(kernel, out_shape=out, in_specs=[smem] * len(scalars) + [f...]
  transfers between devices with their start and end apart: 4 -> 5, of which waited for: 3 -> 5; matrix products, arithmetic and copies ran while one was open for 1% -> 3% of each run, Pallas kernels for 5% -> 6%
where the time goes in v7:
time: 115 us; the launch traced here: 114 us
  blocking collectives  42.9 us (37%)
  starting transfers between devices  21.9 us (19%)
  waiting for transfers between devices  19.4 us (17%)
  between operations  14.2 us (12%)
  Pallas kernels  10.5 us (9%)
  local copies, waits for them, and re-layouts  3.6 us (3%)
  other arithmetic  1.59 us (1%)
    all_to_all x3, blocking collectives, swap(): return lax.all_to_all(blocks, axes, split_axis=0, concat_axis=0, tiled=True)  42.9 us
    all_to_all x2, starting transfers between devices, swap(): return lax.all_to_all(blocks, axes, split_axis=0, concat_axis=0, tiled=True)  15.6 us
    pallas_call x8, Pallas kernels, call(): pl.pallas_call(kernel, out_shape=out, in_specs=[smem] * len(scalars) + [f...  10.5 us
    all_to_all x2, waiting for transfers between devices, swap(): return lax.all_to_all(blocks, axes, split_axis=0, concat_axis=0, tiled=True)  7.88 us
    all_gather x1, waiting for transfers between devices, layer(): weights = lax.all_gather(arrived, FAR, axis=0, tiled=True)  6.74 us
    ppermute x1, starting transfers between devices, layer(): passed = lax.ppermute(after, NEAR, turn)  3.55 us
    ppermute x1, waiting for transfers between devices, layer(): other = lax.ppermute(given, RING, [(0, 3), (1, 2), (2, 1), (3, 0)])  3.08 us
    ppermute x1, starting transfers between devices, layer(): other = lax.ppermute(given, RING, [(0, 3), (1, 2), (2, 1), (3, 0)])  2.78 us
  transfers between devices with their start and end apart: 5, of which 5 were waited for; matrix products, arithmetic and copies ran while one was open for 3% of the time, Pallas kernels for 6%

profile of v7, /device:TPU:1, one launch (start us, length us, event | category | flops | bytes accessed | tf_op | source)
XLA Modules:
  0.0 114.0 jit_solution(10072300370324562156)
XLA Ops:
  7.2 0.0 all-gather.2.cloned.1.call-start
  7.3 1.7 %shard_map.144 = bf16[8,72,128]{2,1,0:T(8,128)(2,1)} custom-call(f32[1]{0:T(128)} %bitcast.1.decay_ref, s32[1]{0:T(128)} %bitcast.10.half_ref, bf16[128,256]{1,0:T(8,128)(2,1)} %up_hbm.1, bf16[256,128]{1,0:T(8,128)(2,1)} %down_hbm.1, f32[1,128]{1,0:T(1,128)} %bitcast.24), custom_call_target="tpu_custom_call" | custom-call | flops 1048576 | bytes 279040 | tf_op jit(solution)/shard_map/pallas_call | solution.py:44
  8.9 11.7 %all_to_all.25.arrived_ref = bf16[8,72,128]{2,1,0:T(8,128)(2,1)} all-to-all(bf16[8,72,128]{2,1,0:T(8,128)(2,1)} %shard_map.144), channel_id=1, replica_groups=mesh['y'=4,'xh'=2,'xl'=2,'b3'=2,'b2'=2,'b1'=2,'b0'=2,'c'=2] {'y','xl'}, dimensions={0} | all-to-all | bytes 294912 | tf_op jit(solution)/shard_map/all_to_all | solution.py:34
  20.6 0.0 all-gather.2.cloned.1.call-update
  20.6 0.0 copy-start.1
  20.6 0.7 copy-done.1
  21.3 0.8 shard_map.140
  22.1 4.4 %all-to-all-start = ((bf16[16,64,128]{2,1,0:T(8,128)(2,1)}), bf16[16,64,128]{2,1,0:T(8,128)(2,1)S(1)}, u32[]{:S(2)}, u32[]{:S(2)}) async-start(bf16[16,64,128]{2,1,0:T(8,128)(2,1)} %shard_map.140), calls=%async_computation | async-start | bytes 524288 | tf_op jit(solution)/shard_map/all_to_all | solution.py:34
  26.5 0.7 convert_element_type.7
  27.2 0.2 fusion
  27.4 0.7 pad_maximum_fusion
  28.1 5.9 %all-to-all-done.refs_0_ = bf16[16,64,128]{2,1,0:T(8,128)(2,1)S(1)} async-done(((bf16[16,64,128]{2,1,0:T(8,128)(2,1)}), bf16[16,64,128]{2,1,0:T(8,128)(2,1)S(1)}, u32[]{:S(2)}, u32[]{:S(2)}) %all-to-all-start) | async-done | bytes 262176 | tf_op jit(solution)/shard_map/all_to_all | solution.py:34
  34.1 0.0 copy-start.3
  34.1 0.7 copy-done.3
  34.8 0.0 copy-start.2
  34.8 5.2 %shard_map.141 = (bf16[16,64,128]{2,1,0:T(8,128)(2,1)}, f32[64,64,64]{2,1,0:T(8,128)}) custom-call(f32[1]{0:T(128)} %bitcast.1.decay_ref, bf16[16,64,128]{2,1,0:T(8,128)(2,1)} %copy-done.3, f32[1,2048]{1,0:T(1,128)} %bitcast.23, bf16[64,2048]{1,0:T(8,128)(2,1)} %bitcast.19, bf16[64,2048]{1,0:T(8,128)(2,1)} %bitcast.20, bf16[64,2048]{1,0:T(8,128)(2,1)} %bitcast.21, ...), custom_call_target="tpu_custom_call" | custom-call | flops 100663296 | bytes 3973376 | tf_op jit(solution)/shard_map/pallas_call | solution.py:44
  40.0 0.0 copy-start
  40.0 11.2 %all_to_all.26.parts_ref = bf16[16,64,128]{2,1,0:T(8,128)(2,1)S(1)} all-to-all(bf16[16,64,128]{2,1,0:T(8,128)(2,1)} %get-tuple-element.8), channel_id=1, replica_groups=mesh['y'=4,'xh'=2,'xl'=2,'b3'=2,'b2'=2,'b1'=2,'b0'=2,'c'=2] {'y','xh','xl'}, dimensions={0} | all-to-all | bytes 524288 | tf_op jit(solution)/shard_map/all_to_all | solution.py:34
  51.2 0.0 copy-done.2
  51.3 3.5 %collective-permute-start = (bf16[64,128]{1,0:T(8,128)(2,1)S(1)}, bf16[64,128]{1,0:T(8,128)(2,1)S(1)}, u32[]{:S(2)}, u32[]{:S(2)}) collective-permute-start(bf16[64,128]{1,0:T(8,128)(2,1)S(1)} %shard_map.142.own_ref.after_ref), channel_id=1, source_target_pairs={{0,2},{2,0},{1,3},{3,1},{4,6},{6,4},{5,7},{7,5},{8,10},{10,8},{9,1... | collective-permute-start | bytes 49160 | tf_op jit(solution)/shard_map/ppermute | solution.py:324
  54.8 1.6 %collective-permute-done.other_ref = bf16[64,128]{1,0:T(8,128)(2,1)S(1)} collective-permute-done((bf16[64,128]{1,0:T(8,128)(2,1)S(1)}, bf16[64,128]{1,0:T(8,128)(2,1)S(1)}, u32[]{:S(2)}, u32[]{:S(2)}) %collective-permute-start) | collective-permute-done | bytes 16416 | tf_op jit(solution)/shard_map/ppermute | solution.py:324
  56.5 0.9 shard_map.143
  57.4 11.1 %all-to-all-start.2 = ((bf16[16,128,128]{2,1,0:T(8,128)(2,1)}), bf16[16,128,128]{2,1,0:T(8,128)(2,1)S(1)}, u32[]{:S(2)}, u32[]{:S(2)}) async-start(bf16[16,128,128]{2,1,0:T(8,128)(2,1)} %shard_map.143), calls=%async_computation.2 | async-start | bytes 1048576 | tf_op jit(solution)/shard_map/all_to_all | solution.py:34
  68.5 6.7 %all-gather.2.cloned.1.call-done = bf16[64,72,128]{2,1,0:T(8,128)(2,1)} async-done(((bf16[8,72,128]{2,1,0:T(8,128)(2,1)}), bf16[64,72,128]{2,1,0:T(8,128)(2,1)}) %all-gather.2.cloned.1.call-update) | async-done | bytes 1179664 | tf_op jit(solution)/shard_map/all_gather | solution.py:279
  75.2 1.1 slice.8.weights_ref
  76.3 1.9 %all-to-all-done.2 = bf16[16,128,128]{2,1,0:T(8,128)(2,1)S(1)} async-done(((bf16[16,128,128]{2,1,0:T(8,128)(2,1)}), bf16[16,128,128]{2,1,0:T(8,128)(2,1)S(1)}, u32[]{:S(2)}, u32[]{:S(2)}) %all-to-all-start.2) | async-done | bytes 524320 | tf_op jit(solution)/shard_map/all_to_all | solution.py:34
  78.3 0.0 copy-done
  78.3 0.7 shard_map.145
  79.0 2.8 %collective-permute-start.1 = (bf16[264,256]{1,0:T(8,128)(2,1)S(1)}, bf16[264,256]{1,0:T(8,128)(2,1)S(1)}, u32[]{:S(2)}, u32[]{:S(2)}) collective-permute-start(bf16[264,256]{1,0:T(8,128)(2,1)S(1)} %get-tuple-element.11), channel_id=1, source_target_pairs={{0,96},{32,64},{64,32},{96,0},{1,97},{33,65},{65,33},{97,1},{2,98}... | collective-permute-start | bytes 405512 | tf_op jit(solution)/shard_map/ppermute | solution.py:347
  81.7 1.1 slice.7.weights_ref
  82.8 3.1 %collective-permute-done.1.other_ref = bf16[264,256]{1,0:T(8,128)(2,1)S(1)} collective-permute-done((bf16[264,256]{1,0:T(8,128)(2,1)S(1)}, bf16[264,256]{1,0:T(8,128)(2,1)S(1)}, u32[]{:S(2)}, u32[]{:S(2)}) %collective-permute-start.1) | collective-permute-done | bytes 135200 | tf_op jit(solution)/shard_map/ppermute | solution.py:347
  85.9 0.5 shard_map.146
  86.4 20.0 %all_to_all.27.parts_ref = bf16[32,64,128]{2,1,0:T(8,128)(2,1)S(1)} all-to-all(bf16[32,64,128]{2,1,0:T(8,128)(2,1)S(1)} %bitcast.17), channel_id=1, replica_groups=mesh['y'=4,'xh'=2,'xl'=2,'b3'=2,'b2'=2,'b1'=2,'b0'=2,'c'=2] {'y','xl','c..., dimensions={0} | all-to-all | bytes 1048576 | tf_op jit(solution)/shard_map/all_to_all | solution.py:34
  106.5 0.7 shard_map.147
  (2 shorter events, 0.1 us)
Async XLA Ops:
  7.2 68.1 %all-gather.2.cloned.1.call-start = ((), (), s32[]{:S(2)}) async-start(), calls=%async_computation.5 | async-start | bytes 1327104 | tf_op jit(solution)/shard_map/all_gather | solution.py:279
  20.6 0.7 copy-start.1
  22.1 12.0 %all-to-all-start = ((bf16[16,64,128]{2,1,0:T(8,128)(2,1)}), bf16[16,64,128]{2,1,0:T(8,128)(2,1)S(1)}, u32[]{:S(2)}, u32[]{:S(2)}) async-start(bf16[16,64,128]{2,1,0:T(8,128)(2,1)} %shard_map.140), calls=%async_computation | async-start | bytes 524288 | tf_op jit(solution)/shard_map/all_to_all | solution.py:34
  34.1 0.7 copy-start.3
  34.8 16.4 %copy-start.2 = (bf16[64,128]{1,0:T(8,128)(2,1)S(1)}, bf16[64,128]{1,0:T(8,128)(2,1)}, u32[]{:S(2)}) copy-start(bf16[64,128]{1,0:T(8,128)(2,1)} %tokens_ref.3) | copy-start | bytes 49156
  40.0 38.2 %copy-start = (bf16[8,72,128]{2,1,0:T(8,128)(2,1)S(1)}, bf16[8,72,128]{2,1,0:T(8,128)(2,1)}, u32[]{:S(2)}) copy-start(bf16[8,72,128]{2,1,0:T(8,128)(2,1)} %all_to_all.25.arrived_ref) | copy-start | bytes 442372
  51.3 5.2 %collective-permute-start = (bf16[64,128]{1,0:T(8,128)(2,1)S(1)}, bf16[64,128]{1,0:T(8,128)(2,1)S(1)}, u32[]{:S(2)}, u32[]{:S(2)}) collective-permute-start(bf16[64,128]{1,0:T(8,128)(2,1)S(1)} %shard_map.142.own_ref.after_ref), channel_id=1, source_target_pairs={{0,2},{2,0},{1,3},{3,1},{4,6},{6,4},{5,7},{7,5},{8,10},{10,8},{9,1... | collective-permute-start | bytes 49160 | tf_op jit(solution)/shard_map/ppermute | solution.py:324
  57.4 20.9 %all-to-all-start.2 = ((bf16[16,128,128]{2,1,0:T(8,128)(2,1)}), bf16[16,128,128]{2,1,0:T(8,128)(2,1)S(1)}, u32[]{:S(2)}, u32[]{:S(2)}) async-start(bf16[16,128,128]{2,1,0:T(8,128)(2,1)} %shard_map.143), calls=%async_computation.2 | async-start | bytes 1048576 | tf_op jit(solution)/shard_map/all_to_all | solution.py:34
  79.0 7.0 %collective-permute-start.1 = (bf16[264,256]{1,0:T(8,128)(2,1)S(1)}, bf16[264,256]{1,0:T(8,128)(2,1)S(1)}, u32[]{:S(2)}, u32[]{:S(2)}) collective-permute-start(bf16[264,256]{1,0:T(8,128)(2,1)S(1)} %get-tuple-element.11), channel_id=1, source_target_pairs={{0,96},{32,64},{64,32},{96,0},{1,97},{33,65},{65,33},{97,1},{2,98}... | collective-permute-start | bytes 405512 | tf_op jit(solution)/shard_map/ppermute | solution.py:347
Sparse Core Ops, SparseCore 0:
  20.7 54.4 all-gather.1

commit v8 on v6

--- a/solution.py
+++ b/solution.py
@@ -17,6 +17,7 @@
 TP = ("b3", "b2", "b1", "b0", "c")
 HALF = "xh"
 COLS = ("y", "xl")
+RING = ("xh", "xl")
 NEAR = "b0"
 CORE = "c"
 FAR = ("b3", "b2", "b1")
@@ -62,7 +63,7 @@
         copy.wait()
 
 
-def pack_kernel(decay_ref, up_hbm, down_hbm, gain_hbm, out_ref, *scratch):
+def pack_kernel(decay_ref, half_ref, up_hbm, down_hbm, gain_hbm, out_ref, *scratch):
     up_ref, down_ref, gain_ref, sems = scratch
     fetch(
         (
@@ -84,9 +85,11 @@
     rows = jnp.where(row == 0, first, jnp.where(row == 1, second, jnp.where(row == 2, third, zero)))
     rows = rows.astype(bf16)
     up = up_ref[...].astype(f32).T.astype(bf16)
+    down = down_ref[...]
     for j in range(cols):
-        out_ref[j, :units] = up[j * units : (j + 1) * units]
-        out_ref[j, units : 2 * units] = down_ref[j * units : (j + 1) * units]
+        at, turned = slice(j * units, (j + 1) * units), slice((j ^ 1) * units, ((j ^ 1) + 1) * units)
+        out_ref[j, :units] = jnp.where(half_ref[0] == 0, up[at], up[turned])
+        out_ref[j, units : 2 * units] = jnp.where(half_ref[0] == 0, down[at], down[turned])
         out_ref[j, 2 * units :] = rows
 
 
@@ -193,7 +196,7 @@
 def up_kernel(rows_ref, arrived_ref, weights_ref, own_ref, sent_ref):
     cols, count, feats = rows_ref.shape
     lines = arrived_ref.shape[1]
-    far, _, units, width = weights_ref.shape
+    far, units, width = weights_ref.shape
     ones = jnp.ones((8, feats), bf16)
     total = jnp.zeros((8, count), f32)
     scaled = []
@@ -208,7 +211,7 @@
         total = total + lax.dot_general(ones, low, NT, preferred_element_type=f32)
     part = lax.dot_general(
         jnp.concatenate(scaled, axis=1),
-        weights_ref[:, 0].reshape(far * units, width),
+        weights_ref[...].reshape(far * units, width),
         NT,
         preferred_element_type=f32,
     )
@@ -232,7 +235,7 @@
     factor = lax.rsqrt(jnp.sum(mine, axis=1, keepdims=True) / D + EPS)
     raised = jnp.maximum(total[:count] * factor, 0.0)
     hidden = (raised * raised).astype(bf16)
-    weight = weights_ref[:, 1].reshape(-1, weights_ref.shape[3])
+    weight = weights_ref[...].reshape(-1, weights_ref.shape[2])
     part = jnp.dot(hidden, weight, preferred_element_type=f32).astype(bf16)
     for j in range(cols):
         out_ref[j] = part[:, j * feats : (j + 1) * feats]
@@ -273,7 +276,7 @@
         up_weight,
         down_weight,
         channel_gain.reshape(1, feats),
-        scalars=(decay,),
+        scalars=(decay, lax.axis_index(HALF)),
         hbm=(0, 1, 2),
         limit=63 << 20,
         scratch=(
@@ -340,6 +343,7 @@
     )
     rows = swap(copies, COLS + (CORE,)).reshape(cols, count, feats)
     weights = weights.reshape(far, 2, units, cols * feats)
+    ups = weights[:, 0]
     own, given = call(
         up_kernel,
         (
@@ -348,16 +352,18 @@
         ),
         rows,
         arrived,
-        weights,
+        ups,
         flops=2 * count * cols * feats * far * units,
     )
-    other = lax.ppermute(given, HALF, turn)
+    weights, given = lax.optimization_barrier((weights, given))
+    downs = weights[:, 1]
+    other = lax.ppermute(given, RING, [(0, 3), (1, 2), (2, 1), (3, 0)])
     lowered = call(
         down_kernel,
         like((cols, count, feats), bf16),
         own,
         other,
-        weights,
+        downs,
         flops=2 * count * cols * feats * far * units,
     )
 

time: 115 us -> 114 us (level)
  blocking collectives: 62.5 us -> 41.5 us
  starting transfers between devices: 11.3 us -> 21.4 us
  waiting for transfers between devices: 11.6 us -> 20.3 us
    all_to_all x4 -> x3, blocking collectives: 62.5 us -> 41.5 us  [swap(): return lax.all_to_all(blocks, axes, split_axis=0, concat_axis=0, tiled=True)]
    all_to_all x1 -> x2, starting transfers between devices: 4.44 us -> 15.1 us  [swap(): return lax.all_to_all(blocks, axes, split_axis=0, concat_axis=0, tiled=True)]
    all_gather x1, waiting for transfers between devices: 0.01 us -> 5.92 us  [layer(): weights = lax.all_gather(mine, FAR, axis=0, tiled=True)]
    all_to_all x1 -> x2, waiting for transfers between devices: 5.95 us -> 8.6 us  [swap(): return lax.all_to_all(blocks, axes, split_axis=0, concat_axis=0, tiled=True)]
    unnamed x10 -> x8, local copies, waits for them, and re-layouts: 2.66 us -> 1.45 us
    squeeze x0 -> x2, local copies, waits for them, and re-layouts: none -> 1.21 us  [the longest x1 1.17 us: layer(): ups = weights[:, 0]]
  transfers between devices with their start and end apart: 4 -> 5, of which waited for: 3 -> 5; matrix products, arithmetic and copies ran while one was open for 1% -> 2% of each run, Pallas kernels for 5% -> 6%
where the time goes in v8:
time: 114 us; the launch traced here: 113 us
  blocking collectives  41.5 us (36%)
  starting transfers between devices  21.4 us (19%)
  waiting for transfers between devices  20.3 us (18%)
  between operations  14.2 us (12%)
  Pallas kernels  11 us (10%)
  local copies, waits for them, and re-layouts  2.65 us (2%)
  other arithmetic  1.58 us (1%)
    all_to_all x3, blocking collectives, swap(): return lax.all_to_all(blocks, axes, split_axis=0, concat_axis=0, tiled=True)  41.5 us
    all_to_all x2, starting transfers between devices, swap(): return lax.all_to_all(blocks, axes, split_axis=0, concat_axis=0, tiled=True)  15.1 us
    pallas_call x9, Pallas kernels, call(): pl.pallas_call(kernel, out_shape=out, in_specs=[smem] * len(scalars) + [f...  11 us
    all_to_all x2, waiting for transfers between devices, swap(): return lax.all_to_all(blocks, axes, split_axis=0, concat_axis=0, tiled=True)  8.6 us
    all_gather x1, waiting for transfers between devices, layer(): weights = lax.all_gather(mine, FAR, axis=0, tiled=True)  5.92 us
    ppermute x1, waiting for transfers between devices, layer(): other = lax.ppermute(given, RING, [(0, 3), (1, 2), (2, 1), (3, 0)])  4.2 us
    ppermute x1, starting transfers between devices, layer(): passed = lax.ppermute(after, NEAR, turn)  3.55 us
    ppermute x1, starting transfers between devices, layer(): other = lax.ppermute(given, RING, [(0, 3), (1, 2), (2, 1), (3, 0)])  2.7 us
  transfers between devices with their start and end apart: 5, of which 5 were waited for; matrix products, arithmetic and copies ran while one was open for 2% of the time, Pallas kernels for 6%

profile of v8, /device:TPU:1, one launch (start us, length us, event | category | flops | bytes accessed | tf_op | source)
XLA Modules:
  0.0 112.5 jit_solution(18337795364143877321)
XLA Ops:
  7.2 0.0 all-gather.2.cloned.1.call-start
  7.3 1.7 %shard_map.144 = bf16[8,72,128]{2,1,0:T(8,128)(2,1)} custom-call(f32[1]{0:T(128)} %bitcast.1.decay_ref, s32[1]{0:T(128)} %bitcast.10.half_ref, bf16[128,256]{1,0:T(8,128)(2,1)} %up_hbm.1, bf16[256,128]{1,0:T(8,128)(2,1)} %down_hbm.1, f32[1,128]{1,0:T(1,128)} %bitcast.33), custom_call_target="tpu_custom_call" | custom-call | flops 1048576 | bytes 279040 | tf_op jit(solution)/shard_map/pallas_call | solution.py:44
  8.9 11.6 %all_to_all.25.arrived_ref = bf16[8,72,128]{2,1,0:T(8,128)(2,1)S(1)} all-to-all(bf16[8,72,128]{2,1,0:T(8,128)(2,1)} %shard_map.144), channel_id=1, replica_groups=mesh['y'=4,'xh'=2,'xl'=2,'b3'=2,'b2'=2,'b1'=2,'b0'=2,'c'=2] {'y','xl'}, dimensions={0} | all-to-all | bytes 294912 | tf_op jit(solution)/shard_map/all_to_all | solution.py:34
  20.5 0.7 shard_map.145
  21.2 0.0 all-gather.2.cloned.1.call-update
  21.2 0.0 copy-start
  21.2 0.7 copy-done
  21.9 0.8 shard_map.140
  22.7 4.4 %all-to-all-start = ((bf16[16,64,128]{2,1,0:T(8,128)(2,1)}), bf16[16,64,128]{2,1,0:T(8,128)(2,1)S(1)}, u32[]{:S(2)}, u32[]{:S(2)}) async-start(bf16[16,64,128]{2,1,0:T(8,128)(2,1)} %shard_map.140), calls=%async_computation | async-start | bytes 524288 | tf_op jit(solution)/shard_map/all_to_all | solution.py:34
  27.1 0.7 convert_element_type.7
  27.8 0.2 fusion
  28.0 0.7 pad_maximum_fusion
  28.7 5.9 %all-to-all-done.refs_0_ = bf16[16,64,128]{2,1,0:T(8,128)(2,1)S(1)} async-done(((bf16[16,64,128]{2,1,0:T(8,128)(2,1)}), bf16[16,64,128]{2,1,0:T(8,128)(2,1)S(1)}, u32[]{:S(2)}, u32[]{:S(2)}) %all-to-all-start) | async-done | bytes 262176 | tf_op jit(solution)/shard_map/all_to_all | solution.py:34
  34.7 0.0 copy-start.2
  34.7 0.7 copy-done.2
  35.4 0.0 copy-start.1
  35.4 5.2 %shard_map.141 = (bf16[16,64,128]{2,1,0:T(8,128)(2,1)}, f32[64,64,64]{2,1,0:T(8,128)}) custom-call(f32[1]{0:T(128)} %bitcast.1.decay_ref, bf16[16,64,128]{2,1,0:T(8,128)(2,1)} %copy-done.2, f32[1,2048]{1,0:T(1,128)} %bitcast.32, bf16[64,2048]{1,0:T(8,128)(2,1)} %bitcast.28, bf16[64,2048]{1,0:T(8,128)(2,1)} %bitcast.29, bf16[64,2048]{1,0:T(8,128)(2,1)} %bitcast.30, ...), custom_call_target="tpu_custom_call" | custom-call | flops 100663296 | bytes 3973376 | tf_op jit(solution)/shard_map/pallas_call | solution.py:44
  40.6 11.0 %all_to_all.26.parts_ref = bf16[16,64,128]{2,1,0:T(8,128)(2,1)S(1)} all-to-all(bf16[16,64,128]{2,1,0:T(8,128)(2,1)} %get-tuple-element.8), channel_id=1, replica_groups=mesh['y'=4,'xh'=2,'xl'=2,'b3'=2,'b2'=2,'b1'=2,'b0'=2,'c'=2] {'y','xh','xl'}, dimensions={0} | all-to-all | bytes 524288 | tf_op jit(solution)/shard_map/all_to_all | solution.py:34
  51.7 0.0 copy-done.1
  51.7 3.5 %collective-permute-start = (bf16[64,128]{1,0:T(8,128)(2,1)S(1)}, bf16[64,128]{1,0:T(8,128)(2,1)S(1)}, u32[]{:S(2)}, u32[]{:S(2)}) collective-permute-start(bf16[64,128]{1,0:T(8,128)(2,1)S(1)} %shard_map.142.own_ref.after_ref), channel_id=1, source_target_pairs={{0,2},{2,0},{1,3},{3,1},{4,6},{6,4},{5,7},{7,5},{8,10},{10,8},{9,1... | collective-permute-start | bytes 49160 | tf_op jit(solution)/shard_map/ppermute | solution.py:336
  55.3 1.6 %collective-permute-done.other_ref = bf16[64,128]{1,0:T(8,128)(2,1)S(1)} collective-permute-done((bf16[64,128]{1,0:T(8,128)(2,1)S(1)}, bf16[64,128]{1,0:T(8,128)(2,1)S(1)}, u32[]{:S(2)}, u32[]{:S(2)}) %collective-permute-start) | collective-permute-done | bytes 16416 | tf_op jit(solution)/shard_map/ppermute | solution.py:336
  56.9 0.9 shard_map.143
  57.8 10.7 %all-to-all-start.2 = ((bf16[16,128,128]{2,1,0:T(8,128)(2,1)}), bf16[16,128,128]{2,1,0:T(8,128)(2,1)S(1)}, u32[]{:S(2)}, u32[]{:S(2)}) async-start(bf16[16,128,128]{2,1,0:T(8,128)(2,1)} %shard_map.143), calls=%async_computation.2 | async-start | bytes 1048576 | tf_op jit(solution)/shard_map/all_to_all | solution.py:34
  68.5 5.9 %all-gather.2.cloned.1.call-done = bf16[512,1024]{1,0:T(8,128)(2,1)} async-done(((bf16[64,1024]{1,0:T(8,128)(2,1)}), bf16[512,1024]{1,0:T(8,128)(2,1)}) %all-gather.2.cloned.1.call-update) | async-done | bytes 1048592 | tf_op jit(solution)/shard_map/all_gather | solution.py:291
  74.4 0.0 copy-start.3
  74.4 1.2 %slice_bitcast_fusion.1.weights_ref = bf16[8,32,1024]{2,1,0:T(8,128)(2,1)S(1)} fusion(bf16[8,2,32,1024]{3,2,1,0:T(8,128)(2,1)} %bitcast.26), kind=kLoop, calls=%fused_computation.1 | loop fusion | bytes 1048576 | tf_op jit(solution)/shard_map/squeeze | solution.py:346
  75.6 2.7 %all-to-all-done.2 = bf16[16,128,128]{2,1,0:T(8,128)(2,1)S(1)} async-done(((bf16[16,128,128]{2,1,0:T(8,128)(2,1)}), bf16[16,128,128]{2,1,0:T(8,128)(2,1)S(1)}, u32[]{:S(2)}, u32[]{:S(2)}) %all-to-all-start.2) | async-done | bytes 524320 | tf_op jit(solution)/shard_map/all_to_all | solution.py:34
  78.2 0.6 shard_map.146
  78.8 2.7 %collective-permute-start.1 = (bf16[264,256]{1,0:T(8,128)(2,1)S(1)}, bf16[264,256]{1,0:T(8,128)(2,1)S(1)}, u32[]{:S(2)}, u32[]{:S(2)}) collective-permute-start(bf16[264,256]{1,0:T(8,128)(2,1)S(1)} %get-tuple-element.11), channel_id=1, source_target_pairs={{0,96},{32,64},{64,32},{96,0},{1,97},{33,65},{65,33},{97,1},{2,98}... | collective-permute-start | bytes 405512 | tf_op jit(solution)/shard_map/ppermute | solution.py:360
  81.5 0.0 copy-done.3
  81.6 4.2 %collective-permute-done.1.other_ref = bf16[264,256]{1,0:T(8,128)(2,1)S(1)} collective-permute-done((bf16[264,256]{1,0:T(8,128)(2,1)S(1)}, bf16[264,256]{1,0:T(8,128)(2,1)S(1)}, u32[]{:S(2)}, u32[]{:S(2)}) %collective-permute-start.1) | collective-permute-done | bytes 135200 | tf_op jit(solution)/shard_map/ppermute | solution.py:360
  85.8 0.4 shard_map.147
  86.1 18.9 %all_to_all.27.parts_ref = bf16[32,64,128]{2,1,0:T(8,128)(2,1)S(1)} all-to-all(bf16[32,64,128]{2,1,0:T(8,128)(2,1)S(1)} %bitcast.24), channel_id=1, replica_groups=mesh['y'=4,'xh'=2,'xl'=2,'b3'=2,'b2'=2,'b1'=2,'b0'=2,'c'=2] {'y','xl','c..., dimensions={0} | all-to-all | bytes 1048576 | tf_op jit(solution)/shard_map/all_to_all | solution.py:34
  105.0 0.7 shard_map.148
  (3 shorter events, 0.1 us)
Async XLA Ops:
  7.2 67.2 %all-gather.2.cloned.1.call-start = ((), (), s32[]{:S(2)}) async-start(), calls=%async_computation.5 | async-start | bytes 1179648 | tf_op jit(solution)/shard_map/all_gather | solution.py:291
  21.2 0.7 copy-start
  22.7 12.0 %all-to-all-start = ((bf16[16,64,128]{2,1,0:T(8,128)(2,1)}), bf16[16,64,128]{2,1,0:T(8,128)(2,1)S(1)}, u32[]{:S(2)}, u32[]{:S(2)}) async-start(bf16[16,64,128]{2,1,0:T(8,128)(2,1)} %shard_map.140), calls=%async_computation | async-start | bytes 524288 | tf_op jit(solution)/shard_map/all_to_all | solution.py:34
  34.7 0.7 copy-start.2
  35.4 16.3 %copy-start.1 = (bf16[64,128]{1,0:T(8,128)(2,1)S(1)}, bf16[64,128]{1,0:T(8,128)(2,1)}, u32[]{:S(2)}) copy-start(bf16[64,128]{1,0:T(8,128)(2,1)} %tokens_ref.3) | copy-start | bytes 49156
  51.7 5.1 %collective-permute-start = (bf16[64,128]{1,0:T(8,128)(2,1)S(1)}, bf16[64,128]{1,0:T(8,128)(2,1)S(1)}, u32[]{:S(2)}, u32[]{:S(2)}) collective-permute-start(bf16[64,128]{1,0:T(8,128)(2,1)S(1)} %shard_map.142.own_ref.after_ref), channel_id=1, source_target_pairs={{0,2},{2,0},{1,3},{3,1},{4,6},{6,4},{5,7},{7,5},{8,10},{10,8},{9,1... | collective-permute-start | bytes 49160 | tf_op jit(solution)/shard_map/ppermute | solution.py:336
  57.8 20.4 %all-to-all-start.2 = ((bf16[16,128,128]{2,1,0:T(8,128)(2,1)}), bf16[16,128,128]{2,1,0:T(8,128)(2,1)S(1)}, u32[]{:S(2)}, u32[]{:S(2)}) async-start(bf16[16,128,128]{2,1,0:T(8,128)(2,1)} %shard_map.143), calls=%async_computation.2 | async-start | bytes 1048576 | tf_op jit(solution)/shard_map/all_to_all | solution.py:34
  74.4 7.1 %copy-start.3 = (bf16[512,1024]{1,0:T(8,128)(2,1)S(1)}, bf16[512,1024]{1,0:T(8,128)(2,1)}, u32[]{:S(2)}) copy-start(bf16[512,1024]{1,0:T(8,128)(2,1)} %all-gather.2.cloned.1.call-done) | copy-start | bytes 3145732
  78.8 7.0 %collective-permute-start.1 = (bf16[264,256]{1,0:T(8,128)(2,1)S(1)}, bf16[264,256]{1,0:T(8,128)(2,1)S(1)}, u32[]{:S(2)}, u32[]{:S(2)}) collective-permute-start(bf16[264,256]{1,0:T(8,128)(2,1)S(1)} %get-tuple-element.11), channel_id=1, source_target_pairs={{0,96},{32,64},{64,32},{96,0},{1,97},{33,65},{65,33},{97,1},{2,98}... | collective-permute-start | bytes 405512 | tf_op jit(solution)/shard_map/ppermute | solution.py:360
Sparse Core Ops, SparseCore 0:
  21.3 53.0 all-gather.1

commit v9 on v8

--- a/solution.py
+++ b/solution.py
@@ -107,8 +107,8 @@
 
 
 def retention_kernel(decay_ref, *refs):
-    sources, (shares_ref, new_hbm) = refs[:11], refs[11:13]
-    targets, (normed_ref, readout_ref, new_ref, sems, out_sems) = refs[13:24], refs[24:]
+    sources, (shares_ref, keys_ref, values_ref) = refs[:11], refs[11:14]
+    targets, (normed_ref, readout_ref, sems) = refs[14:25], refs[25:]
     copies = [
         pltpu.make_async_copy(a, b, sems.at[n]) for n, (a, b) in enumerate(zip(sources, targets))
     ]
@@ -144,21 +144,11 @@
     keys = rotated(key_ref) * HEAD_DIM ** (-0.5)
     values = project(value_ref[...])
     gating = project(gate_ref[...])
-    columns, key_columns = queries.T, keys.T
+    keys_ref[...] = keys
+    values_ref[...] = values
+    columns = queries.T
     for copy in copies[8:]:
         copy.wait()
-    step = served // out_sems.shape[0]
-    given = [
-        pltpu.make_async_copy(
-            new_ref.at[pl.ds(n * step, step)], new_hbm.at[pl.ds(n * step, step)], out_sems.at[n]
-        )
-        for n in range(out_sems.shape[0])
-    ]
-    for b in range(served):
-        added = key_columns[:, b : b + 1] * values[b : b + 1]
-        new_ref[b] = decay_ref[0] * state_ref[b] + added
-        if b % step == step - 1 and b > step:
-            given[b // step - 1].start()
     for b in range(state_ref.shape[0]):
         readout_ref[b : b + 1] = jnp.sum(state_ref[b] * columns[:, b : b + 1], axis=0, keepdims=True)
     matched = jnp.sum(keys * queries, axis=1, keepdims=True)
@@ -167,11 +157,9 @@
     grouped = readout * lax.rsqrt(square + EPS) * gain_ref[...]
     merged = (grouped * (gating * jax.nn.sigmoid(gating))).astype(bf16)
     shares = jnp.dot(merged, output_ref[...], preferred_element_type=f32).astype(bf16)
+    feats = shares_ref.shape[2]
     for k in range(shares_ref.shape[0]):
         shares_ref[k] = shares[:, k * feats : (k + 1) * feats]
-    given[-1].start()
-    for copy in given:
-        copy.wait()
 
 
 def sum_of(parts_ref):
@@ -312,20 +300,21 @@
         output_weight,
         group_gain.reshape(1, HEAD_DIM),
     )
-    shares, new_state = call(
+    shares, keys_new, values_new = call(
         retention_kernel,
-        (like((kv, served, feats), bf16), like(state.shape, f32)),
+        (
+            like((kv, served, feats), bf16),
+            like((served, HEAD_DIM), f32),
+            like((served, HEAD_DIM), f32),
+        ),
         *operands,
         scalars=(decay,),
         hbm=tuple(range(len(operands))),
-        out_hbm=(1,),
         scratch=(
             *(pltpu.VMEM(a.shape, a.dtype) for a in operands),
             pltpu.VMEM((served, kv * feats), bf16),
             pltpu.VMEM((served, HEAD_DIM), f32),
-            pltpu.VMEM(state.shape, f32),
             pltpu.SemaphoreType.DMA((len(operands),)),
-            pltpu.SemaphoreType.DMA((4,)),
         ),
         limit=63 << 20,
         flops=2 * served * D * 6 * HEAD_DIM,
@@ -370,6 +359,7 @@
     lowered = lowered.reshape(cols * 2 * cores, served, feats)
     lowered = swap(lowered, COLS + (CORE, NEAR))
     mixed = call(final_kernel, like((served, feats), bf16), lowered, after)
+    new_state = decay * state + keys_new[:, :, None] * values_new[:, None, :]
     return (mixed, new_state[:, None])
 
 

time: 114 us -> 115 us (level)
  blocking collectives: 41.5 us -> 22.6 us
  starting transfers between devices: 21.4 us -> 30.3 us
  waiting for transfers between devices: 20.3 us -> 29.1 us
  other arithmetic: 1.58 us -> 3.26 us
    all_to_all x3 -> x2, blocking collectives: 41.5 us -> 22.6 us  [swap(): return lax.all_to_all(blocks, axes, split_axis=0, concat_axis=0, tiled=True)]
    all_to_all x2 -> x3, waiting for transfers between devices: 8.6 us -> 18.1 us  [swap(): return lax.all_to_all(blocks, axes, split_axis=0, concat_axis=0, tiled=True)]
    all_to_all x2 -> x3, starting transfers between devices: 15.1 us -> 24.4 us  [swap(): return lax.all_to_all(blocks, axes, split_axis=0, concat_axis=0, tiled=True)]
    add x0 -> x1, other arithmetic: none -> 1.68 us  [layer(): new_state = decay * state + keys_new[:, :, None] * values_new[:, None, :]]
  transfers between devices with their start and end apart: 5 -> 6, of which waited for: 5 -> 6; matrix products, arithmetic and copies ran while one was open for 2% -> 5% of each run, Pallas kernels for 6% -> 5%
where the time goes in v9:
time: 115 us; the launch traced here: 114 us
  starting transfers between devices  30.3 us (26%)
  waiting for transfers between devices  29.1 us (25%)
  blocking collectives  22.6 us (20%)
  between operations  14.2 us (12%)
  Pallas kernels  10.5 us (9%)
  local copies, waits for them, and re-layouts  3.59 us (3%)
  other arithmetic  3.26 us (3%)
    all_to_all x3, starting transfers between devices, swap(): return lax.all_to_all(blocks, axes, split_axis=0, concat_axis=0, tiled=True)  24.4 us
    all_to_all x2, blocking collectives, swap(): return lax.all_to_all(blocks, axes, split_axis=0, concat_axis=0, tiled=True)  22.6 us
    all_to_all x3, waiting for transfers between devices, swap(): return lax.all_to_all(blocks, axes, split_axis=0, concat_axis=0, tiled=True)  18.1 us
    pallas_call x9, Pallas kernels, call(): pl.pallas_call(kernel, out_shape=out, in_specs=[smem] * len(scalars) + [f...  10.5 us
    all_gather x1, waiting for transfers between devices, layer(): weights = lax.all_gather(mine, FAR, axis=0, tiled=True)  5.97 us
    ppermute x1, waiting for transfers between devices, layer(): other = lax.ppermute(given, RING, [(0, 3), (1, 2), (2, 1), (3, 0)])  3.64 us
    ppermute x1, starting transfers between devices, layer(): passed = lax.ppermute(after, NEAR, turn)  3.55 us
    ppermute x1, starting transfers between devices, layer(): other = lax.ppermute(given, RING, [(0, 3), (1, 2), (2, 1), (3, 0)])  2.36 us
  transfers between devices with their start and end apart: 6, of which 6 were waited for; matrix products, arithmetic and copies ran while one was open for 5% of the time, Pallas kernels for 5%

profile of v9, /device:TPU:1, one launch (start us, length us, event | category | flops | bytes accessed | tf_op | source)
XLA Modules:
  0.0 113.5 jit_solution(1271422322453497400)
XLA Ops:
  7.2 0.0 all-gather.2.cloned.1.call-start
  7.3 1.7 %shard_map.144 = bf16[8,72,128]{2,1,0:T(8,128)(2,1)} custom-call(f32[1]{0:T(128)} %bitcast.1.decay_ref, s32[1]{0:T(128)} %bitcast.10.half_ref, bf16[128,256]{1,0:T(8,128)(2,1)} %up_hbm.1, bf16[256,128]{1,0:T(8,128)(2,1)} %down_hbm.1, f32[1,128]{1,0:T(1,128)} %bitcast.29), custom_call_target="tpu_custom_call" | custom-call | flops 1048576 | bytes 279040 | tf_op jit(solution)/shard_map/pallas_call | solution.py:44
  8.9 11.6 %all_to_all.25.arrived_ref = bf16[8,72,128]{2,1,0:T(8,128)(2,1)S(1)} all-to-all(bf16[8,72,128]{2,1,0:T(8,128)(2,1)} %shard_map.144), channel_id=1, replica_groups=mesh['y'=4,'xh'=2,'xl'=2,'b3'=2,'b2'=2,'b1'=2,'b0'=2,'c'=2] {'y','xl'}, dimensions={0} | all-to-all | bytes 294912 | tf_op jit(solution)/shard_map/all_to_all | solution.py:34
  20.5 0.7 shard_map.145
  21.2 0.0 all-gather.2.cloned.1.call-update
  21.2 0.0 copy-start
  21.2 0.7 copy-done
  21.9 0.8 shard_map.140
  22.7 4.4 %all-to-all-start = ((bf16[16,64,128]{2,1,0:T(8,128)(2,1)}), bf16[16,64,128]{2,1,0:T(8,128)(2,1)S(1)}, u32[]{:S(2)}, u32[]{:S(2)}) async-start(bf16[16,64,128]{2,1,0:T(8,128)(2,1)} %shard_map.140), calls=%async_computation | async-start | bytes 524288 | tf_op jit(solution)/shard_map/all_to_all | solution.py:34
  27.1 0.7 convert_element_type.7
  27.8 0.2 fusion
  28.0 0.7 pad_maximum_fusion
  28.7 6.0 %all-to-all-done.refs_0_ = bf16[16,64,128]{2,1,0:T(8,128)(2,1)S(1)} async-done(((bf16[16,64,128]{2,1,0:T(8,128)(2,1)}), bf16[16,64,128]{2,1,0:T(8,128)(2,1)S(1)}, u32[]{:S(2)}, u32[]{:S(2)}) %all-to-all-start) | async-done | bytes 262176 | tf_op jit(solution)/shard_map/all_to_all | solution.py:34
  34.7 0.0 copy-start.3
  34.7 0.7 copy-done.3
  35.4 0.0 copy-start.1
  35.4 4.0 %shard_map.141 = (bf16[16,64,128]{2,1,0:T(8,128)(2,1)}, f32[64,64]{1,0:T(8,128)}, f32[64,64]{1,0:T(8,128)}) custom-call(f32[1]{0:T(128)} %bitcast.1.decay_ref, bf16[16,64,128]{2,1,0:T(8,128)(2,1)} %copy-done.3, f32[1,2048]{1,0:T(1,128)} %bitcast.28, bf16[64,2048]{1,0:T(8,128)(2,1)} %bitcast.24, bf16[64,2048]{1,0:T(8,128)(2,1)} %bitcast.25, ...), custom_call_target="tpu_custom_call" | custom-call | flops 100663296 | bytes 2957568 | tf_op jit(solution)/shard_map/pallas_call | solution.py:44
  39.4 11.0 %all_to_all.26.parts_ref = bf16[16,64,128]{2,1,0:T(8,128)(2,1)S(1)} all-to-all(bf16[16,64,128]{2,1,0:T(8,128)(2,1)} %get-tuple-element.9), channel_id=1, replica_groups=mesh['y'=4,'xh'=2,'xl'=2,'b3'=2,'b2'=2,'b1'=2,'b0'=2,'c'=2] {'y','xh','xl'}, dimensions={0} | all-to-all | bytes 524288 | tf_op jit(solution)/shard_map/all_to_all | solution.py:34
  50.4 0.0 copy-done.1
  50.4 3.5 %collective-permute-start = (bf16[64,128]{1,0:T(8,128)(2,1)S(1)}, bf16[64,128]{1,0:T(8,128)(2,1)S(1)}, u32[]{:S(2)}, u32[]{:S(2)}) collective-permute-start(bf16[64,128]{1,0:T(8,128)(2,1)S(1)} %shard_map.142.own_ref.after_ref), channel_id=1, source_target_pairs={{0,2},{2,0},{1,3},{3,1},{4,6},{6,4},{5,7},{7,5},{8,10},{10,8},{9,1... | collective-permute-start | bytes 49160 | tf_op jit(solution)/shard_map/ppermute | solution.py:325
  54.0 1.4 %collective-permute-done.other_ref = bf16[64,128]{1,0:T(8,128)(2,1)S(1)} collective-permute-done((bf16[64,128]{1,0:T(8,128)(2,1)S(1)}, bf16[64,128]{1,0:T(8,128)(2,1)S(1)}, u32[]{:S(2)}, u32[]{:S(2)}) %collective-permute-start) | collective-permute-done | bytes 16416 | tf_op jit(solution)/shard_map/ppermute | solution.py:325
  55.4 0.9 shard_map.143
  56.3 11.4 %all-to-all-start.2 = ((bf16[16,128,128]{2,1,0:T(8,128)(2,1)}), bf16[16,128,128]{2,1,0:T(8,128)(2,1)S(1)}, u32[]{:S(2)}, u32[]{:S(2)}) async-start(bf16[16,128,128]{2,1,0:T(8,128)(2,1)} %shard_map.143), calls=%async_computation.2 | async-start | bytes 1048576 | tf_op jit(solution)/shard_map/all_to_all | solution.py:34
  67.7 6.0 %all-gather.2.cloned.1.call-done = bf16[512,1024]{1,0:T(8,128)(2,1)} async-done(((bf16[64,1024]{1,0:T(8,128)(2,1)}), bf16[512,1024]{1,0:T(8,128)(2,1)}) %all-gather.2.cloned.1.call-update) | async-done | bytes 1048592 | tf_op jit(solution)/shard_map/all_gather | solution.py:279
  73.6 1.1 slice_bitcast_fusion.1.weights_ref
  74.7 2.7 %all-to-all-done.2 = bf16[16,128,128]{2,1,0:T(8,128)(2,1)S(1)} async-done(((bf16[16,128,128]{2,1,0:T(8,128)(2,1)}), bf16[16,128,128]{2,1,0:T(8,128)(2,1)S(1)}, u32[]{:S(2)}, u32[]{:S(2)}) %all-to-all-start.2) | async-done | bytes 524320 | tf_op jit(solution)/shard_map/all_to_all | solution.py:34
  77.4 0.0 copy-start.4
  77.4 0.0 copy-start.5
  77.4 0.6 shard_map.146
  78.0 0.0 copy-start.2
  78.0 2.4 %collective-permute-start.1 = (bf16[264,256]{1,0:T(8,128)(2,1)S(1)}, bf16[264,256]{1,0:T(8,128)(2,1)S(1)}, u32[]{:S(2)}, u32[]{:S(2)}) collective-permute-start(bf16[264,256]{1,0:T(8,128)(2,1)S(1)} %get-tuple-element.12), channel_id=1, source_target_pairs={{0,96},{32,64},{64,32},{96,0},{1,97},{33,65},{65,33},{97,1},{2,98}... | collective-permute-start | bytes 405512 | tf_op jit(solution)/shard_map/ppermute | solution.py:349
  80.4 1.1 slice_bitcast_fusion.weights_ref
  81.5 3.6 %collective-permute-done.1.other_ref = bf16[264,256]{1,0:T(8,128)(2,1)S(1)} collective-permute-done((bf16[264,256]{1,0:T(8,128)(2,1)S(1)}, bf16[264,256]{1,0:T(8,128)(2,1)S(1)}, u32[]{:S(2)}, u32[]{:S(2)}) %collective-permute-start.1) | collective-permute-done | bytes 135200 | tf_op jit(solution)/shard_map/ppermute | solution.py:349
  85.1 1.2 %shard_map.147 = bf16[8,256,128]{2,1,0:T(8,128)(2,1)} custom-call(f32[264,256]{1,0:T(8,128)S(1)} %get-tuple-element.10.own_ref, bf16[264,256]{1,0:T(8,128)(2,1)S(1)} %collective-permute-done.1.other_ref, bf16[8,32,1024]{2,1,0:T(8,128)(2,1)S(1)} %slice_bitcast_fusion.weights_ref), custom_call_target="tpu_custom_call" | custom-call | flops 134217728 | bytes 1454080 | tf_op jit(solution)/shard_map/pallas_call | solution.py:44
  86.3 8.6 %all-to-all-start.4 = ((bf16[32,64,128]{2,1,0:T(8,128)(2,1)}), bf16[32,64,128]{2,1,0:T(8,128)(2,1)S(1)}, u32[]{:S(2)}, u32[]{:S(2)}) async-start(bf16[32,64,128]{2,1,0:T(8,128)(2,1)} %bitcast.15), calls=%async_computation.4 | async-start | bytes 1048576 | tf_op jit(solution)/shard_map/all_to_all | solution.py:34
  94.9 0.0 copy-done.4
  94.9 0.0 copy-done.5
  94.9 0.0 copy-done.2
  94.9 1.7 %multiply_add_fusion = f32[64,1,64,64]{3,2,1,0:T(8,128)} fusion(f32[64,1,64,64]{3,2,1,0:T(8,128)S(1)} %copy-done.2, f32[64,64]{1,0:T(8,128)S(1)} %copy-done.5, f32[64,64]{1,0:T(8,128)S(1)} %copy-done.4, f32[]{:T(128)} %sub.7), kind=kLoop, calls=%fused_computation | loop fusion | flops 786432 | bytes 2129924 | tf_op jit(solution)/shard_map/add | solution.py:362
  96.6 9.4 %all-to-all-done.4.parts_ref = bf16[32,64,128]{2,1,0:T(8,128)(2,1)S(1)} async-done(((bf16[32,64,128]{2,1,0:T(8,128)(2,1)}), bf16[32,64,128]{2,1,0:T(8,128)(2,1)S(1)}, u32[]{:S(2)}, u32[]{:S(2)}) %all-to-all-start.4) | async-done | bytes 524320 | tf_op jit(solution)/shard_map/all_to_all | solution.py:34
  106.0 0.7 shard_map.148
  (2 shorter events, 0.1 us)
Async XLA Ops:
  7.2 66.5 %all-gather.2.cloned.1.call-start = ((), (), s32[]{:S(2)}) async-start(), calls=%async_computation.5 | async-start | bytes 1179648 | tf_op jit(solution)/shard_map/all_gather | solution.py:279
  21.2 0.7 copy-start
  22.7 12.0 %all-to-all-start = ((bf16[16,64,128]{2,1,0:T(8,128)(2,1)}), bf16[16,64,128]{2,1,0:T(8,128)(2,1)S(1)}, u32[]{:S(2)}, u32[]{:S(2)}) async-start(bf16[16,64,128]{2,1,0:T(8,128)(2,1)} %shard_map.140), calls=%async_computation | async-start | bytes 524288 | tf_op jit(solution)/shard_map/all_to_all | solution.py:34
  34.7 0.7 copy-start.3
  35.4 15.0 %copy-start.1 = (bf16[64,128]{1,0:T(8,128)(2,1)S(1)}, bf16[64,128]{1,0:T(8,128)(2,1)}, u32[]{:S(2)}) copy-start(bf16[64,128]{1,0:T(8,128)(2,1)} %tokens_ref.3) | copy-start | bytes 49156
  50.4 5.0 %collective-permute-start = (bf16[64,128]{1,0:T(8,128)(2,1)S(1)}, bf16[64,128]{1,0:T(8,128)(2,1)S(1)}, u32[]{:S(2)}, u32[]{:S(2)}) collective-permute-start(bf16[64,128]{1,0:T(8,128)(2,1)S(1)} %shard_map.142.own_ref.after_ref), channel_id=1, source_target_pairs={{0,2},{2,0},{1,3},{3,1},{4,6},{6,4},{5,7},{7,5},{8,10},{10,8},{9,1... | collective-permute-start | bytes 49160 | tf_op jit(solution)/shard_map/ppermute | solution.py:325
  56.3 21.1 %all-to-all-start.2 = ((bf16[16,128,128]{2,1,0:T(8,128)(2,1)}), bf16[16,128,128]{2,1,0:T(8,128)(2,1)S(1)}, u32[]{:S(2)}, u32[]{:S(2)}) async-start(bf16[16,128,128]{2,1,0:T(8,128)(2,1)} %shard_map.143), calls=%async_computation.2 | async-start | bytes 1048576 | tf_op jit(solution)/shard_map/all_to_all | solution.py:34
  77.4 17.4 %copy-start.4 = (f32[64,64]{1,0:T(8,128)S(1)}, f32[64,64]{1,0:T(8,128)}, u32[]{:S(2)}) copy-start(f32[64,64]{1,0:T(8,128)} %get-tuple-element.14) | copy-start | bytes 49156
  77.4 17.4 %copy-start.5 = (f32[64,64]{1,0:T(8,128)S(1)}, f32[64,64]{1,0:T(8,128)}, u32[]{:S(2)}) copy-start(f32[64,64]{1,0:T(8,128)} %get-tuple-element.15) | copy-start | bytes 49156
  78.0 16.9 %copy-start.2 = (f32[64,1,64,64]{3,2,1,0:T(8,128)S(1)}, f32[64,1,64,64]{3,2,1,0:T(8,128)}, u32[]{:S(2)}) copy-start(f32[64,1,64,64]{3,2,1,0:T(8,128)} %param.25) | copy-start | bytes 3145732
  78.0 7.1 %collective-permute-start.1 = (bf16[264,256]{1,0:T(8,128)(2,1)S(1)}, bf16[264,256]{1,0:T(8,128)(2,1)S(1)}, u32[]{:S(2)}, u32[]{:S(2)}) collective-permute-start(bf16[264,256]{1,0:T(8,128)(2,1)S(1)} %get-tuple-element.12), channel_id=1, source_target_pairs={{0,96},{32,64},{64,32},{96,0},{1,97},{33,65},{65,33},{97,1},{2,98}... | collective-permute-start | bytes 405512 | tf_op jit(solution)/shard_map/ppermute | solution.py:349
  86.3 19.7 %all-to-all-start.4 = ((bf16[32,64,128]{2,1,0:T(8,128)(2,1)}), bf16[32,64,128]{2,1,0:T(8,128)(2,1)S(1)}, u32[]{:S(2)}, u32[]{:S(2)}) async-start(bf16[32,64,128]{2,1,0:T(8,128)(2,1)} %bitcast.15), calls=%async_computation.4 | async-start | bytes 1048576 | tf_op jit(solution)/shard_map/all_to_all | solution.py:34
Sparse Core Ops, SparseCore 0:
  21.3 52.2 all-gather.1
